TPU v7x, 1024 devices: a whole 4x8x16 slice. The times are simulated.
1024 devices in a mesh: rep: 2 (over z_hi), fs: 64 (over z_lo, y), tp: 8 (over x, core).
Axes of the slice: x: 4, y: 8, z: 16 (z_hi: 2, z_lo: 8; z = z_hi * 8 + z_lo), core: 2. Of those that a mesh axis runs over, the one named last changes fastest.
Arguments:
- tokens: bfloat16 [65536, 2048], P(('rep', 'fs')), may hold values from -6 to 6
- norm_gain: float32 [2048], replicated, may hold values from 0.1 to 1.9
- up_weight: bfloat16 [2048, 4096], P('fs', 'tp'), may hold values from -0.125 to 0.125
- down_weight: bfloat16 [4096, 2048], P('tp', 'fs'), may hold values from -0.09375 to 0.09375
Outputs:
- result: bfloat16 [65536, 2048], P(('rep', 'fs', 'tp'))
All inputs are finite; a program needn't handle non-finite values.
Results may differ from a plain program's by a relative error of at most 0.012.
Values may be sent and summed in bfloat16 or wider, within the bound.
No kernel may reach another device: no remote copies, remote signals or barrier semaphores. Data moves between devices by JAX's collectives and lax.ppermute only.
A program may use at most 64 MiB of HBM per device.

v0:
```python
import jax
import jax.numpy as jnp
from jax import lax
from jax.experimental import pallas as pl
from jax.experimental.pallas import tpu as pltpu
from jax.sharding import Mesh
from jax.sharding import PartitionSpec as P


EPS = 1e-06
REP, Z, Y, X, CORE = 2, 8, 8, 4, 2
VMEM = pl.BlockSpec(memory_space=pltpu.VMEM)
SMEM = pl.BlockSpec(memory_space=pltpu.SMEM)


UP_STEPS = (("y", 4), ("z", 4), ("y", 2), ("z", 2), ("z", 1), ("y", 1))
DOWN_STEPS = (("y", 4), ("z", 4), ("z", 2), ("y", 2), ("y", 1), ("z", 1))


def from_side(array, axis, shift):
    names, size = (("y", "core"), Y) if axis == "y" else (("rep", "z", "core"), REP * Z)
    pairs = []
    for i in range(size):
        pairs.append(((i + shift) % size * 2, i * 2))
        pairs.append(((i - shift) % size * 2 + 1, i * 2 + 1))
    return lax.ppermute(array, names, pairs)


def along_x(array, forward):
    pairs = []
    for x in range(X):
        pairs.append((x * 2, (x + forward) % X * 2))
        pairs.append((x * 2 + 1, (x - forward) % X * 2 + 1))
    return lax.ppermute(array, ("x", "core"), pairs)


def offsets(steps):
    laid = [(0, 0)]
    for axis, shift in steps:
        dz, dy = (shift, 0) if axis == "z" else (0, shift)
        laid = laid + [(z + dz, y + dy) for z, y in laid]
    return laid


def kernel_call(kernel, outs, n_vmem, scratch=(), smem=True, mib=8, flops=0, **rest):
    single = not isinstance(outs, tuple)
    return pl.pallas_call(
        kernel,
        out_shape=outs,
        in_specs=([SMEM] if smem else []) + [VMEM] * n_vmem,
        out_specs=VMEM if single else (VMEM,) * len(outs),
        scratch_shapes=[pltpu.VMEM(s, jnp.bfloat16) for s in scratch],
        compiler_params=pltpu.CompilerParams(vmem_limit_bytes=mib * 2**20),
        cost_estimate=pl.CostEstimate(
            flops=flops, bytes_accessed=2**20, transcendentals=0
        )
        if flops
        else None,
        **rest,
    )


def bf16(*shape):
    return jax.ShapeDtypeStruct(shape, jnp.bfloat16)


def pair_kernel(up, down, out, sem):
    first = pltpu.make_async_copy(up, out.at[0, 0], sem.at[0])
    second = pltpu.make_async_copy(down, out.at[1, 0], sem.at[1])
    first.start()
    second.start()
    first.wait()
    second.wait()


def pair(up, down):
    return pl.pallas_call(
        pair_kernel,
        out_shape=bf16(2, 1, 32, 512),
        in_specs=[pl.BlockSpec(memory_space=pltpu.HBM)] * 2,
        out_specs=VMEM,
        scratch_shapes=[pltpu.SemaphoreType.DMA((2,))],
        compiler_params=pltpu.CompilerParams(vmem_limit_bytes=2**20),
    )(up, down)


def join_kernel(a, b, out):
    n = a.shape[0]
    out[:n] = a[...]
    out[n:] = b[...]


def join(a, b):
    n = a.shape[0]
    return kernel_call(join_kernel, bf16(2 * n, 32, 512), 2, smem=False)(a, b)


def join_both_kernel(a, b, out):
    n = a.shape[1]
    out[:, :n] = a[...]
    out[:, n:] = b[...]


def join_both(a, b):
    n = a.shape[1]
    return kernel_call(join_both_kernel, bf16(2, 2 * n, 32, 512), 2, smem=False)(a, b)


def join_apart_kernel(a, b, up, down):
    n = a.shape[1]
    for k, out in enumerate((up, down)):
        out[:n] = a[k]
        out[n:] = b[k]


def join_apart(a, b):
    out = bf16(2 * a.shape[1], 32, 512)
    return kernel_call(join_apart_kernel, (out, out), 2, smem=False)(a, b)


def place(where, piece, laid, whole, halved):
    z, y, sign = where[0], where[1], where[3]
    for j, (dz, dy) in enumerate(laid):
        at_z = (z + sign * dz) & (Z - 1)
        at_y = (y + sign * dy) & (Y - 1)
        at = ((at_z >> 1) if halved else at_z) * Y + at_y
        whole[pl.ds(pl.multiple_of(at * 32, 32), 32), :] = piece[j]


def down_product(hidden, down, theirs, own, part):
    @pl.loop(0, 4)
    def _(n):
        columns = pl.ds(pl.multiple_of(n * 256, 256), 256)
        made = lax.dot_general(
            hidden[...],
            down[columns, :],
            (((1,), (1,)), ((), ())),
            preferred_element_type=jnp.float32,
        ).astype(jnp.bfloat16)
        theirs[part, :, columns] = made[:256]
        own[part, :, columns] = made[256:]


def early_kernel(where, normed, u0, u1, d0, theirs, own, hidden, up, down):
    laid = offsets(UP_STEPS)
    place(where, u0, laid[:32], up, False)
    place(where, u1, laid[32:], up, False)
    core = where[2]

    @pl.loop(0, 2)
    def _(n):
        columns = pl.ds(pl.multiple_of(n * 256, 256), 256)
        lifted = jnp.dot(
            normed[...], up[:, columns], preferred_element_type=jnp.float32
        )
        active = jnp.square(jnp.maximum(lifted, 0.0)).astype(jnp.bfloat16)
        for j in range(X * CORE):
            x, c = divmod(j, CORE)
            side = jnp.where(core == c, 256, 0)
            rows = pl.ds(pl.multiple_of(side + x * 64, 64), 64)
            hidden[rows, columns] = active[j * 64 : (j + 1) * 64]

    place(where, d0, offsets(DOWN_STEPS)[:32], down, True)
    down_product(hidden, down, theirs, own, 0)


def late_kernel(where, hidden, d1, theirs_in, own_in, theirs, own, down):
    place(where, d1, offsets(DOWN_STEPS)[32:], down, True)
    down_product(hidden, down, theirs, own, 1)


def add_kernel(where, own, beside, keep, ahead, back, far):
    x, sign = where[4], where[3]
    for out, step in ((far, 2), (back, -sign), (ahead, sign), (keep, 0)):
        rows = pl.ds(pl.multiple_of(((x + step) & (X - 1)) * 64, 64), 64)
        for part in range(2):
            total = own[part, rows].astype(jnp.float32)
            total = total + beside[part, rows].astype(jnp.float32)
            out[part] = total.astype(jnp.bfloat16)


def sum_kernel(a, b, out):
    out[...] = (a[...].astype(jnp.float32) + b[...].astype(jnp.float32)).astype(
        jnp.bfloat16
    )


def last_kernel(where, residual, a, b, c, out):
    odd = where[0] & 1
    for part in range(2):
        for k in range(4):
            at = (2 * k + (odd ^ part)) * 256
            columns = pl.ds(pl.multiple_of(at, 256), 256)
            here = slice(k * 256, (k + 1) * 256)
            total = residual[:, columns].astype(jnp.float32)
            for term in (a, b, c):
                total = total + term[part, :, here].astype(jnp.float32)
            out[:, columns] = total.astype(jnp.bfloat16)


def gathered(up_weight, down_weight):
    held = pair(up_weight, down_weight.T)
    held = join_both(held, from_side(held, *UP_STEPS[0]))
    up, down = join_apart(held, from_side(held, *UP_STEPS[1]))
    for k in range(2, 5):
        up_in = from_side(up, *UP_STEPS[k])
        down_in = from_side(down, *DOWN_STEPS[k])
        up, down = join(up, up_in), join(down, down_in)
    up_in = from_side(up, *UP_STEPS[5])
    down_in = from_side(down, *DOWN_STEPS[5])
    return (up, up_in), (down, down_in)


def over_tp(where, theirs, own, residual):
    beside = lax.ppermute(theirs, "core", [(0, 1), (1, 0)])
    piece = bf16(2, 64, 1024)
    keep, ahead, back, far = kernel_call(add_kernel, (piece,) * 4, 2)(
        where, own, beside
    )
    far_in = along_x(far, 1)
    back_in = along_x(back, -1)
    ahead = kernel_call(sum_kernel, piece, 2, smem=False)(ahead, far_in)
    ahead_in = along_x(ahead, 1)
    return kernel_call(last_kernel, bf16(64, 2048), 4)(
        where, residual, keep, back_in, ahead_in
    )


def shards(tokens, norm_gain, up_weight, down_weight):
    core, x = lax.axis_index("core"), lax.axis_index("x")
    (u0, u1), (d0, d1) = gathered(up_weight, down_weight)
    xf = tokens.astype(jnp.float32)
    scale = lax.rsqrt(jnp.mean(xf * xf, axis=-1, keepdims=True) + EPS)
    normed = (xf * scale * norm_gain).astype(jnp.bfloat16)
    where = jnp.stack(
        [lax.axis_index("z"), lax.axis_index("y"), core, 1 - 2 * core, x]
    ).astype(jnp.int32)
    residual = lax.dynamic_slice_in_dim(tokens, (x * CORE + core) * 64, 64, 0)
    out = bf16(2, 256, 1024)
    theirs, own, hidden = kernel_call(
        early_kernel,
        (out, out, bf16(512, 512)),
        4,
        scratch=((2048, 512), (1024, 512)),
        mib=14,
        flops=3 * 2**29,
    )(where, normed, u0, u1, d0)
    theirs, own = kernel_call(
        late_kernel,
        (out, out),
        4,
        scratch=((1024, 512),),
        mib=8,
        flops=2**29,
        input_output_aliases={3: 0, 4: 1},
    )(where, hidden, d1, theirs, own)
    return over_tp(where, theirs, own, residual)


def solution(mesh):
    torus = Mesh(
        mesh.devices.reshape(REP, Z, Y, X, CORE), ("rep", "z", "y", "x", "core")
    )
    rep_fs = ("rep", "z", "y")
    tp = ("x", "core")
    in_specs = (P(rep_fs, None), P(), P(("z", "y"), tp), P(tp, ("z", "y")))
    return jax.shard_map(
        shards,
        mesh=torus,
        in_specs=in_specs,
        out_specs=P(rep_fs + tp, None),
        check_vma=False,
    )
```

profile of v0, /device:TPU:56, one launch (start us, length us, event | category | flops | bytes accessed | tf_op | source)
XLA Modules:
  0.0 123.3 jit_solution(9850116296834385922)
XLA Ops:
  0.0 0.8 copy-done
  1.6 4.7 %collective-permute-start = (bf16[2,1,32,512]{3,2,1,0:T(8,128)(2,1)S(1)}, bf16[2,1,32,512]{3,2,1,0:T(8,128)(2,1)S(1)}, u32[]{:S(2)}, u32[]{:S(2)}) collective-permute-start(bf16[2,1,32,512]{3,2,1,0:T(8,128)(2,1)S(1)} %shard_map.46.a), channel_id=1, source_target_pairs={{32,0},{33,1},{40,8},{41,9},{48,16},{49,17},{56,24},{57,25},{0,32}... | collective-permute-start | bytes 196616 | tf_op jit(solution)/shard_map/ppermute | solution.py:26
  6.3 6.3 %collective-permute-done.b = bf16[2,1,32,512]{3,2,1,0:T(8,128)(2,1)S(1)} collective-permute-done((bf16[2,1,32,512]{3,2,1,0:T(8,128)(2,1)S(1)}, bf16[2,1,32,512]{3,2,1,0:T(8,128)(2,1)S(1)}, u32[]{:S(2)}, u32[]{:S(2)}) %collective-permute-start) | collective-permute-done | bytes 65568 | tf_op jit(solution)/shard_map/ppermute | solution.py:26
  12.6 18.2 %collective-permute-start.1 = (bf16[2,2,32,512]{3,2,1,0:T(8,128)(2,1)S(1)}, bf16[2,2,32,512]{3,2,1,0:T(8,128)(2,1)S(1)}, u32[]{:S(2)}, u32[]{:S(2)}) collective-permute-start(bf16[2,2,32,512]{3,2,1,0:T(8,128)(2,1)S(1)} %shard_map.47.a), channel_id=1, source_target_pairs={{256,0},{769,1},{320,64},{833,65},{384,128},{897,129},{448,192},{9... | collective-permute-start | bytes 393224 | tf_op jit(solution)/shard_map/ppermute | solution.py:26
  30.8 6.9 %collective-permute-done.1.b = bf16[2,2,32,512]{3,2,1,0:T(8,128)(2,1)S(1)} collective-permute-done((bf16[2,2,32,512]{3,2,1,0:T(8,128)(2,1)S(1)}, bf16[2,2,32,512]{3,2,1,0:T(8,128)(2,1)S(1)}, u32[]{:S(2)}, u32[]{:S(2)}) %collective-permute-start.1) | collective-permute-done | bytes 131104 | tf_op jit(solution)/shard_map/ppermute | solution.py:26
  37.8 3.4 %collective-permute-start.2 = (bf16[4,32,512]{2,1,0:T(8,128)(2,1)S(1)}, bf16[4,32,512]{2,1,0:T(8,128)(2,1)S(1)}, u32[]{:S(2)}, u32[]{:S(2)}) collective-permute-start(bf16[4,32,512]{2,1,0:T(8,128)(2,1)S(1)} %get-tuple-element.16.a), channel_id=1, source_target_pairs={{16,0},{49,1},{24,8},{57,9},{32,16},{1,17},{40,24},{9,25},{48,32},... | collective-permute-start | bytes 393224 | tf_op jit(solution)/shard_map/ppermute | solution.py:26
  41.2 5.7 %collective-permute-start.6 = (bf16[4,32,512]{2,1,0:T(8,128)(2,1)S(1)}, bf16[4,32,512]{2,1,0:T(8,128)(2,1)S(1)}, u32[]{:S(2)}, u32[]{:S(2)}) collective-permute-start(bf16[4,32,512]{2,1,0:T(8,128)(2,1)S(1)} %get-tuple-element.17.a), channel_id=1, source_target_pairs={{128,0},{897,1},{192,64},{961,65},{256,128},{1,129},{320,192},{65,... | collective-permute-start | bytes 393224 | tf_op jit(solution)/shard_map/ppermute | solution.py:26
  47.4 6.0 %collective-permute-start.3 = (bf16[8,32,512]{2,1,0:T(8,128)(2,1)S(1)}, bf16[8,32,512]{2,1,0:T(8,128)(2,1)S(1)}, u32[]{:S(2)}, u32[]{:S(2)}) collective-permute-start(bf16[8,32,512]{2,1,0:T(8,128)(2,1)S(1)} %shard_map.49.a), channel_id=1, source_target_pairs={{128,0},{897,1},{192,64},{961,65},{256,128},{1,129},{320,192},{65,... | collective-permute-start | bytes 786440 | tf_op jit(solution)/shard_map/ppermute | solution.py:26
  53.4 1.9 %collective-permute-start.7 = (bf16[8,32,512]{2,1,0:T(8,128)(2,1)S(1)}, bf16[8,32,512]{2,1,0:T(8,128)(2,1)S(1)}, u32[]{:S(2)}, u32[]{:S(2)}) collective-permute-start(bf16[8,32,512]{2,1,0:T(8,128)(2,1)S(1)} %shard_map.52.a), channel_id=1, source_target_pairs={{16,0},{49,1},{24,8},{57,9},{32,16},{1,17},{40,24},{9,25},{48,32},... | collective-permute-start | bytes 786440 | tf_op jit(solution)/shard_map/ppermute | solution.py:26
  55.3 3.8 %collective-permute-done.3.b = bf16[8,32,512]{2,1,0:T(8,128)(2,1)S(1)} collective-permute-done((bf16[8,32,512]{2,1,0:T(8,128)(2,1)S(1)}, bf16[8,32,512]{2,1,0:T(8,128)(2,1)S(1)}, u32[]{:S(2)}, u32[]{:S(2)}) %collective-permute-start.3) | collective-permute-done | bytes 262176 | tf_op jit(solution)/shard_map/ppermute | solution.py:26
  59.2 5.8 %collective-permute-start.4 = (bf16[16,32,512]{2,1,0:T(8,128)(2,1)S(1)}, bf16[16,32,512]{2,1,0:T(8,128)(2,1)S(1)}, u32[]{:S(2)}, u32[]{:S(2)}) collective-permute-start(bf16[16,32,512]{2,1,0:T(8,128)(2,1)S(1)} %shard_map.50.a), channel_id=1, source_target_pairs={{64,0},{961,1},{128,64},{1,65},{192,128},{65,129},{256,192},{129,1... | collective-permute-start | bytes 1572872 | tf_op jit(solution)/shard_map/ppermute | solution.py:26
  65.0 1.3 %collective-permute-done.7.b = bf16[8,32,512]{2,1,0:T(8,128)(2,1)S(1)} collective-permute-done((bf16[8,32,512]{2,1,0:T(8,128)(2,1)S(1)}, bf16[8,32,512]{2,1,0:T(8,128)(2,1)S(1)}, u32[]{:S(2)}, u32[]{:S(2)}) %collective-permute-start.7) | collective-permute-done | bytes 262176 | tf_op jit(solution)/shard_map/ppermute | solution.py:26
  66.3 3.8 %collective-permute-start.8 = (bf16[16,32,512]{2,1,0:T(8,128)(2,1)S(1)}, bf16[16,32,512]{2,1,0:T(8,128)(2,1)S(1)}, u32[]{:S(2)}, u32[]{:S(2)}) collective-permute-start(bf16[16,32,512]{2,1,0:T(8,128)(2,1)S(1)} %shard_map.53.a), channel_id=1, source_target_pairs={{8,0},{57,1},{16,8},{1,9},{24,16},{9,17},{32,24},{17,25},{40,32},{... | collective-permute-start | bytes 1572872 | tf_op jit(solution)/shard_map/ppermute | solution.py:26
  70.2 1.5 %collective-permute-done.4.b = bf16[16,32,512]{2,1,0:T(8,128)(2,1)S(1)} collective-permute-done((bf16[16,32,512]{2,1,0:T(8,128)(2,1)S(1)}, bf16[16,32,512]{2,1,0:T(8,128)(2,1)S(1)}, u32[]{:S(2)}, u32[]{:S(2)}) %collective-permute-start.4) | collective-permute-done | bytes 524320 | tf_op jit(solution)/shard_map/ppermute | solution.py:26
  71.8 3.8 %collective-permute-start.5 = (bf16[32,32,512]{2,1,0:T(8,128)(2,1)S(1)}, bf16[32,32,512]{2,1,0:T(8,128)(2,1)}, u32[]{:S(2)}, u32[]{:S(2)}) collective-permute-start(bf16[32,32,512]{2,1,0:T(8,128)(2,1)S(1)} %shard_map.51.u0), channel_id=1, source_target_pairs={{8,0},{57,1},{16,8},{1,9},{24,16},{9,17},{32,24},{17,25},{40,32},{... | collective-permute-start | bytes 3145736 | tf_op jit(solution)/shard_map/ppermute | solution.py:26
  75.5 3.2 %collective-permute-done.8.b = bf16[16,32,512]{2,1,0:T(8,128)(2,1)S(1)} collective-permute-done((bf16[16,32,512]{2,1,0:T(8,128)(2,1)S(1)}, bf16[16,32,512]{2,1,0:T(8,128)(2,1)S(1)}, u32[]{:S(2)}, u32[]{:S(2)}) %collective-permute-start.8) | collective-permute-done | bytes 524320 | tf_op jit(solution)/shard_map/ppermute | solution.py:26
  78.8 3.8 %collective-permute-start.9 = (bf16[32,32,512]{2,1,0:T(8,128)(2,1)S(1)}, bf16[32,32,512]{2,1,0:T(8,128)(2,1)S(1)}, u32[]{:S(2)}, u32[]{:S(2)}) collective-permute-start(bf16[32,32,512]{2,1,0:T(8,128)(2,1)S(1)} %shard_map.54.d0), channel_id=1, source_target_pairs={{64,0},{961,1},{128,64},{1,65},{192,128},{65,129},{256,192},{129,1... | collective-permute-start | bytes 3145736 | tf_op jit(solution)/shard_map/ppermute | solution.py:26
  83.2 2.1 %fusion.2.normed = bf16[512,2048]{1,0:T(8,128)(2,1)S(1)} fusion(bf16[512,2048]{1,0:T(8,128)(2,1)} %param.4, f32[2048]{0:T(1024)S(1)} %copy-done.3, f32[512]{0:T(512)S(1)} %add_rsqrt_fusion), kind=kLoop, calls=%fused_computation.4 | loop fusion | flops 4194304 | bytes 4204544 | tf_op jit(solution)/shard_map/convert_element_type | solution.py:234
  85.3 4.8 %collective-permute-done.5.u1 = bf16[32,32,512]{2,1,0:T(8,128)(2,1)} collective-permute-done((bf16[32,32,512]{2,1,0:T(8,128)(2,1)S(1)}, bf16[32,32,512]{2,1,0:T(8,128)(2,1)}, u32[]{:S(2)}, u32[]{:S(2)}) %collective-permute-start.5) | collective-permute-done | bytes 1048608 | tf_op jit(solution)/shard_map/ppermute | solution.py:26
  90.1 4.3 %shard_map.55 = (bf16[2,256,1024]{2,1,0:T(8,128)(2,1)S(1)}, bf16[2,256,1024]{2,1,0:T(8,128)(2,1)S(1)}, bf16[512,512]{1,0:T(8,128)(2,1)S(1)}) custom-call(s32[5]{0:T(128)S(1)} %stack.23.where, bf16[512,2048]{1,0:T(8,128)(2,1)S(1)} %fusion.2.normed, bf16[32,32,512]{2,1,0:T(8,128)(2,1)S(1)} %shard_map.51.u0, bf16[32,32,512]{2,1,0:T(8,128)(2,1)} %collective-permute-done.5.u1, ...), custom_call_target="tpu_custom_call" | custom-call | flops 1610612736 | bytes 1048576 | tf_op jit(solution)/shard_map/pallas_call | solution.py:240
  94.4 1.1 collective-permute-done.9.d1
  95.5 2.0 %shard_map.56 = (bf16[2,256,1024]{2,1,0:T(8,128)(2,1)S(1)}, bf16[2,256,1024]{2,1,0:T(8,128)(2,1)S(1)}) custom-call(s32[5]{0:T(128)S(1)} %stack.23.where, bf16[512,512]{1,0:T(8,128)(2,1)S(1)} %get-tuple-element.18.hidden, bf16[32,32,512]{2,1,0:T(8,128)(2,1)S(1)} %collective-permute-done.9.d1, ...), custom_call_target="tpu_custom_call", output_to_operand_aliasing={{0}: (3, {}), {1}: (4, {})} | custom-call | flops 536870912 | bytes 1048576 | tf_op jit(solution)/shard_map/pallas_call | solution.py:248
  97.5 1.9 %collective-permute-start.10 = (bf16[2,256,1024]{2,1,0:T(8,128)(2,1)S(1)}, bf16[2,256,1024]{2,1,0:T(8,128)(2,1)S(1)}, u32[]{:S(2)}, u32[]{:S(2)}) collective-permute-start(bf16[2,256,1024]{2,1,0:T(8,128)(2,1)S(1)} %get-tuple-element.22), channel_id=1, source_target_pairs={{0,1},{1,0},{2,3},{3,2},{4,5},{5,4},{6,7},{7,6},{8,9},{9,8},{10,11... | collective-permute-start | bytes 3145736 | tf_op jit(solution)/shard_map/ppermute | solution.py:215
  99.4 2.6 %collective-permute-done.10.beside = bf16[2,256,1024]{2,1,0:T(8,128)(2,1)S(1)} collective-permute-done((bf16[2,256,1024]{2,1,0:T(8,128)(2,1)S(1)}, bf16[2,256,1024]{2,1,0:T(8,128)(2,1)S(1)}, u32[]{:S(2)}, u32[]{:S(2)}) %collective-permute-start.10) | collective-permute-done | bytes 1048608 | tf_op jit(solution)/shard_map/ppermute | solution.py:215
  102.0 0.8 shard_map.57
  102.8 3.1 %collective-permute-start.12 = (bf16[2,64,1024]{2,1,0:T(8,128)(2,1)S(1)}, bf16[2,64,1024]{2,1,0:T(8,128)(2,1)S(1)}, u32[]{:S(2)}, u32[]{:S(2)}) collective-permute-start(bf16[2,64,1024]{2,1,0:T(8,128)(2,1)S(1)} %get-tuple-element.26), channel_id=1, source_target_pairs={{0,2},{1,7},{2,4},{3,1},{4,6},{5,3},{6,0},{7,5},{8,10},{9,15},{10,... | collective-permute-start | bytes 786440 | tf_op jit(solution)/shard_map/ppermute | solution.py:34
  105.9 4.0 %collective-permute-start.11 = (bf16[2,64,1024]{2,1,0:T(8,128)(2,1)S(1)}, bf16[2,64,1024]{2,1,0:T(8,128)(2,1)S(1)}, u32[]{:S(2)}, u32[]{:S(2)}) collective-permute-start(bf16[2,64,1024]{2,1,0:T(8,128)(2,1)S(1)} %get-tuple-element.24), channel_id=1, source_target_pairs={{0,6},{1,3},{2,0},{3,5},{4,2},{5,7},{6,4},{7,1},{8,14},{9,11},{10,... | collective-permute-start | bytes 786440 | tf_op jit(solution)/shard_map/ppermute | solution.py:34
  109.9 2.4 %collective-permute-done.12.b = bf16[2,64,1024]{2,1,0:T(8,128)(2,1)S(1)} collective-permute-done((bf16[2,64,1024]{2,1,0:T(8,128)(2,1)S(1)}, bf16[2,64,1024]{2,1,0:T(8,128)(2,1)S(1)}, u32[]{:S(2)}, u32[]{:S(2)}) %collective-permute-start.12) | collective-permute-done | bytes 262176 | tf_op jit(solution)/shard_map/ppermute | solution.py:34
  112.4 2.3 %collective-permute-start.13 = (bf16[2,64,1024]{2,1,0:T(8,128)(2,1)S(1)}, bf16[2,64,1024]{2,1,0:T(8,128)(2,1)S(1)}, u32[]{:S(2)}, u32[]{:S(2)}) collective-permute-start(bf16[2,64,1024]{2,1,0:T(8,128)(2,1)S(1)} %shard_map.58), channel_id=1, source_target_pairs={{0,2},{1,7},{2,4},{3,1},{4,6},{5,3},{6,0},{7,5},{8,10},{9,15},{10,... | collective-permute-start | bytes 786440 | tf_op jit(solution)/shard_map/ppermute | solution.py:34
  114.7 1.0 constant_dynamic-slice_fusion.residual
  115.7 6.1 %collective-permute-done.13.c = bf16[2,64,1024]{2,1,0:T(8,128)(2,1)S(1)} collective-permute-done((bf16[2,64,1024]{2,1,0:T(8,128)(2,1)S(1)}, bf16[2,64,1024]{2,1,0:T(8,128)(2,1)S(1)}, u32[]{:S(2)}, u32[]{:S(2)}) %collective-permute-start.13) | collective-permute-done | bytes 262176 | tf_op jit(solution)/shard_map/ppermute | solution.py:34
  121.9 1.4 %shard_map.59 = bf16[64,2048]{1,0:T(8,128)(2,1)} custom-call(s32[5]{0:T(128)S(1)} %stack.23.where, bf16[64,2048]{1,0:T(8,128)(2,1)S(1)} %constant_dynamic-slice_fusion.residual, bf16[2,64,1024]{2,1,0:T(8,128)(2,1)S(1)} %get-tuple-element.23.a, bf16[2,64,1024]{2,1,0:T(8,128)(2,1)S(1)} %collective-permute-done.11.b, ...), custom_call_target="tpu_custom_call" | custom-call | tf_op jit(solution)/shard_map/pallas_call | solution.py:224
  (23 shorter events, 2.3 us)
Async XLA Ops:
  0.0 0.8 copy-start
  0.8 0.8 copy-start.1
  1.6 11.0 %collective-permute-start = (bf16[2,1,32,512]{3,2,1,0:T(8,128)(2,1)S(1)}, bf16[2,1,32,512]{3,2,1,0:T(8,128)(2,1)S(1)}, u32[]{:S(2)}, u32[]{:S(2)}) collective-permute-start(bf16[2,1,32,512]{3,2,1,0:T(8,128)(2,1)S(1)} %shard_map.46.a), channel_id=1, source_target_pairs={{32,0},{33,1},{40,8},{41,9},{48,16},{49,17},{56,24},{57,25},{0,32}... | collective-permute-start | bytes 196616 | tf_op jit(solution)/shard_map/ppermute | solution.py:26
  12.6 25.1 %collective-permute-start.1 = (bf16[2,2,32,512]{3,2,1,0:T(8,128)(2,1)S(1)}, bf16[2,2,32,512]{3,2,1,0:T(8,128)(2,1)S(1)}, u32[]{:S(2)}, u32[]{:S(2)}) collective-permute-start(bf16[2,2,32,512]{3,2,1,0:T(8,128)(2,1)S(1)} %shard_map.47.a), channel_id=1, source_target_pairs={{256,0},{769,1},{320,64},{833,65},{384,128},{897,129},{448,192},{9... | collective-permute-start | bytes 393224 | tf_op jit(solution)/shard_map/ppermute | solution.py:26
  37.8 9.6 %collective-permute-start.2 = (bf16[4,32,512]{2,1,0:T(8,128)(2,1)S(1)}, bf16[4,32,512]{2,1,0:T(8,128)(2,1)S(1)}, u32[]{:S(2)}, u32[]{:S(2)}) collective-permute-start(bf16[4,32,512]{2,1,0:T(8,128)(2,1)S(1)} %get-tuple-element.16.a), channel_id=1, source_target_pairs={{16,0},{49,1},{24,8},{57,9},{32,16},{1,17},{40,24},{9,25},{48,32},... | collective-permute-start | bytes 393224 | tf_op jit(solution)/shard_map/ppermute | solution.py:26
  41.2 12.2 %collective-permute-start.6 = (bf16[4,32,512]{2,1,0:T(8,128)(2,1)S(1)}, bf16[4,32,512]{2,1,0:T(8,128)(2,1)S(1)}, u32[]{:S(2)}, u32[]{:S(2)}) collective-permute-start(bf16[4,32,512]{2,1,0:T(8,128)(2,1)S(1)} %get-tuple-element.17.a), channel_id=1, source_target_pairs={{128,0},{897,1},{192,64},{961,65},{256,128},{1,129},{320,192},{65,... | collective-permute-start | bytes 393224 | tf_op jit(solution)/shard_map/ppermute | solution.py:26
  47.4 11.7 %collective-permute-start.3 = (bf16[8,32,512]{2,1,0:T(8,128)(2,1)S(1)}, bf16[8,32,512]{2,1,0:T(8,128)(2,1)S(1)}, u32[]{:S(2)}, u32[]{:S(2)}) collective-permute-start(bf16[8,32,512]{2,1,0:T(8,128)(2,1)S(1)} %shard_map.49.a), channel_id=1, source_target_pairs={{128,0},{897,1},{192,64},{961,65},{256,128},{1,129},{320,192},{65,... | collective-permute-start | bytes 786440 | tf_op jit(solution)/shard_map/ppermute | solution.py:26
  53.4 12.8 %collective-permute-start.7 = (bf16[8,32,512]{2,1,0:T(8,128)(2,1)S(1)}, bf16[8,32,512]{2,1,0:T(8,128)(2,1)S(1)}, u32[]{:S(2)}, u32[]{:S(2)}) collective-permute-start(bf16[8,32,512]{2,1,0:T(8,128)(2,1)S(1)} %shard_map.52.a), channel_id=1, source_target_pairs={{16,0},{49,1},{24,8},{57,9},{32,16},{1,17},{40,24},{9,25},{48,32},... | collective-permute-start | bytes 786440 | tf_op jit(solution)/shard_map/ppermute | solution.py:26
  59.2 12.5 %collective-permute-start.4 = (bf16[16,32,512]{2,1,0:T(8,128)(2,1)S(1)}, bf16[16,32,512]{2,1,0:T(8,128)(2,1)S(1)}, u32[]{:S(2)}, u32[]{:S(2)}) collective-permute-start(bf16[16,32,512]{2,1,0:T(8,128)(2,1)S(1)} %shard_map.50.a), channel_id=1, source_target_pairs={{64,0},{961,1},{128,64},{1,65},{192,128},{65,129},{256,192},{129,1... | collective-permute-start | bytes 1572872 | tf_op jit(solution)/shard_map/ppermute | solution.py:26
  66.3 16.3 %copy-start.2 = (bf16[512,2048]{1,0:T(8,128)(2,1)S(1)}, bf16[512,2048]{1,0:T(8,128)(2,1)}, u32[]{:S(2)}) copy-start(bf16[512,2048]{1,0:T(8,128)(2,1)} %param.4) | copy-start | bytes 6291460
  66.3 12.4 %collective-permute-start.8 = (bf16[16,32,512]{2,1,0:T(8,128)(2,1)S(1)}, bf16[16,32,512]{2,1,0:T(8,128)(2,1)S(1)}, u32[]{:S(2)}, u32[]{:S(2)}) collective-permute-start(bf16[16,32,512]{2,1,0:T(8,128)(2,1)S(1)} %shard_map.53.a), channel_id=1, source_target_pairs={{8,0},{57,1},{16,8},{1,9},{24,16},{9,17},{32,24},{17,25},{40,32},{... | collective-permute-start | bytes 1572872 | tf_op jit(solution)/shard_map/ppermute | solution.py:26
  71.8 11.4 %copy-start.3 = (f32[2048]{0:T(1024)S(1)}, f32[2048]{0:T(1024)}, u32[]{:S(2)}) copy-start(f32[2048]{0:T(1024)} %param.5) | copy-start | bytes 24580
  71.8 18.3 %collective-permute-start.5 = (bf16[32,32,512]{2,1,0:T(8,128)(2,1)S(1)}, bf16[32,32,512]{2,1,0:T(8,128)(2,1)}, u32[]{:S(2)}, u32[]{:S(2)}) collective-permute-start(bf16[32,32,512]{2,1,0:T(8,128)(2,1)S(1)} %shard_map.51.u0), channel_id=1, source_target_pairs={{8,0},{57,1},{16,8},{1,9},{24,16},{9,17},{32,24},{17,25},{40,32},{... | collective-permute-start | bytes 3145736 | tf_op jit(solution)/shard_map/ppermute | solution.py:26
  78.8 16.7 %collective-permute-start.9 = (bf16[32,32,512]{2,1,0:T(8,128)(2,1)S(1)}, bf16[32,32,512]{2,1,0:T(8,128)(2,1)S(1)}, u32[]{:S(2)}, u32[]{:S(2)}) collective-permute-start(bf16[32,32,512]{2,1,0:T(8,128)(2,1)S(1)} %shard_map.54.d0), channel_id=1, source_target_pairs={{64,0},{961,1},{128,64},{1,65},{192,128},{65,129},{256,192},{129,1... | collective-permute-start | bytes 3145736 | tf_op jit(solution)/shard_map/ppermute | solution.py:26
  97.5 4.6 %collective-permute-start.10 = (bf16[2,256,1024]{2,1,0:T(8,128)(2,1)S(1)}, bf16[2,256,1024]{2,1,0:T(8,128)(2,1)S(1)}, u32[]{:S(2)}, u32[]{:S(2)}) collective-permute-start(bf16[2,256,1024]{2,1,0:T(8,128)(2,1)S(1)} %get-tuple-element.22), channel_id=1, source_target_pairs={{0,1},{1,0},{2,3},{3,2},{4,5},{5,4},{6,7},{7,6},{8,9},{9,8},{10,11... | collective-permute-start | bytes 3145736 | tf_op jit(solution)/shard_map/ppermute | solution.py:215
  102.8 9.5 %collective-permute-start.12 = (bf16[2,64,1024]{2,1,0:T(8,128)(2,1)S(1)}, bf16[2,64,1024]{2,1,0:T(8,128)(2,1)S(1)}, u32[]{:S(2)}, u32[]{:S(2)}) collective-permute-start(bf16[2,64,1024]{2,1,0:T(8,128)(2,1)S(1)} %get-tuple-element.26), channel_id=1, source_target_pairs={{0,2},{1,7},{2,4},{3,1},{4,6},{5,3},{6,0},{7,5},{8,10},{9,15},{10,... | collective-permute-start | bytes 786440 | tf_op jit(solution)/shard_map/ppermute | solution.py:34
  105.9 9.8 %collective-permute-start.11 = (bf16[2,64,1024]{2,1,0:T(8,128)(2,1)S(1)}, bf16[2,64,1024]{2,1,0:T(8,128)(2,1)S(1)}, u32[]{:S(2)}, u32[]{:S(2)}) collective-permute-start(bf16[2,64,1024]{2,1,0:T(8,128)(2,1)S(1)} %get-tuple-element.24), channel_id=1, source_target_pairs={{0,6},{1,3},{2,0},{3,5},{4,2},{5,7},{6,4},{7,1},{8,14},{9,11},{10,... | collective-permute-start | bytes 786440 | tf_op jit(solution)/shard_map/ppermute | solution.py:34
  112.4 9.5 %collective-permute-start.13 = (bf16[2,64,1024]{2,1,0:T(8,128)(2,1)S(1)}, bf16[2,64,1024]{2,1,0:T(8,128)(2,1)S(1)}, u32[]{:S(2)}, u32[]{:S(2)}) collective-permute-start(bf16[2,64,1024]{2,1,0:T(8,128)(2,1)S(1)} %shard_map.58), channel_id=1, source_target_pairs={{0,2},{1,7},{2,4},{3,1},{4,6},{5,3},{6,0},{7,5},{8,10},{9,15},{10,... | collective-permute-start | bytes 786440 | tf_op jit(solution)/shard_map/ppermute | solution.py:34
where the time goes:
time: 124 us; the launch traced here: 123 us
  starting transfers between devices  68.4 us (55%)
  waiting for transfers between devices  40.5 us (33%)
  Pallas kernels  8.86 us (7%)
  other arithmetic  2.63 us (2%)
  local copies, waits for them, and re-layouts  2.58 us (2%)
    ppermute x10, starting transfers between devices, from_side(): return lax.ppermute(array, names, pairs)  57.1 us
    ppermute x10, waiting for transfers between devices, from_side(): return lax.ppermute(array, names, pairs)  29.3 us
    ppermute x3, starting transfers between devices, along_x(): return lax.ppermute(array, ('x', 'core'), pairs)  9.39 us
    ppermute x3, waiting for transfers between devices, along_x(): return lax.ppermute(array, ('x', 'core'), pairs)  8.55 us
    pallas_call x1, Pallas kernels, shards(): kernel_call(early_kernel, (out, out, bf16(512, 512)), 4, scratch=((2048,...  4.28 us
    ppermute x1, waiting for transfers between devices, over_tp(): beside = lax.ppermute(theirs, 'core', [(0, 1), (1, 0)])  2.63 us
  transfers between devices with their start and end apart: 14, of which 12 were waited for; matrix products, arithmetic and copies ran while one was open for 3% of the time, Pallas kernels for 4%

commit v1 on v0

v1 whole, which is shorter than its diff:
```python
import jax
import jax.numpy as jnp
from jax import lax
from jax.experimental import pallas as pl
from jax.experimental.pallas import tpu as pltpu
from jax.sharding import Mesh
from jax.sharding import PartitionSpec as P


EPS = 1e-06
REP, Z, Y, X, CORE = 2, 8, 8, 4, 2
VMEM = pl.BlockSpec(memory_space=pltpu.VMEM)
SMEM = pl.BlockSpec(memory_space=pltpu.SMEM)


UP_STEPS = ((0, 4), (4, 0), (0, 2), (2, 0))
DOWN_STEPS = ((0, 4), (4, 0), (2, 0), (0, 2))
CLASSES = ((0, 1), (1, 0), (1, 1))


def from_side(array, dz, dy):
    deep = REP * Z
    pairs = []
    for z in range(deep):
        for y in range(Y):
            for core, sign in ((0, 1), (1, -1)):
                source = ((z + sign * dz) % deep * Y + (y + sign * dy) % Y) * 2 + core
                pairs.append((source, (z * Y + y) * 2 + core))
    return lax.ppermute(array, ("rep", "z", "y", "core"), pairs)


def along_x(array, ahead):
    pairs = [(x, (x + ahead) % X) for x in range(X)]
    return lax.ppermute(array, "x", pairs)


def offsets(steps):
    laid = [(0, 0)]
    for dz, dy in steps:
        laid = laid + [(z + dz, y + dy) for z, y in laid]
    return laid


def shifted(steps, dz, dy):
    return [(z + dz, y + dy) for z, y in offsets(steps)]


def kernel_call(kernel, outs, n_vmem, scratch=(), smem=True, mib=8, flops=0, **rest):
    single = not isinstance(outs, tuple)
    return pl.pallas_call(
        kernel,
        out_shape=outs,
        in_specs=([SMEM] if smem else []) + [VMEM] * n_vmem,
        out_specs=VMEM if single else (VMEM,) * len(outs),
        scratch_shapes=[pltpu.VMEM(s, jnp.bfloat16) for s in scratch],
        compiler_params=pltpu.CompilerParams(vmem_limit_bytes=mib * 2**20),
        cost_estimate=pl.CostEstimate(
            flops=flops, bytes_accessed=2**20, transcendentals=0
        )
        if flops
        else None,
        **rest,
    )


def bf16(*shape):
    return jax.ShapeDtypeStruct(shape, jnp.bfloat16)


def pair_kernel(up, down, out, sem):
    first = pltpu.make_async_copy(up, out.at[0, 0], sem.at[0])
    second = pltpu.make_async_copy(down, out.at[1, 0], sem.at[1])
    first.start()
    second.start()
    first.wait()
    second.wait()


def pair(up, down):
    return pl.pallas_call(
        pair_kernel,
        out_shape=bf16(2, 1, 32, 512),
        in_specs=[pl.BlockSpec(memory_space=pl.ANY)] * 2,
        out_specs=VMEM,
        scratch_shapes=[pltpu.SemaphoreType.DMA((2,))],
        compiler_params=pltpu.CompilerParams(vmem_limit_bytes=63 * 2**20),
    )(up, down)


def join_kernel(a, b, out):
    n = a.shape[0]
    out[:n] = a[...]
    out[n:] = b[...]


def join(a, b):
    n = a.shape[0]
    return kernel_call(join_kernel, bf16(2 * n, 32, 512), 2, smem=False)(a, b)


def join_first_kernel(up, down, b, out):
    for k, own in enumerate((up, down)):
        out[k, 0] = own[...]
        out[k, 1] = b[k, 0]


def join_first(up, down, b):
    return kernel_call(join_first_kernel, bf16(2, 2, 32, 512), 3, smem=False)(
        up, down, b
    )


def join_apart_kernel(a, b, up, down):
    n = a.shape[1]
    for k, out in enumerate((up, down)):
        out[:n] = a[k]
        out[n:] = b[k]


def join_apart(a, b):
    out = bf16(2 * a.shape[1], 32, 512)
    return kernel_call(join_apart_kernel, (out, out), 2, smem=False)(a, b)


def place(where, piece, laid, whole, halved):
    z, y, sign = where[0], where[1], 1 - 2 * where[2]
    for j, (dz, dy) in enumerate(laid):
        at_z = (z + sign * dz) & (Z - 1)
        at_y = (y + sign * dy) & (Y - 1)
        at = ((at_z >> 1) if halved else at_z) * Y + at_y
        whole[pl.ds(pl.multiple_of(at * 32, 32), 32), :] = piece[j]


def down_product(hidden, down, theirs, own, part):
    @pl.loop(0, 4)
    def _(n):
        columns = pl.ds(pl.multiple_of(n * 256, 256), 256)
        made = lax.dot_general(
            hidden[...],
            down[columns, :],
            (((1,), (1,)), ((), ())),
            preferred_element_type=jnp.float32,
        ).astype(jnp.bfloat16)
        theirs[part, :, columns] = made[:256]
        own[part, :, columns] = made[256:]


def up_kernel(where, normed, u0, u1, u2, u3, hidden, up):
    for piece, shift in zip((u0, u1, u2, u3), ((0, 0), *CLASSES), strict=True):
        place(where, piece, shifted(UP_STEPS, *shift), up, False)
    core = where[2]

    @pl.loop(0, 2)
    def _(n):
        columns = pl.ds(pl.multiple_of(n * 256, 256), 256)
        lifted = jnp.dot(
            normed[...], up[:, columns], preferred_element_type=jnp.float32
        )
        active = jnp.square(jnp.maximum(lifted, 0.0)).astype(jnp.bfloat16)
        for j in range(X * CORE):
            x, c = divmod(j, CORE)
            side = jnp.where(core == c, 256, 0)
            rows = pl.ds(pl.multiple_of(side + x * 64, 64), 64)
            hidden[rows, columns] = active[j * 64 : (j + 1) * 64]


def early_kernel(where, hidden, d0, d1, theirs, own, down):
    place(where, d0, offsets(DOWN_STEPS), down, True)
    place(where, d1, shifted(DOWN_STEPS, *CLASSES[0]), down, True)
    down_product(hidden, down, theirs, own, 0)


def late_kernel(where, hidden, d2, d3, theirs_in, own_in, theirs, own, down):
    place(where, d2, shifted(DOWN_STEPS, *CLASSES[1]), down, True)
    place(where, d3, shifted(DOWN_STEPS, *CLASSES[2]), down, True)
    down_product(hidden, down, theirs, own, 1)


def add_kernel(where, own, beside, keep, ahead, back, far):
    x = where[3]
    for out, step in ((far, 2), (ahead, 1), (back, 3), (keep, 0)):
        rows = pl.ds(pl.multiple_of(((x + step) & (X - 1)) * 64, 64), 64)
        for part in range(2):
            total = own[part, rows].astype(jnp.float32)
            total = total + beside[part, rows].astype(jnp.float32)
            out[part] = total.astype(jnp.bfloat16)


def last_kernel(where, residual, a, b, c, d, out):
    odd = where[0] & 1
    for part in range(2):
        for k in range(4):
            at = (2 * k + (odd ^ part)) * 256
            columns = pl.ds(pl.multiple_of(at, 256), 256)
            here = slice(k * 256, (k + 1) * 256)
            total = residual[:, columns].astype(jnp.float32)
            for term in (a, b, c, d):
                total = total + term[part, :, here].astype(jnp.float32)
            out[:, columns] = total.astype(jnp.bfloat16)


def gathered(up_weight, down_weight):
    held_in = from_side(pair(up_weight, down_weight.T), *UP_STEPS[0])
    held = join_first(up_weight, down_weight.T, held_in)
    up, down = join_apart(held, from_side(held, *UP_STEPS[1]))
    for k in range(2, 4):
        up_in = from_side(up, *UP_STEPS[k])
        down_in = from_side(down, *DOWN_STEPS[k])
        up, down = join(up, up_in), join(down, down_in)
    ups, downs = [up], [down]
    for shift in CLASSES:
        ups.append(from_side(up, *shift))
    for shift in CLASSES:
        downs.append(from_side(down, *shift))
    return ups, downs


def over_tp(where, theirs, own, residual):
    beside = lax.ppermute(theirs, "core", [(0, 1), (1, 0)])
    piece = bf16(2, 64, 1024)
    keep, ahead, back, far = kernel_call(add_kernel, (piece,) * 4, 2)(
        where, own, beside
    )
    far, ahead, back = along_x(far, 2), along_x(ahead, 1), along_x(back, 3)
    return kernel_call(last_kernel, bf16(64, 2048), 5)(
        where, residual, keep, ahead, back, far
    )


def shards(tokens, norm_gain, up_weight, down_weight):
    core, x = lax.axis_index("core"), lax.axis_index("x")
    ups, downs = gathered(up_weight, down_weight)
    xf = tokens.astype(jnp.float32)
    scale = lax.rsqrt(jnp.mean(xf * xf, axis=-1, keepdims=True) + EPS)
    normed = (xf * scale * norm_gain).astype(jnp.bfloat16)
    where = jnp.stack([lax.axis_index("z"), lax.axis_index("y"), core, x]).astype(
        jnp.int32
    )
    residual = lax.dynamic_slice_in_dim(tokens, (x * CORE + core) * 64, 64, 0)
    hidden = kernel_call(
        up_kernel, bf16(512, 512), 5, scratch=((2048, 512),), mib=12, flops=2**30
    )(where, normed, *ups)
    out = bf16(2, 256, 1024)
    half = ((1024, 512),)
    theirs, own = kernel_call(
        early_kernel, (out, out), 3, scratch=half, flops=2**29
    )(where, hidden, *downs[:2])
    theirs, own = kernel_call(
        late_kernel,
        (out, out),
        5,
        scratch=half,
        flops=2**29,
        input_output_aliases={4: 0, 5: 1},
    )(where, hidden, *downs[2:], theirs, own)
    return over_tp(where, theirs, own, residual)


def solution(mesh):
    torus = Mesh(
        mesh.devices.reshape(REP, Z, Y, X, CORE), ("rep", "z", "y", "x", "core")
    )
    rep_fs = ("rep", "z", "y")
    tp = ("x", "core")
    in_specs = (P(rep_fs, None), P(), P(("z", "y"), tp), P(tp, ("z", "y")))
    return jax.shard_map(
        shards,
        mesh=torus,
        in_specs=in_specs,
        out_specs=P(rep_fs + tp, None),
        check_vma=False,
    )
```

time: 124 us -> 133 us (1.073)
  the two profiles are of different devices: /device:TPU:56 before, /device:TPU:1 now
where the time goes in v1:
time: 133 us; the launch traced here: 131 us
  starting transfers between devices  68.4 us (51%)
  waiting for transfers between devices  49.1 us (37%)
  Pallas kernels  9.87 us (7%)
  local copies, waits for them, and re-layouts  2.5 us (2%)
    ppermute x12, starting transfers between devices, from_side(): return lax.ppermute(array, ('rep', 'z', 'y', 'core'), pairs)  51.9 us
    ppermute x12, waiting for transfers between devices, from_side(): return lax.ppermute(array, ('rep', 'z', 'y', 'core'), pairs)  40.6 us
    ppermute x3, starting transfers between devices, along_x(): return lax.ppermute(array, 'x', pairs)  9.55 us
    ppermute x1, starting transfers between devices, over_tp(): beside = lax.ppermute(theirs, 'core', [(0, 1), (1, 0)])  6.95 us
    ppermute x3, waiting for transfers between devices, along_x(): return lax.ppermute(array, 'x', pairs)  6.27 us
  transfers between devices with their start and end apart: 16, of which 10 were waited for; matrix products, arithmetic and copies ran while one was open for 2% of the time, Pallas kernels for 3%

profile of v1, /device:TPU:1, one launch (start us, length us, event | category | flops | bytes accessed | tf_op | source)
XLA Modules:
  0.0 131.3 jit_solution(4580032816581593437)
XLA Ops:
  0.0 1.4 %shard_map.46 = bf16[2,1,32,512]{3,2,1,0:T(8,128)(2,1)} custom-call(bf16[32,512]{1,0:T(8,128)(2,1)} %up.3, bf16[32,512]{1,0:T(8,128)(2,1)} %bitcast.5), custom_call_target="tpu_custom_call" | custom-call | tf_op jit(solution)/shard_map/pallas_call | solution.py:80
  1.4 8.3 %collective-permute-start = (bf16[2,1,32,512]{3,2,1,0:T(8,128)(2,1)}, bf16[2,1,32,512]{3,2,1,0:T(8,128)(2,1)S(1)}, u32[]{:S(2)}, u32[]{:S(2)}) collective-permute-start(bf16[2,1,32,512]{3,2,1,0:T(8,128)(2,1)} %shard_map.46), channel_id=1, source_target_pairs={{32,0},{33,1},{40,8},{41,9},{48,16},{49,17},{56,24},{57,25},{0,32}... | collective-permute-start | bytes 196616 | tf_op jit(solution)/shard_map/ppermute | solution.py:29
  9.7 1.9 %collective-permute-done.b = bf16[2,1,32,512]{3,2,1,0:T(8,128)(2,1)S(1)} collective-permute-done((bf16[2,1,32,512]{3,2,1,0:T(8,128)(2,1)}, bf16[2,1,32,512]{3,2,1,0:T(8,128)(2,1)S(1)}, u32[]{:S(2)}, u32[]{:S(2)}) %collective-permute-start) | collective-permute-done | bytes 65568 | tf_op jit(solution)/shard_map/ppermute | solution.py:29
  13.2 10.8 %collective-permute-start.1 = (bf16[2,2,32,512]{3,2,1,0:T(8,128)(2,1)S(1)}, bf16[2,2,32,512]{3,2,1,0:T(8,128)(2,1)S(1)}, u32[]{:S(2)}, u32[]{:S(2)}) collective-permute-start(bf16[2,2,32,512]{3,2,1,0:T(8,128)(2,1)S(1)} %shard_map.47.a), channel_id=1, source_target_pairs={{256,0},{769,1},{264,8},{777,9},{272,16},{785,17},{280,24},{793,25... | collective-permute-start | bytes 393224 | tf_op jit(solution)/shard_map/ppermute | solution.py:29
  23.9 9.9 %collective-permute-done.1.b = bf16[2,2,32,512]{3,2,1,0:T(8,128)(2,1)S(1)} collective-permute-done((bf16[2,2,32,512]{3,2,1,0:T(8,128)(2,1)S(1)}, bf16[2,2,32,512]{3,2,1,0:T(8,128)(2,1)S(1)}, u32[]{:S(2)}, u32[]{:S(2)}) %collective-permute-start.1) | collective-permute-done | bytes 131104 | tf_op jit(solution)/shard_map/ppermute | solution.py:29
  33.9 6.1 %collective-permute-start.2 = (bf16[4,32,512]{2,1,0:T(8,128)(2,1)S(1)}, bf16[4,32,512]{2,1,0:T(8,128)(2,1)S(1)}, u32[]{:S(2)}, u32[]{:S(2)}) collective-permute-start(bf16[4,32,512]{2,1,0:T(8,128)(2,1)S(1)} %get-tuple-element.15.a), channel_id=1, source_target_pairs={{16,0},{49,1},{24,8},{57,9},{32,16},{1,17},{40,24},{9,25},{48,32},... | collective-permute-start | bytes 393224 | tf_op jit(solution)/shard_map/ppermute | solution.py:29
  39.9 3.3 %collective-permute-done.2.b = bf16[4,32,512]{2,1,0:T(8,128)(2,1)S(1)} collective-permute-done((bf16[4,32,512]{2,1,0:T(8,128)(2,1)S(1)}, bf16[4,32,512]{2,1,0:T(8,128)(2,1)S(1)}, u32[]{:S(2)}, u32[]{:S(2)}) %collective-permute-start.2) | collective-permute-done | bytes 131104 | tf_op jit(solution)/shard_map/ppermute | solution.py:29
  43.3 6.6 %collective-permute-start.3 = (bf16[8,32,512]{2,1,0:T(8,128)(2,1)S(1)}, bf16[8,32,512]{2,1,0:T(8,128)(2,1)S(1)}, u32[]{:S(2)}, u32[]{:S(2)}) collective-permute-start(bf16[8,32,512]{2,1,0:T(8,128)(2,1)S(1)} %shard_map.49.a), channel_id=1, source_target_pairs={{128,0},{897,1},{136,8},{905,9},{144,16},{913,17},{152,24},{921,25... | collective-permute-start | bytes 786440 | tf_op jit(solution)/shard_map/ppermute | solution.py:29
  49.9 1.9 %collective-permute-start.7 = (bf16[4,32,512]{2,1,0:T(8,128)(2,1)S(1)}, bf16[4,32,512]{2,1,0:T(8,128)(2,1)S(1)}, u32[]{:S(2)}, u32[]{:S(2)}) collective-permute-start(bf16[4,32,512]{2,1,0:T(8,128)(2,1)S(1)} %get-tuple-element.16.a), channel_id=1, source_target_pairs={{128,0},{897,1},{136,8},{905,9},{144,16},{913,17},{152,24},{921,25... | collective-permute-start | bytes 393224 | tf_op jit(solution)/shard_map/ppermute | solution.py:29
  51.8 9.3 %collective-permute-done.3.b = bf16[8,32,512]{2,1,0:T(8,128)(2,1)S(1)} collective-permute-done((bf16[8,32,512]{2,1,0:T(8,128)(2,1)S(1)}, bf16[8,32,512]{2,1,0:T(8,128)(2,1)S(1)}, u32[]{:S(2)}, u32[]{:S(2)}) %collective-permute-start.3) | collective-permute-done | bytes 262176 | tf_op jit(solution)/shard_map/ppermute | solution.py:29
  61.1 3.5 %collective-permute-start.4 = (bf16[16,32,512]{2,1,0:T(8,128)(2,1)S(1)}, bf16[16,32,512]{2,1,0:T(8,128)(2,1)S(1)}, u32[]{:S(2)}, u32[]{:S(2)}) collective-permute-start(bf16[16,32,512]{2,1,0:T(8,128)(2,1)S(1)} %shard_map.50.u0), channel_id=1, source_target_pairs={{8,0},{57,1},{16,8},{1,9},{24,16},{9,17},{32,24},{17,25},{40,32},{... | collective-permute-start | bytes 1572872 | tf_op jit(solution)/shard_map/ppermute | solution.py:29
  65.2 3.7 %collective-permute-start.8 = (bf16[8,32,512]{2,1,0:T(8,128)(2,1)S(1)}, bf16[8,32,512]{2,1,0:T(8,128)(2,1)S(1)}, u32[]{:S(2)}, u32[]{:S(2)}) collective-permute-start(bf16[8,32,512]{2,1,0:T(8,128)(2,1)S(1)} %shard_map.52.a), channel_id=1, source_target_pairs={{16,0},{49,1},{24,8},{57,9},{32,16},{1,17},{40,24},{9,25},{48,32},... | collective-permute-start | bytes 786440 | tf_op jit(solution)/shard_map/ppermute | solution.py:29
  68.9 1.9 %collective-permute-start.5 = (bf16[16,32,512]{2,1,0:T(8,128)(2,1)S(1)}, bf16[16,32,512]{2,1,0:T(8,128)(2,1)S(1)}, u32[]{:S(2)}, u32[]{:S(2)}) collective-permute-start(bf16[16,32,512]{2,1,0:T(8,128)(2,1)S(1)} %shard_map.50.u0), channel_id=1, source_target_pairs={{64,0},{961,1},{72,8},{969,9},{80,16},{977,17},{88,24},{985,25},{9... | collective-permute-start | bytes 1572872 | tf_op jit(solution)/shard_map/ppermute | solution.py:29
  70.9 1.9 %collective-permute-start.6 = (bf16[16,32,512]{2,1,0:T(8,128)(2,1)S(1)}, bf16[16,32,512]{2,1,0:T(8,128)(2,1)S(1)}, u32[]{:S(2)}, u32[]{:S(2)}) collective-permute-start(bf16[16,32,512]{2,1,0:T(8,128)(2,1)S(1)} %shard_map.50.u0), channel_id=1, source_target_pairs={{72,0},{1017,1},{80,8},{961,9},{88,16},{969,17},{96,24},{977,25},{... | collective-permute-start | bytes 1572872 | tf_op jit(solution)/shard_map/ppermute | solution.py:29
  72.8 5.1 %collective-permute-done.8.b = bf16[8,32,512]{2,1,0:T(8,128)(2,1)S(1)} collective-permute-done((bf16[8,32,512]{2,1,0:T(8,128)(2,1)S(1)}, bf16[8,32,512]{2,1,0:T(8,128)(2,1)S(1)}, u32[]{:S(2)}, u32[]{:S(2)}) %collective-permute-start.8) | collective-permute-done | bytes 262176 | tf_op jit(solution)/shard_map/ppermute | solution.py:29
  77.9 3.4 %collective-permute-start.11 = (bf16[16,32,512]{2,1,0:T(8,128)(2,1)S(1)}, bf16[16,32,512]{2,1,0:T(8,128)(2,1)S(1)}, u32[]{:S(2)}, u32[]{:S(2)}) collective-permute-start(bf16[16,32,512]{2,1,0:T(8,128)(2,1)S(1)} %shard_map.53.d0), channel_id=1, source_target_pairs={{8,0},{57,1},{16,8},{1,9},{24,16},{9,17},{32,24},{17,25},{40,32},{... | collective-permute-start | bytes 1572872 | tf_op jit(solution)/shard_map/ppermute | solution.py:29
  81.3 1.9 %collective-permute-start.10 = (bf16[16,32,512]{2,1,0:T(8,128)(2,1)S(1)}, bf16[16,32,512]{2,1,0:T(8,128)(2,1)S(1)}, u32[]{:S(2)}, u32[]{:S(2)}) collective-permute-start(bf16[16,32,512]{2,1,0:T(8,128)(2,1)S(1)} %shard_map.53.d0), channel_id=1, source_target_pairs={{72,0},{1017,1},{80,8},{961,9},{88,16},{969,17},{96,24},{977,25},{... | collective-permute-start | bytes 1572872 | tf_op jit(solution)/shard_map/ppermute | solution.py:29
  83.3 1.9 %collective-permute-start.9 = (bf16[16,32,512]{2,1,0:T(8,128)(2,1)S(1)}, bf16[16,32,512]{2,1,0:T(8,128)(2,1)S(1)}, u32[]{:S(2)}, u32[]{:S(2)}) collective-permute-start(bf16[16,32,512]{2,1,0:T(8,128)(2,1)S(1)} %shard_map.53.d0), channel_id=1, source_target_pairs={{64,0},{961,1},{72,8},{969,9},{80,16},{977,17},{88,24},{985,25},{9... | collective-permute-start | bytes 1572872 | tf_op jit(solution)/shard_map/ppermute | solution.py:29
  85.8 2.1 %collective-permute-done.6.u3 = bf16[16,32,512]{2,1,0:T(8,128)(2,1)S(1)} collective-permute-done((bf16[16,32,512]{2,1,0:T(8,128)(2,1)S(1)}, bf16[16,32,512]{2,1,0:T(8,128)(2,1)S(1)}, u32[]{:S(2)}, u32[]{:S(2)}) %collective-permute-start.6) | collective-permute-done | bytes 524320 | tf_op jit(solution)/shard_map/ppermute | solution.py:29
  87.9 2.2 %shard_map.51.hidden = bf16[512,512]{1,0:T(8,128)(2,1)S(1)} custom-call(s32[4]{0:T(128)S(1)} %pad_add_fusion.where, bf16[512,2048]{1,0:T(8,128)(2,1)S(1)} %fusion.2.normed, bf16[16,32,512]{2,1,0:T(8,128)(2,1)S(1)} %shard_map.50.u0, bf16[16,32,512]{2,1,0:T(8,128)(2,1)S(1)} %collective-permute-done.4.u1, bf16[16,32,512]{2,1,0:T(8,128)(2,1)S(1)} %collective-permute-done.5.u2, ...), custom_call_target="tpu_custom_call" | custom-call | flops 1073741824 | bytes 1048576 | tf_op jit(solution)/shard_map/pallas_call | solution.py:240
  90.1 9.0 %collective-permute-done.11.d1 = bf16[16,32,512]{2,1,0:T(8,128)(2,1)S(1)} collective-permute-done((bf16[16,32,512]{2,1,0:T(8,128)(2,1)S(1)}, bf16[16,32,512]{2,1,0:T(8,128)(2,1)S(1)}, u32[]{:S(2)}, u32[]{:S(2)}) %collective-permute-start.11) | collective-permute-done | bytes 524320 | tf_op jit(solution)/shard_map/ppermute | solution.py:29
  99.0 2.0 %shard_map.54 = (bf16[2,256,1024]{2,1,0:T(8,128)(2,1)S(1)}, bf16[2,256,1024]{2,1,0:T(8,128)(2,1)S(1)}) custom-call(s32[4]{0:T(128)S(1)} %pad_add_fusion.where, bf16[512,512]{1,0:T(8,128)(2,1)S(1)} %shard_map.51.hidden, bf16[16,32,512]{2,1,0:T(8,128)(2,1)S(1)} %shard_map.53.d0, bf16[16,32,512]{2,1,0:T(8,128)(2,1)S(1)} %collective-permute-done.11.d1), custom_call_target="tpu_custom_call" | custom-call | flops 536870912 | bytes 1048576 | tf_op jit(solution)/shard_map/pallas_call | solution.py:245
  101.1 2.0 %shard_map.55 = (bf16[2,256,1024]{2,1,0:T(8,128)(2,1)S(1)}, bf16[2,256,1024]{2,1,0:T(8,128)(2,1)S(1)}) custom-call(s32[4]{0:T(128)S(1)} %pad_add_fusion.where, bf16[512,512]{1,0:T(8,128)(2,1)S(1)} %shard_map.51.hidden, bf16[16,32,512]{2,1,0:T(8,128)(2,1)S(1)} %collective-permute-done.9.d2, ...), custom_call_target="tpu_custom_call", output_to_operand_aliasing={{0}: (4, {}), {1}: (5, {})} | custom-call | flops 536870912 | bytes 1048576 | tf_op jit(solution)/shard_map/pallas_call | solution.py:248
  103.0 7.0 %collective-permute-start.12 = (bf16[2,256,1024]{2,1,0:T(8,128)(2,1)S(1)}, bf16[2,256,1024]{2,1,0:T(8,128)(2,1)S(1)}, u32[]{:S(2)}, u32[]{:S(2)}) collective-permute-start(bf16[2,256,1024]{2,1,0:T(8,128)(2,1)S(1)} %get-tuple-element.20), channel_id=1, source_target_pairs={{0,1},{1,0},{2,3},{3,2},{4,5},{5,4},{6,7},{7,6},{8,9},{9,8},{10,11... | collective-permute-start | bytes 3145736 | tf_op jit(solution)/shard_map/ppermute | solution.py:219
  110.0 2.3 %collective-permute-done.12.beside = bf16[2,256,1024]{2,1,0:T(8,128)(2,1)S(1)} collective-permute-done((bf16[2,256,1024]{2,1,0:T(8,128)(2,1)S(1)}, bf16[2,256,1024]{2,1,0:T(8,128)(2,1)S(1)}, u32[]{:S(2)}, u32[]{:S(2)}) %collective-permute-start.12) | collective-permute-done | bytes 1048608 | tf_op jit(solution)/shard_map/ppermute | solution.py:219
  113.1 2.7 %collective-permute-start.13 = (bf16[2,64,1024]{2,1,0:T(8,128)(2,1)S(1)}, bf16[2,64,1024]{2,1,0:T(8,128)(2,1)S(1)}, u32[]{:S(2)}, u32[]{:S(2)}) collective-permute-start(bf16[2,64,1024]{2,1,0:T(8,128)(2,1)S(1)} %get-tuple-element.22), channel_id=1, source_target_pairs={{0,2},{2,4},{4,6},{6,0},{1,3},{3,5},{5,7},{7,1},{8,10},{10,12},{12... | collective-permute-start | bytes 786440 | tf_op jit(solution)/shard_map/ppermute | solution.py:34
  115.8 3.7 %collective-permute-start.14 = (bf16[2,64,1024]{2,1,0:T(8,128)(2,1)S(1)}, bf16[2,64,1024]{2,1,0:T(8,128)(2,1)S(1)}, u32[]{:S(2)}, u32[]{:S(2)}) collective-permute-start(bf16[2,64,1024]{2,1,0:T(8,128)(2,1)S(1)} %get-tuple-element.23), channel_id=1, source_target_pairs={{0,6},{2,0},{4,2},{6,4},{1,7},{3,1},{5,3},{7,5},{8,14},{10,8},{12,... | collective-permute-start | bytes 786440 | tf_op jit(solution)/shard_map/ppermute | solution.py:34
  119.6 3.1 %collective-permute-start.15 = (bf16[2,64,1024]{2,1,0:T(8,128)(2,1)S(1)}, bf16[2,64,1024]{2,1,0:T(8,128)(2,1)S(1)}, u32[]{:S(2)}, u32[]{:S(2)}) collective-permute-start(bf16[2,64,1024]{2,1,0:T(8,128)(2,1)S(1)} %get-tuple-element.24), channel_id=1, source_target_pairs={{0,4},{2,6},{4,0},{6,2},{1,5},{3,7},{5,1},{7,3},{8,12},{10,14},{12... | collective-permute-start | bytes 786440 | tf_op jit(solution)/shard_map/ppermute | solution.py:34
  122.6 1.0 constant_dynamic-slice_fusion.residual
  123.7 1.3 collective-permute-done.14.c
  124.9 5.0 %collective-permute-done.15.d = bf16[2,64,1024]{2,1,0:T(8,128)(2,1)S(1)} collective-permute-done((bf16[2,64,1024]{2,1,0:T(8,128)(2,1)S(1)}, bf16[2,64,1024]{2,1,0:T(8,128)(2,1)S(1)}, u32[]{:S(2)}, u32[]{:S(2)}) %collective-permute-start.15) | collective-permute-done | bytes 262176 | tf_op jit(solution)/shard_map/ppermute | solution.py:34
  129.9 1.4 %shard_map.57 = bf16[64,2048]{1,0:T(8,128)(2,1)} custom-call(s32[4]{0:T(128)S(1)} %pad_add_fusion.where, bf16[64,2048]{1,0:T(8,128)(2,1)S(1)} %constant_dynamic-slice_fusion.residual, bf16[2,64,1024]{2,1,0:T(8,128)(2,1)S(1)} %get-tuple-element.21.a, bf16[2,64,1024]{2,1,0:T(8,128)(2,1)S(1)} %collective-permute-done.13.b, ...), custom_call_target="tpu_custom_call" | custom-call | tf_op jit(solution)/shard_map/pallas_call | solution.py:225
  (25 shorter events, 3.6 us)
Async XLA Ops:
  1.4 10.2 %collective-permute-start = (bf16[2,1,32,512]{3,2,1,0:T(8,128)(2,1)}, bf16[2,1,32,512]{3,2,1,0:T(8,128)(2,1)S(1)}, u32[]{:S(2)}, u32[]{:S(2)}) collective-permute-start(bf16[2,1,32,512]{3,2,1,0:T(8,128)(2,1)} %shard_map.46), channel_id=1, source_target_pairs={{32,0},{33,1},{40,8},{41,9},{48,16},{49,17},{56,24},{57,25},{0,32}... | collective-permute-start | bytes 196616 | tf_op jit(solution)/shard_map/ppermute | solution.py:29
  11.6 0.8 copy-start
  12.4 0.8 copy-start.1
  13.1 51.5 %copy-start.2 = (bf16[512,2048]{1,0:T(8,128)(2,1)S(1)}, bf16[512,2048]{1,0:T(8,128)(2,1)}, u32[]{:S(2)}) copy-start(bf16[512,2048]{1,0:T(8,128)(2,1)} %param.4) | copy-start | bytes 6291460
  13.2 20.7 %collective-permute-start.1 = (bf16[2,2,32,512]{3,2,1,0:T(8,128)(2,1)S(1)}, bf16[2,2,32,512]{3,2,1,0:T(8,128)(2,1)S(1)}, u32[]{:S(2)}, u32[]{:S(2)}) collective-permute-start(bf16[2,2,32,512]{3,2,1,0:T(8,128)(2,1)S(1)} %shard_map.47.a), channel_id=1, source_target_pairs={{256,0},{769,1},{264,8},{777,9},{272,16},{785,17},{280,24},{793,25... | collective-permute-start | bytes 393224 | tf_op jit(solution)/shard_map/ppermute | solution.py:29
  33.9 9.4 %collective-permute-start.2 = (bf16[4,32,512]{2,1,0:T(8,128)(2,1)S(1)}, bf16[4,32,512]{2,1,0:T(8,128)(2,1)S(1)}, u32[]{:S(2)}, u32[]{:S(2)}) collective-permute-start(bf16[4,32,512]{2,1,0:T(8,128)(2,1)S(1)} %get-tuple-element.15.a), channel_id=1, source_target_pairs={{16,0},{49,1},{24,8},{57,9},{32,16},{1,17},{40,24},{9,25},{48,32},... | collective-permute-start | bytes 393224 | tf_op jit(solution)/shard_map/ppermute | solution.py:29
  43.3 17.8 %collective-permute-start.3 = (bf16[8,32,512]{2,1,0:T(8,128)(2,1)S(1)}, bf16[8,32,512]{2,1,0:T(8,128)(2,1)S(1)}, u32[]{:S(2)}, u32[]{:S(2)}) collective-permute-start(bf16[8,32,512]{2,1,0:T(8,128)(2,1)S(1)} %shard_map.49.a), channel_id=1, source_target_pairs={{128,0},{897,1},{136,8},{905,9},{144,16},{913,17},{152,24},{921,25... | collective-permute-start | bytes 786440 | tf_op jit(solution)/shard_map/ppermute | solution.py:29
  49.9 15.2 %collective-permute-start.7 = (bf16[4,32,512]{2,1,0:T(8,128)(2,1)S(1)}, bf16[4,32,512]{2,1,0:T(8,128)(2,1)S(1)}, u32[]{:S(2)}, u32[]{:S(2)}) collective-permute-start(bf16[4,32,512]{2,1,0:T(8,128)(2,1)S(1)} %get-tuple-element.16.a), channel_id=1, source_target_pairs={{128,0},{897,1},{136,8},{905,9},{144,16},{913,17},{152,24},{921,25... | collective-permute-start | bytes 393224 | tf_op jit(solution)/shard_map/ppermute | solution.py:29
  61.1 24.1 %copy-start.3 = (f32[2048]{0:T(1024)S(1)}, f32[2048]{0:T(1024)}, u32[]{:S(2)}) copy-start(f32[2048]{0:T(1024)} %param.5) | copy-start | bytes 24580
  61.1 22.2 %collective-permute-start.4 = (bf16[16,32,512]{2,1,0:T(8,128)(2,1)S(1)}, bf16[16,32,512]{2,1,0:T(8,128)(2,1)S(1)}, u32[]{:S(2)}, u32[]{:S(2)}) collective-permute-start(bf16[16,32,512]{2,1,0:T(8,128)(2,1)S(1)} %shard_map.50.u0), channel_id=1, source_target_pairs={{8,0},{57,1},{16,8},{1,9},{24,16},{9,17},{32,24},{17,25},{40,32},{... | collective-permute-start | bytes 1572872 | tf_op jit(solution)/shard_map/ppermute | solution.py:29
  65.2 12.7 %collective-permute-start.8 = (bf16[8,32,512]{2,1,0:T(8,128)(2,1)S(1)}, bf16[8,32,512]{2,1,0:T(8,128)(2,1)S(1)}, u32[]{:S(2)}, u32[]{:S(2)}) collective-permute-start(bf16[8,32,512]{2,1,0:T(8,128)(2,1)S(1)} %shard_map.52.a), channel_id=1, source_target_pairs={{16,0},{49,1},{24,8},{57,9},{32,16},{1,17},{40,24},{9,25},{48,32},... | collective-permute-start | bytes 786440 | tf_op jit(solution)/shard_map/ppermute | solution.py:29
  68.9 16.8 %collective-permute-start.5 = (bf16[16,32,512]{2,1,0:T(8,128)(2,1)S(1)}, bf16[16,32,512]{2,1,0:T(8,128)(2,1)S(1)}, u32[]{:S(2)}, u32[]{:S(2)}) collective-permute-start(bf16[16,32,512]{2,1,0:T(8,128)(2,1)S(1)} %shard_map.50.u0), channel_id=1, source_target_pairs={{64,0},{961,1},{72,8},{969,9},{80,16},{977,17},{88,24},{985,25},{9... | collective-permute-start | bytes 1572872 | tf_op jit(solution)/shard_map/ppermute | solution.py:29
  70.9 17.0 %collective-permute-start.6 = (bf16[16,32,512]{2,1,0:T(8,128)(2,1)S(1)}, bf16[16,32,512]{2,1,0:T(8,128)(2,1)S(1)}, u32[]{:S(2)}, u32[]{:S(2)}) collective-permute-start(bf16[16,32,512]{2,1,0:T(8,128)(2,1)S(1)} %shard_map.50.u0), channel_id=1, source_target_pairs={{72,0},{1017,1},{80,8},{961,9},{88,16},{969,17},{96,24},{977,25},{... | collective-permute-start | bytes 1572872 | tf_op jit(solution)/shard_map/ppermute | solution.py:29
  77.9 21.1 %collective-permute-start.11 = (bf16[16,32,512]{2,1,0:T(8,128)(2,1)S(1)}, bf16[16,32,512]{2,1,0:T(8,128)(2,1)S(1)}, u32[]{:S(2)}, u32[]{:S(2)}) collective-permute-start(bf16[16,32,512]{2,1,0:T(8,128)(2,1)S(1)} %shard_map.53.d0), channel_id=1, source_target_pairs={{8,0},{57,1},{16,8},{1,9},{24,16},{9,17},{32,24},{17,25},{40,32},{... | collective-permute-start | bytes 1572872 | tf_op jit(solution)/shard_map/ppermute | solution.py:29
  81.3 19.7 %collective-permute-start.10 = (bf16[16,32,512]{2,1,0:T(8,128)(2,1)S(1)}, bf16[16,32,512]{2,1,0:T(8,128)(2,1)S(1)}, u32[]{:S(2)}, u32[]{:S(2)}) collective-permute-start(bf16[16,32,512]{2,1,0:T(8,128)(2,1)S(1)} %shard_map.53.d0), channel_id=1, source_target_pairs={{72,0},{1017,1},{80,8},{961,9},{88,16},{969,17},{96,24},{977,25},{... | collective-permute-start | bytes 1572872 | tf_op jit(solution)/shard_map/ppermute | solution.py:29
  83.3 17.8 %collective-permute-start.9 = (bf16[16,32,512]{2,1,0:T(8,128)(2,1)S(1)}, bf16[16,32,512]{2,1,0:T(8,128)(2,1)S(1)}, u32[]{:S(2)}, u32[]{:S(2)}) collective-permute-start(bf16[16,32,512]{2,1,0:T(8,128)(2,1)S(1)} %shard_map.53.d0), channel_id=1, source_target_pairs={{64,0},{961,1},{72,8},{969,9},{80,16},{977,17},{88,24},{985,25},{9... | collective-permute-start | bytes 1572872 | tf_op jit(solution)/shard_map/ppermute | solution.py:29
  103.0 9.2 %collective-permute-start.12 = (bf16[2,256,1024]{2,1,0:T(8,128)(2,1)S(1)}, bf16[2,256,1024]{2,1,0:T(8,128)(2,1)S(1)}, u32[]{:S(2)}, u32[]{:S(2)}) collective-permute-start(bf16[2,256,1024]{2,1,0:T(8,128)(2,1)S(1)} %get-tuple-element.20), channel_id=1, source_target_pairs={{0,1},{1,0},{2,3},{3,2},{4,5},{5,4},{6,7},{7,6},{8,9},{9,8},{10,11... | collective-permute-start | bytes 3145736 | tf_op jit(solution)/shard_map/ppermute | solution.py:219
  113.1 10.6 %collective-permute-start.13 = (bf16[2,64,1024]{2,1,0:T(8,128)(2,1)S(1)}, bf16[2,64,1024]{2,1,0:T(8,128)(2,1)S(1)}, u32[]{:S(2)}, u32[]{:S(2)}) collective-permute-start(bf16[2,64,1024]{2,1,0:T(8,128)(2,1)S(1)} %get-tuple-element.22), channel_id=1, source_target_pairs={{0,2},{2,4},{4,6},{6,0},{1,3},{3,5},{5,7},{7,1},{8,10},{10,12},{12... | collective-permute-start | bytes 786440 | tf_op jit(solution)/shard_map/ppermute | solution.py:34
  115.8 9.1 %collective-permute-start.14 = (bf16[2,64,1024]{2,1,0:T(8,128)(2,1)S(1)}, bf16[2,64,1024]{2,1,0:T(8,128)(2,1)S(1)}, u32[]{:S(2)}, u32[]{:S(2)}) collective-permute-start(bf16[2,64,1024]{2,1,0:T(8,128)(2,1)S(1)} %get-tuple-element.23), channel_id=1, source_target_pairs={{0,6},{2,0},{4,2},{6,4},{1,7},{3,1},{5,3},{7,5},{8,14},{10,8},{12,... | collective-permute-start | bytes 786440 | tf_op jit(solution)/shard_map/ppermute | solution.py:34
  119.6 10.3 %collective-permute-start.15 = (bf16[2,64,1024]{2,1,0:T(8,128)(2,1)S(1)}, bf16[2,64,1024]{2,1,0:T(8,128)(2,1)S(1)}, u32[]{:S(2)}, u32[]{:S(2)}) collective-permute-start(bf16[2,64,1024]{2,1,0:T(8,128)(2,1)S(1)} %get-tuple-element.24), channel_id=1, source_target_pairs={{0,4},{2,6},{4,0},{6,2},{1,5},{3,7},{5,1},{7,3},{8,12},{10,14},{12... | collective-permute-start | bytes 786440 | tf_op jit(solution)/shard_map/ppermute | solution.py:34

commit v2 on v0

v2 whole, which is shorter than its diff:
```python
import jax
import jax.numpy as jnp
from jax import lax
from jax.experimental import pallas as pl
from jax.experimental.pallas import tpu as pltpu
from jax.sharding import Mesh
from jax.sharding import PartitionSpec as P


EPS = 1e-06
REP, Z, Y, X, CORE = 2, 8, 8, 4, 2
VMEM = pl.BlockSpec(memory_space=pltpu.VMEM)
SMEM = pl.BlockSpec(memory_space=pltpu.SMEM)


UP_STEPS = (("y", 4), ("z", 4), ("y", 2), ("z", 2), ("z", 1), ("y", 1))
DOWN_STEPS = (("z", 4), ("y", 4), ("z", 2), ("y", 2), ("y", 1), ("z", 1))


def from_side(array, axis, shift):
    names, size = (("y", "core"), Y) if axis == "y" else (("rep", "z", "core"), REP * Z)
    pairs = []
    for i in range(size):
        pairs.append(((i + shift) % size * 2, i * 2))
        pairs.append(((i - shift) % size * 2 + 1, i * 2 + 1))
    return lax.ppermute(array, names, pairs)


def along_x(array, ahead):
    pairs = [(x, (x + ahead) % X) for x in range(X)]
    return lax.ppermute(array, "x", pairs)


def offsets(steps):
    laid = [(0, 0)]
    for axis, shift in steps:
        dz, dy = (shift, 0) if axis == "z" else (0, shift)
        laid = laid + [(z + dz, y + dy) for z, y in laid]
    return laid


def kernel_call(kernel, outs, n_vmem, scratch=(), smem=True, mib=8, flops=0, **rest):
    single = not isinstance(outs, tuple)
    return pl.pallas_call(
        kernel,
        out_shape=outs,
        in_specs=([SMEM] if smem else []) + [VMEM] * n_vmem,
        out_specs=VMEM if single else (VMEM,) * len(outs),
        scratch_shapes=[pltpu.VMEM(s, jnp.bfloat16) for s in scratch],
        compiler_params=pltpu.CompilerParams(vmem_limit_bytes=mib * 2**20),
        cost_estimate=pl.CostEstimate(
            flops=flops, bytes_accessed=2**20, transcendentals=0
        )
        if flops
        else None,
        **rest,
    )


def bf16(*shape):
    return jax.ShapeDtypeStruct(shape, jnp.bfloat16)


def join_kernel(a, b, out):
    n = a.shape[0]
    out[:n] = a[...]
    out[n:] = b[...]


def join(a, b):
    n = a.shape[0]
    return kernel_call(join_kernel, bf16(2 * n, 32, 512), 2, smem=False)(a, b)


def stage_kernel(where, up, down, up_out, down_out):
    up_out[...] = up[...]
    down_out[...] = down[...]


def norm_kernel(tokens, gain, normed):
    @pl.loop(0, 16)
    def _(n):
        rows = pl.ds(pl.multiple_of(n * 32, 32), 32)
        xf = tokens[rows, :].astype(jnp.float32)
        scale = lax.rsqrt(jnp.mean(xf * xf, axis=-1, keepdims=True) + EPS)
        normed[rows, :] = (xf * scale * gain[...]).astype(jnp.bfloat16)


def place(where, piece, laid, whole, halved):
    z, y, sign = where[0], where[1], 1 - 2 * where[2]
    for j, (dz, dy) in enumerate(laid):
        at_z = (z + sign * dz) & (Z - 1)
        at_y = (y + sign * dy) & (Y - 1)
        at = ((at_z >> 1) if halved else at_z) * Y + at_y
        whole[pl.ds(pl.multiple_of(at * 32, 32), 32), :] = piece[j]


def down_product(hidden, rows, down, out, part):
    @pl.loop(0, 4)
    def _(n):
        columns = pl.ds(pl.multiple_of(n * 256, 256), 256)
        out[part, :, columns] = lax.dot_general(
            hidden[rows, :],
            down[columns, :],
            (((1,), (1,)), ((), ())),
            preferred_element_type=jnp.float32,
        ).astype(jnp.bfloat16)


THEIRS, OWN = slice(0, 256), slice(256, 512)


def up_kernel(where, normed, u0, u1, hidden, up):
    laid = offsets(UP_STEPS)
    place(where, u0, laid[:32], up, False)
    place(where, u1, laid[32:], up, False)
    core = where[2]

    @pl.loop(0, 2)
    def _(n):
        columns = pl.ds(pl.multiple_of(n * 256, 256), 256)
        lifted = jnp.dot(
            normed[...], up[:, columns], preferred_element_type=jnp.float32
        )
        active = jnp.square(jnp.maximum(lifted, 0.0)).astype(jnp.bfloat16)
        for j in range(X * CORE):
            x, c = divmod(j, CORE)
            side = jnp.where(core == c, 256, 0)
            rows = pl.ds(pl.multiple_of(side + x * 64, 64), 64)
            hidden[rows, columns] = active[j * 64 : (j + 1) * 64]


def early_kernel(where, hidden, d0, theirs, own, down):
    place(where, d0, offsets(DOWN_STEPS)[:32], down, True)
    down_product(hidden, THEIRS, down, theirs, 0)
    down_product(hidden, OWN, down, own, 0)


def late_kernel(where, hidden, d1, theirs_in, theirs, down):
    place(where, d1, offsets(DOWN_STEPS)[32:], down, True)
    down_product(hidden, THEIRS, down, theirs, 1)


def own_kernel(hidden, down, own_in, own):
    down_product(hidden, OWN, down, own, 1)


def add_kernel(where, own, beside, keep, ahead, back, far):
    x = where[3]
    for out, step in ((far, 2), (ahead, 1), (back, 3), (keep, 0)):
        rows = pl.ds(pl.multiple_of(((x + step) & (X - 1)) * 64, 64), 64)
        for part in range(2):
            total = own[part, rows].astype(jnp.float32)
            total = total + beside[part, rows].astype(jnp.float32)
            out[part] = total.astype(jnp.bfloat16)


def last_kernel(where, residual, a, b, c, d, out):
    odd = where[0] & 1
    for part in range(2):
        for k in range(4):
            at = (2 * k + (odd ^ part)) * 256
            columns = pl.ds(pl.multiple_of(at, 256), 256)
            here = slice(k * 256, (k + 1) * 256)
            total = residual[:, columns].astype(jnp.float32)
            for term in (a, b, c, d):
                total = total + term[part, :, here].astype(jnp.float32)
            out[:, columns] = total.astype(jnp.bfloat16)


def gathered(where, up, down):
    for k in range(5):
        up_in = from_side(up, *UP_STEPS[k])
        down_in = from_side(down, *DOWN_STEPS[k])
        if k == 0:
            own = bf16(1, 32, 512)
            up, down = kernel_call(stage_kernel, (own, own), 2)(where, up, down)
        up = join(up, up_in)
        down = join(down, down_in)
    up_in = from_side(up, *UP_STEPS[5])
    down_in = from_side(down, *DOWN_STEPS[5])
    return (up, up_in), (down, down_in)


def over_tp(where, beside, own, residual):
    piece = bf16(2, 64, 1024)
    keep, ahead, back, far = kernel_call(add_kernel, (piece,) * 4, 2)(
        where, own, beside
    )
    far, ahead, back = along_x(far, 2), along_x(ahead, 1), along_x(back, 3)
    return kernel_call(last_kernel, bf16(64, 2048), 5)(
        where, residual, keep, ahead, back, far
    )


def shards(tokens, norm_gain, up_weight, down_weight):
    core, x = lax.axis_index("core"), lax.axis_index("x")
    where = jnp.stack([lax.axis_index("z"), lax.axis_index("y"), core, x]).astype(
        jnp.int32
    )
    up, down = gathered(where, up_weight[None], down_weight.T[None])
    normed = kernel_call(
        norm_kernel, bf16(512, 2048), 2, smem=False, mib=12, flops=2**24
    )(tokens, norm_gain[None])
    residual = lax.dynamic_slice_in_dim(tokens, (x * CORE + core) * 64, 64, 0)
    hidden = kernel_call(
        up_kernel, bf16(512, 512), 3, scratch=((2048, 512),), mib=12, flops=2**30
    )(where, normed, *up)
    out = bf16(2, 256, 1024)
    theirs, own = kernel_call(
        early_kernel, (out, out), 2, scratch=((1024, 512),), flops=2**29
    )(where, hidden, down[0])
    theirs, rest = kernel_call(
        late_kernel,
        (out, bf16(1024, 512)),
        3,
        flops=2**28,
        input_output_aliases={3: 0},
    )(where, hidden, down[1], theirs)
    beside = lax.ppermute(theirs, "core", [(0, 1), (1, 0)])
    own = kernel_call(
        own_kernel,
        out,
        3,
        smem=False,
        flops=2**28,
        input_output_aliases={2: 0},
    )(hidden, rest, own)
    return over_tp(where, beside, own, residual)


def solution(mesh):
    torus = Mesh(
        mesh.devices.reshape(REP, Z, Y, X, CORE), ("rep", "z", "y", "x", "core")
    )
    rep_fs = ("rep", "z", "y")
    tp = ("x", "core")
    in_specs = (P(rep_fs, None), P(), P(("z", "y"), tp), P(tp, ("z", "y")))
    return jax.shard_map(
        shards,
        mesh=torus,
        in_specs=in_specs,
        out_specs=P(rep_fs + tp, None),
        check_vma=False,
    )
```

time: 124 us -> 139 us (1.12)
  the two profiles are of different devices: /device:TPU:56 before, /device:TPU:1 now
where the time goes in v2:
time: 139 us; the launch traced here: 136 us
  starting transfers between devices  72.3 us (52%)
  waiting for transfers between devices  48.5 us (35%)
  Pallas kernels  13.6 us (10%)
  local copies, waits for them, and re-layouts  1.55 us (1%)
    ppermute x12, starting transfers between devices, from_side(): return lax.ppermute(array, names, pairs)  55.5 us
    ppermute x12, waiting for transfers between devices, from_side(): return lax.ppermute(array, names, pairs)  40.5 us
    ppermute x3, starting transfers between devices, along_x(): return lax.ppermute(array, 'x', pairs)  9.94 us
    ppermute x3, waiting for transfers between devices, along_x(): return lax.ppermute(array, 'x', pairs)  6.86 us
    ppermute x1, starting transfers between devices, shards(): beside = lax.ppermute(theirs, 'core', [(0, 1), (1, 0)])  6.82 us
  transfers between devices with their start and end apart: 16, of which 12 were waited for; matrix products, arithmetic and copies ran while one was open for 0% of the time, Pallas kernels for 7%

profile of v2, /device:TPU:1, one launch (start us, length us, event | category | flops | bytes accessed | tf_op | source)
XLA Modules:
  0.0 136.3 jit_solution(7445133076132420669)
XLA Ops:
  0.0 8.3 %collective-permute-start = (bf16[1,32,512]{2,1,0:T(8,128)(2,1)}, bf16[1,32,512]{2,1,0:T(8,128)(2,1)S(1)}, u32[]{:S(2)}, u32[]{:S(2)}) collective-permute-start(bf16[1,32,512]{2,1,0:T(8,128)(2,1)} %bitcast.9), channel_id=1, source_target_pairs={{32,0},{33,1},{40,8},{41,9},{48,16},{49,17},{56,24},{57,25},{0,32}... | collective-permute-start | bytes 98312 | tf_op jit(solution)/shard_map/ppermute | solution.py:26
  10.5 10.6 %collective-permute-start.1 = (bf16[2,32,512]{2,1,0:T(8,128)(2,1)S(1)}, bf16[2,32,512]{2,1,0:T(8,128)(2,1)S(1)}, u32[]{:S(2)}, u32[]{:S(2)}) collective-permute-start(bf16[2,32,512]{2,1,0:T(8,128)(2,1)S(1)} %shard_map.48.a), channel_id=1, source_target_pairs={{256,0},{769,1},{320,64},{833,65},{384,128},{897,129},{448,192},{9... | collective-permute-start | bytes 196616 | tf_op jit(solution)/shard_map/ppermute | solution.py:26
  21.1 9.2 %collective-permute-done.1.b = bf16[2,32,512]{2,1,0:T(8,128)(2,1)S(1)} collective-permute-done((bf16[2,32,512]{2,1,0:T(8,128)(2,1)S(1)}, bf16[2,32,512]{2,1,0:T(8,128)(2,1)S(1)}, u32[]{:S(2)}, u32[]{:S(2)}) %collective-permute-start.1) | collective-permute-done | bytes 65568 | tf_op jit(solution)/shard_map/ppermute | solution.py:26
  30.3 3.8 %collective-permute-start.2 = (bf16[4,32,512]{2,1,0:T(8,128)(2,1)S(1)}, bf16[4,32,512]{2,1,0:T(8,128)(2,1)S(1)}, u32[]{:S(2)}, u32[]{:S(2)}) collective-permute-start(bf16[4,32,512]{2,1,0:T(8,128)(2,1)S(1)} %shard_map.49.a), channel_id=1, source_target_pairs={{16,0},{49,1},{24,8},{57,9},{32,16},{1,17},{40,24},{9,25},{48,32},... | collective-permute-start | bytes 393224 | tf_op jit(solution)/shard_map/ppermute | solution.py:26
  34.0 2.8 %collective-permute-start.6 = (bf16[1,32,512]{2,1,0:T(8,128)(2,1)}, bf16[1,32,512]{2,1,0:T(8,128)(2,1)S(1)}, u32[]{:S(2)}, u32[]{:S(2)}) collective-permute-start(bf16[1,32,512]{2,1,0:T(8,128)(2,1)} %bitcast.11), channel_id=1, source_target_pairs={{256,0},{769,1},{320,64},{833,65},{384,128},{897,129},{448,192},{9... | collective-permute-start | bytes 98312 | tf_op jit(solution)/shard_map/ppermute | solution.py:26
  36.8 6.0 %collective-permute-done.6.b = bf16[1,32,512]{2,1,0:T(8,128)(2,1)S(1)} collective-permute-done((bf16[1,32,512]{2,1,0:T(8,128)(2,1)}, bf16[1,32,512]{2,1,0:T(8,128)(2,1)S(1)}, u32[]{:S(2)}, u32[]{:S(2)}) %collective-permute-start.6) | collective-permute-done | bytes 32800 | tf_op jit(solution)/shard_map/ppermute | solution.py:26
  42.8 5.2 %collective-permute-start.7 = (bf16[2,32,512]{2,1,0:T(8,128)(2,1)S(1)}, bf16[2,32,512]{2,1,0:T(8,128)(2,1)S(1)}, u32[]{:S(2)}, u32[]{:S(2)}) collective-permute-start(bf16[2,32,512]{2,1,0:T(8,128)(2,1)S(1)} %shard_map.54.a), channel_id=1, source_target_pairs={{32,0},{33,1},{40,8},{41,9},{48,16},{49,17},{56,24},{57,25},{0,32}... | collective-permute-start | bytes 196616 | tf_op jit(solution)/shard_map/ppermute | solution.py:26
  48.1 5.3 %collective-permute-start.3 = (bf16[8,32,512]{2,1,0:T(8,128)(2,1)S(1)}, bf16[8,32,512]{2,1,0:T(8,128)(2,1)S(1)}, u32[]{:S(2)}, u32[]{:S(2)}) collective-permute-start(bf16[8,32,512]{2,1,0:T(8,128)(2,1)S(1)} %shard_map.50.a), channel_id=1, source_target_pairs={{128,0},{897,1},{192,64},{961,65},{256,128},{1,129},{320,192},{65,... | collective-permute-start | bytes 786440 | tf_op jit(solution)/shard_map/ppermute | solution.py:26
  53.4 3.9 %collective-permute-start.8 = (bf16[4,32,512]{2,1,0:T(8,128)(2,1)S(1)}, bf16[4,32,512]{2,1,0:T(8,128)(2,1)S(1)}, u32[]{:S(2)}, u32[]{:S(2)}) collective-permute-start(bf16[4,32,512]{2,1,0:T(8,128)(2,1)S(1)} %shard_map.55.a), channel_id=1, source_target_pairs={{128,0},{897,1},{192,64},{961,65},{256,128},{1,129},{320,192},{65,... | collective-permute-start | bytes 393224 | tf_op jit(solution)/shard_map/ppermute | solution.py:26
  57.3 8.5 %collective-permute-done.8.b = bf16[4,32,512]{2,1,0:T(8,128)(2,1)S(1)} collective-permute-done((bf16[4,32,512]{2,1,0:T(8,128)(2,1)S(1)}, bf16[4,32,512]{2,1,0:T(8,128)(2,1)S(1)}, u32[]{:S(2)}, u32[]{:S(2)}) %collective-permute-start.8) | collective-permute-done | bytes 131104 | tf_op jit(solution)/shard_map/ppermute | solution.py:26
  65.8 3.4 %collective-permute-start.9 = (bf16[8,32,512]{2,1,0:T(8,128)(2,1)S(1)}, bf16[8,32,512]{2,1,0:T(8,128)(2,1)S(1)}, u32[]{:S(2)}, u32[]{:S(2)}) collective-permute-start(bf16[8,32,512]{2,1,0:T(8,128)(2,1)S(1)} %shard_map.56.a), channel_id=1, source_target_pairs={{16,0},{49,1},{24,8},{57,9},{32,16},{1,17},{40,24},{9,25},{48,32},... | collective-permute-start | bytes 786440 | tf_op jit(solution)/shard_map/ppermute | solution.py:26
  69.3 4.2 %collective-permute-start.4 = (bf16[16,32,512]{2,1,0:T(8,128)(2,1)S(1)}, bf16[16,32,512]{2,1,0:T(8,128)(2,1)S(1)}, u32[]{:S(2)}, u32[]{:S(2)}) collective-permute-start(bf16[16,32,512]{2,1,0:T(8,128)(2,1)S(1)} %shard_map.51.a), channel_id=1, source_target_pairs={{64,0},{961,1},{128,64},{1,65},{192,128},{65,129},{256,192},{129,1... | collective-permute-start | bytes 1572872 | tf_op jit(solution)/shard_map/ppermute | solution.py:26
  73.4 4.1 %collective-permute-done.9.b = bf16[8,32,512]{2,1,0:T(8,128)(2,1)S(1)} collective-permute-done((bf16[8,32,512]{2,1,0:T(8,128)(2,1)S(1)}, bf16[8,32,512]{2,1,0:T(8,128)(2,1)S(1)}, u32[]{:S(2)}, u32[]{:S(2)}) %collective-permute-start.9) | collective-permute-done | bytes 262176 | tf_op jit(solution)/shard_map/ppermute | solution.py:26
  77.6 2.9 %collective-permute-start.10 = (bf16[16,32,512]{2,1,0:T(8,128)(2,1)S(1)}, bf16[16,32,512]{2,1,0:T(8,128)(2,1)S(1)}, u32[]{:S(2)}, u32[]{:S(2)}) collective-permute-start(bf16[16,32,512]{2,1,0:T(8,128)(2,1)S(1)} %shard_map.57.a), channel_id=1, source_target_pairs={{8,0},{57,1},{16,8},{1,9},{24,16},{9,17},{32,24},{17,25},{40,32},{... | collective-permute-start | bytes 1572872 | tf_op jit(solution)/shard_map/ppermute | solution.py:26
  81.0 2.6 %collective-permute-start.5 = (bf16[32,32,512]{2,1,0:T(8,128)(2,1)S(1)}, bf16[32,32,512]{2,1,0:T(8,128)(2,1)S(1)}, u32[]{:S(2)}, u32[]{:S(2)}) collective-permute-start(bf16[32,32,512]{2,1,0:T(8,128)(2,1)S(1)} %shard_map.52.u0), channel_id=1, source_target_pairs={{8,0},{57,1},{16,8},{1,9},{24,16},{9,17},{32,24},{17,25},{40,32},{... | collective-permute-start | bytes 3145736 | tf_op jit(solution)/shard_map/ppermute | solution.py:26
  83.6 5.3 %collective-permute-done.10.b = bf16[16,32,512]{2,1,0:T(8,128)(2,1)S(1)} collective-permute-done((bf16[16,32,512]{2,1,0:T(8,128)(2,1)S(1)}, bf16[16,32,512]{2,1,0:T(8,128)(2,1)S(1)}, u32[]{:S(2)}, u32[]{:S(2)}) %collective-permute-start.10) | collective-permute-done | bytes 524320 | tf_op jit(solution)/shard_map/ppermute | solution.py:26
  89.0 2.6 %collective-permute-start.11 = (bf16[32,32,512]{2,1,0:T(8,128)(2,1)S(1)}, bf16[32,32,512]{2,1,0:T(8,128)(2,1)S(1)}, u32[]{:S(2)}, u32[]{:S(2)}) collective-permute-start(bf16[32,32,512]{2,1,0:T(8,128)(2,1)S(1)} %shard_map.58.d0), channel_id=1, source_target_pairs={{64,0},{961,1},{128,64},{1,65},{192,128},{65,129},{256,192},{129,1... | collective-permute-start | bytes 3145736 | tf_op jit(solution)/shard_map/ppermute | solution.py:26
  91.6 2.1 %shard_map.46.normed = bf16[512,2048]{1,0:T(8,128)(2,1)S(1)} custom-call(bf16[512,2048]{1,0:T(8,128)(2,1)S(1)} %copy-done, f32[1,2048]{1,0:T(1,128)S(1)} %bitcast.13), custom_call_target="tpu_custom_call" | custom-call | flops 16777216 | bytes 1048576 | tf_op jit(solution)/shard_map/pallas_call | solution.py:202
  93.7 6.4 %collective-permute-done.5.u1 = bf16[32,32,512]{2,1,0:T(8,128)(2,1)S(1)} collective-permute-done((bf16[32,32,512]{2,1,0:T(8,128)(2,1)S(1)}, bf16[32,32,512]{2,1,0:T(8,128)(2,1)S(1)}, u32[]{:S(2)}, u32[]{:S(2)}) %collective-permute-start.5) | collective-permute-done | bytes 1048608 | tf_op jit(solution)/shard_map/ppermute | solution.py:26
  100.1 2.2 %shard_map.53.hidden = bf16[512,512]{1,0:T(8,128)(2,1)S(1)} custom-call(s32[4]{0:T(128)S(1)} %pad_add_fusion.where, bf16[512,2048]{1,0:T(8,128)(2,1)S(1)} %shard_map.46.normed, bf16[32,32,512]{2,1,0:T(8,128)(2,1)S(1)} %shard_map.52.u0, bf16[32,32,512]{2,1,0:T(8,128)(2,1)S(1)} %collective-permute-done.5.u1), custom_call_target="tpu_custom_call" | custom-call | flops 1073741824 | bytes 1048576 | tf_op jit(solution)/shard_map/pallas_call | solution.py:206
  102.3 2.8 %shard_map.59 = (bf16[2,256,1024]{2,1,0:T(8,128)(2,1)S(1)}, bf16[2,256,1024]{2,1,0:T(8,128)(2,1)S(1)}) custom-call(s32[4]{0:T(128)S(1)} %pad_add_fusion.where, bf16[512,512]{1,0:T(8,128)(2,1)S(1)} %shard_map.53.hidden, bf16[32,32,512]{2,1,0:T(8,128)(2,1)S(1)} %shard_map.58.d0), custom_call_target="tpu_custom_call" | custom-call | flops 536870912 | bytes 1048576 | tf_op jit(solution)/shard_map/pallas_call | solution.py:210
  105.7 1.7 %shard_map.60 = (bf16[2,256,1024]{2,1,0:T(8,128)(2,1)S(1)}, bf16[1024,512]{1,0:T(8,128)(2,1)S(1)}) custom-call(s32[4]{0:T(128)S(1)} %pad_add_fusion.where, bf16[512,512]{1,0:T(8,128)(2,1)S(1)} %shard_map.53.hidden, bf16[32,32,512]{2,1,0:T(8,128)(2,1)S(1)} %collective-permute-done.11.d1, ...), custom_call_target="tpu_custom_call", output_to_operand_aliasing={{0}: (3, {})} | custom-call | flops 268435456 | bytes 1048576 | tf_op jit(solution)/shard_map/pallas_call | solution.py:213
  107.4 6.8 %collective-permute-start.12 = (bf16[2,256,1024]{2,1,0:T(8,128)(2,1)S(1)}, bf16[2,256,1024]{2,1,0:T(8,128)(2,1)S(1)}, u32[]{:S(2)}, u32[]{:S(2)}) collective-permute-start(bf16[2,256,1024]{2,1,0:T(8,128)(2,1)S(1)} %get-tuple-element.20), channel_id=1, source_target_pairs={{0,1},{1,0},{2,3},{3,2},{4,5},{5,4},{6,7},{7,6},{8,9},{9,8},{10,11... | collective-permute-start | bytes 3145736 | tf_op jit(solution)/shard_map/ppermute | solution.py:220
  114.3 1.1 shard_map.61.own
  115.4 1.2 collective-permute-done.12.beside
  116.5 1.5 %shard_map.62 = (bf16[2,64,1024]{2,1,0:T(8,128)(2,1)S(1)}, bf16[2,64,1024]{2,1,0:T(8,128)(2,1)}, bf16[2,64,1024]{2,1,0:T(8,128)(2,1)}, bf16[2,64,1024]{2,1,0:T(8,128)(2,1)S(1)}) custom-call(s32[4]{0:T(128)S(1)} %pad_add_fusion.where, bf16[2,256,1024]{2,1,0:T(8,128)(2,1)S(1)} %shard_map.61.own, bf16[2,256,1024]{2,1,0:T(8,128)(2,1)S(1)} %collective-permute-done.12.beside), custom_call_target="tpu_custom_call" | custom-call | tf_op jit(solution)/shard_map/pallas_call | solution.py:187
  118.0 3.1 %collective-permute-start.13 = (bf16[2,64,1024]{2,1,0:T(8,128)(2,1)}, bf16[2,64,1024]{2,1,0:T(8,128)(2,1)S(1)}, u32[]{:S(2)}, u32[]{:S(2)}) collective-permute-start(bf16[2,64,1024]{2,1,0:T(8,128)(2,1)} %get-tuple-element.22), channel_id=1, source_target_pairs={{0,2},{2,4},{4,6},{6,0},{1,3},{3,5},{5,7},{7,1},{8,10},{10,12},{12... | collective-permute-start | bytes 786440 | tf_op jit(solution)/shard_map/ppermute | solution.py:31
  121.2 3.4 %collective-permute-start.14 = (bf16[2,64,1024]{2,1,0:T(8,128)(2,1)}, bf16[2,64,1024]{2,1,0:T(8,128)(2,1)S(1)}, u32[]{:S(2)}, u32[]{:S(2)}) collective-permute-start(bf16[2,64,1024]{2,1,0:T(8,128)(2,1)} %get-tuple-element.23), channel_id=1, source_target_pairs={{0,6},{2,0},{4,2},{6,4},{1,7},{3,1},{5,3},{7,5},{8,14},{10,8},{12,... | collective-permute-start | bytes 786440 | tf_op jit(solution)/shard_map/ppermute | solution.py:31
  124.5 3.5 %collective-permute-start.15 = (bf16[2,64,1024]{2,1,0:T(8,128)(2,1)S(1)}, bf16[2,64,1024]{2,1,0:T(8,128)(2,1)S(1)}, u32[]{:S(2)}, u32[]{:S(2)}) collective-permute-start(bf16[2,64,1024]{2,1,0:T(8,128)(2,1)S(1)} %get-tuple-element.24), channel_id=1, source_target_pairs={{0,4},{2,6},{4,0},{6,2},{1,5},{3,7},{5,1},{7,3},{8,12},{10,14},{12... | collective-permute-start | bytes 786440 | tf_op jit(solution)/shard_map/ppermute | solution.py:31
  128.8 1.6 %collective-permute-done.14.c = bf16[2,64,1024]{2,1,0:T(8,128)(2,1)S(1)} collective-permute-done((bf16[2,64,1024]{2,1,0:T(8,128)(2,1)}, bf16[2,64,1024]{2,1,0:T(8,128)(2,1)S(1)}, u32[]{:S(2)}, u32[]{:S(2)}) %collective-permute-start.14) | collective-permute-done | bytes 262176 | tf_op jit(solution)/shard_map/ppermute | solution.py:31
  130.5 4.4 %collective-permute-done.15.d = bf16[2,64,1024]{2,1,0:T(8,128)(2,1)S(1)} collective-permute-done((bf16[2,64,1024]{2,1,0:T(8,128)(2,1)S(1)}, bf16[2,64,1024]{2,1,0:T(8,128)(2,1)S(1)}, u32[]{:S(2)}, u32[]{:S(2)}) %collective-permute-start.15) | collective-permute-done | bytes 262176 | tf_op jit(solution)/shard_map/ppermute | solution.py:31
  134.9 1.4 %shard_map.63 = bf16[64,2048]{1,0:T(8,128)(2,1)} custom-call(s32[4]{0:T(128)S(1)} %pad_add_fusion.where, bf16[64,2048]{1,0:T(8,128)(2,1)S(1)} %constant_dynamic-slice_fusion.residual, bf16[2,64,1024]{2,1,0:T(8,128)(2,1)S(1)} %get-tuple-element.21.a, bf16[2,64,1024]{2,1,0:T(8,128)(2,1)S(1)} %collective-permute-done.13.b, ...), custom_call_target="tpu_custom_call" | custom-call | tf_op jit(solution)/shard_map/pallas_call | solution.py:191
  (28 shorter events, 4.3 us)
Async XLA Ops:
  0.0 10.4 %collective-permute-start = (bf16[1,32,512]{2,1,0:T(8,128)(2,1)}, bf16[1,32,512]{2,1,0:T(8,128)(2,1)S(1)}, u32[]{:S(2)}, u32[]{:S(2)}) collective-permute-start(bf16[1,32,512]{2,1,0:T(8,128)(2,1)} %bitcast.9), channel_id=1, source_target_pairs={{32,0},{33,1},{40,8},{41,9},{48,16},{49,17},{56,24},{57,25},{0,32}... | collective-permute-start | bytes 98312 | tf_op jit(solution)/shard_map/ppermute | solution.py:26
  8.4 0.8 copy-start.1
  9.1 0.8 copy-start.2
  10.5 19.8 %collective-permute-start.1 = (bf16[2,32,512]{2,1,0:T(8,128)(2,1)S(1)}, bf16[2,32,512]{2,1,0:T(8,128)(2,1)S(1)}, u32[]{:S(2)}, u32[]{:S(2)}) collective-permute-start(bf16[2,32,512]{2,1,0:T(8,128)(2,1)S(1)} %shard_map.48.a), channel_id=1, source_target_pairs={{256,0},{769,1},{320,64},{833,65},{384,128},{897,129},{448,192},{9... | collective-permute-start | bytes 196616 | tf_op jit(solution)/shard_map/ppermute | solution.py:26
  30.3 17.8 %collective-permute-start.2 = (bf16[4,32,512]{2,1,0:T(8,128)(2,1)S(1)}, bf16[4,32,512]{2,1,0:T(8,128)(2,1)S(1)}, u32[]{:S(2)}, u32[]{:S(2)}) collective-permute-start(bf16[4,32,512]{2,1,0:T(8,128)(2,1)S(1)} %shard_map.49.a), channel_id=1, source_target_pairs={{16,0},{49,1},{24,8},{57,9},{32,16},{1,17},{40,24},{9,25},{48,32},... | collective-permute-start | bytes 393224 | tf_op jit(solution)/shard_map/ppermute | solution.py:26
  34.0 8.8 %collective-permute-start.6 = (bf16[1,32,512]{2,1,0:T(8,128)(2,1)}, bf16[1,32,512]{2,1,0:T(8,128)(2,1)S(1)}, u32[]{:S(2)}, u32[]{:S(2)}) collective-permute-start(bf16[1,32,512]{2,1,0:T(8,128)(2,1)} %bitcast.11), channel_id=1, source_target_pairs={{256,0},{769,1},{320,64},{833,65},{384,128},{897,129},{448,192},{9... | collective-permute-start | bytes 98312 | tf_op jit(solution)/shard_map/ppermute | solution.py:26
  42.8 10.5 %collective-permute-start.7 = (bf16[2,32,512]{2,1,0:T(8,128)(2,1)S(1)}, bf16[2,32,512]{2,1,0:T(8,128)(2,1)S(1)}, u32[]{:S(2)}, u32[]{:S(2)}) collective-permute-start(bf16[2,32,512]{2,1,0:T(8,128)(2,1)S(1)} %shard_map.54.a), channel_id=1, source_target_pairs={{32,0},{33,1},{40,8},{41,9},{48,16},{49,17},{56,24},{57,25},{0,32}... | collective-permute-start | bytes 196616 | tf_op jit(solution)/shard_map/ppermute | solution.py:26
  48.1 21.1 %collective-permute-start.3 = (bf16[8,32,512]{2,1,0:T(8,128)(2,1)S(1)}, bf16[8,32,512]{2,1,0:T(8,128)(2,1)S(1)}, u32[]{:S(2)}, u32[]{:S(2)}) collective-permute-start(bf16[8,32,512]{2,1,0:T(8,128)(2,1)S(1)} %shard_map.50.a), channel_id=1, source_target_pairs={{128,0},{897,1},{192,64},{961,65},{256,128},{1,129},{320,192},{65,... | collective-permute-start | bytes 786440 | tf_op jit(solution)/shard_map/ppermute | solution.py:26
  53.4 12.4 %collective-permute-start.8 = (bf16[4,32,512]{2,1,0:T(8,128)(2,1)S(1)}, bf16[4,32,512]{2,1,0:T(8,128)(2,1)S(1)}, u32[]{:S(2)}, u32[]{:S(2)}) collective-permute-start(bf16[4,32,512]{2,1,0:T(8,128)(2,1)S(1)} %shard_map.55.a), channel_id=1, source_target_pairs={{128,0},{897,1},{192,64},{961,65},{256,128},{1,129},{320,192},{65,... | collective-permute-start | bytes 393224 | tf_op jit(solution)/shard_map/ppermute | solution.py:26
  65.8 11.8 %collective-permute-start.9 = (bf16[8,32,512]{2,1,0:T(8,128)(2,1)S(1)}, bf16[8,32,512]{2,1,0:T(8,128)(2,1)S(1)}, u32[]{:S(2)}, u32[]{:S(2)}) collective-permute-start(bf16[8,32,512]{2,1,0:T(8,128)(2,1)S(1)} %shard_map.56.a), channel_id=1, source_target_pairs={{16,0},{49,1},{24,8},{57,9},{32,16},{1,17},{40,24},{9,25},{48,32},... | collective-permute-start | bytes 786440 | tf_op jit(solution)/shard_map/ppermute | solution.py:26
  69.3 11.6 %collective-permute-start.4 = (bf16[16,32,512]{2,1,0:T(8,128)(2,1)S(1)}, bf16[16,32,512]{2,1,0:T(8,128)(2,1)S(1)}, u32[]{:S(2)}, u32[]{:S(2)}) collective-permute-start(bf16[16,32,512]{2,1,0:T(8,128)(2,1)S(1)} %shard_map.51.a), channel_id=1, source_target_pairs={{64,0},{961,1},{128,64},{1,65},{192,128},{65,129},{256,192},{129,1... | collective-permute-start | bytes 1572872 | tf_op jit(solution)/shard_map/ppermute | solution.py:26
  77.6 14.0 %copy-start = (bf16[512,2048]{1,0:T(8,128)(2,1)S(1)}, bf16[512,2048]{1,0:T(8,128)(2,1)}, u32[]{:S(2)}) copy-start(bf16[512,2048]{1,0:T(8,128)(2,1)} %tokens.1) | copy-start | bytes 6291460
  77.6 14.0 %copy-start.3 = (f32[2048]{0:T(1024)S(1)}, f32[2048]{0:T(1024)}, u32[]{:S(2)}) copy-start(f32[2048]{0:T(1024)} %param.5) | copy-start | bytes 24580
  77.6 11.3 %collective-permute-start.10 = (bf16[16,32,512]{2,1,0:T(8,128)(2,1)S(1)}, bf16[16,32,512]{2,1,0:T(8,128)(2,1)S(1)}, u32[]{:S(2)}, u32[]{:S(2)}) collective-permute-start(bf16[16,32,512]{2,1,0:T(8,128)(2,1)S(1)} %shard_map.57.a), channel_id=1, source_target_pairs={{8,0},{57,1},{16,8},{1,9},{24,16},{9,17},{32,24},{17,25},{40,32},{... | collective-permute-start | bytes 1572872 | tf_op jit(solution)/shard_map/ppermute | solution.py:26
  81.0 19.1 %collective-permute-start.5 = (bf16[32,32,512]{2,1,0:T(8,128)(2,1)S(1)}, bf16[32,32,512]{2,1,0:T(8,128)(2,1)S(1)}, u32[]{:S(2)}, u32[]{:S(2)}) collective-permute-start(bf16[32,32,512]{2,1,0:T(8,128)(2,1)S(1)} %shard_map.52.u0), channel_id=1, source_target_pairs={{8,0},{57,1},{16,8},{1,9},{24,16},{9,17},{32,24},{17,25},{40,32},{... | collective-permute-start | bytes 3145736 | tf_op jit(solution)/shard_map/ppermute | solution.py:26
  89.0 16.8 %collective-permute-start.11 = (bf16[32,32,512]{2,1,0:T(8,128)(2,1)S(1)}, bf16[32,32,512]{2,1,0:T(8,128)(2,1)S(1)}, u32[]{:S(2)}, u32[]{:S(2)}) collective-permute-start(bf16[32,32,512]{2,1,0:T(8,128)(2,1)S(1)} %shard_map.58.d0), channel_id=1, source_target_pairs={{64,0},{961,1},{128,64},{1,65},{192,128},{65,129},{256,192},{129,1... | collective-permute-start | bytes 3145736 | tf_op jit(solution)/shard_map/ppermute | solution.py:26
  107.4 9.1 %collective-permute-start.12 = (bf16[2,256,1024]{2,1,0:T(8,128)(2,1)S(1)}, bf16[2,256,1024]{2,1,0:T(8,128)(2,1)S(1)}, u32[]{:S(2)}, u32[]{:S(2)}) collective-permute-start(bf16[2,256,1024]{2,1,0:T(8,128)(2,1)S(1)} %get-tuple-element.20), channel_id=1, source_target_pairs={{0,1},{1,0},{2,3},{3,2},{4,5},{5,4},{6,7},{7,6},{8,9},{9,8},{10,11... | collective-permute-start | bytes 3145736 | tf_op jit(solution)/shard_map/ppermute | solution.py:220
  118.0 10.8 %collective-permute-start.13 = (bf16[2,64,1024]{2,1,0:T(8,128)(2,1)}, bf16[2,64,1024]{2,1,0:T(8,128)(2,1)S(1)}, u32[]{:S(2)}, u32[]{:S(2)}) collective-permute-start(bf16[2,64,1024]{2,1,0:T(8,128)(2,1)} %get-tuple-element.22), channel_id=1, source_target_pairs={{0,2},{2,4},{4,6},{6,0},{1,3},{3,5},{5,7},{7,1},{8,10},{10,12},{12... | collective-permute-start | bytes 786440 | tf_op jit(solution)/shard_map/ppermute | solution.py:31
  121.2 9.3 %collective-permute-start.14 = (bf16[2,64,1024]{2,1,0:T(8,128)(2,1)}, bf16[2,64,1024]{2,1,0:T(8,128)(2,1)S(1)}, u32[]{:S(2)}, u32[]{:S(2)}) collective-permute-start(bf16[2,64,1024]{2,1,0:T(8,128)(2,1)} %get-tuple-element.23), channel_id=1, source_target_pairs={{0,6},{2,0},{4,2},{6,4},{1,7},{3,1},{5,3},{7,5},{8,14},{10,8},{12,... | collective-permute-start | bytes 786440 | tf_op jit(solution)/shard_map/ppermute | solution.py:31
  124.5 10.4 %collective-permute-start.15 = (bf16[2,64,1024]{2,1,0:T(8,128)(2,1)S(1)}, bf16[2,64,1024]{2,1,0:T(8,128)(2,1)S(1)}, u32[]{:S(2)}, u32[]{:S(2)}) collective-permute-start(bf16[2,64,1024]{2,1,0:T(8,128)(2,1)S(1)} %get-tuple-element.24), channel_id=1, source_target_pairs={{0,4},{2,6},{4,0},{6,2},{1,5},{3,7},{5,1},{7,3},{8,12},{10,14},{12... | collective-permute-start | bytes 786440 | tf_op jit(solution)/shard_map/ppermute | solution.py:31

commit v3 on v2

--- a/solution.py
+++ b/solution.py
@@ -13,8 +13,8 @@
 SMEM = pl.BlockSpec(memory_space=pltpu.SMEM)
 
 
-UP_STEPS = (("y", 4), ("z", 4), ("y", 2), ("z", 2), ("z", 1), ("y", 1))
-DOWN_STEPS = (("z", 4), ("y", 4), ("z", 2), ("y", 2), ("y", 1), ("z", 1))
+UP_STEPS = (("y", 4), ("z", 4), ("y", 2), ("z", 2))
+DOWN_STEPS = (("z", 4), ("y", 4), ("z", 2), ("y", 2))
 
 
 def from_side(array, axis, shift):
@@ -26,9 +26,12 @@
     return lax.ppermute(array, names, pairs)
 
 
-def along_x(array, ahead):
-    pairs = [(x, (x + ahead) % X) for x in range(X)]
-    return lax.ppermute(array, "x", pairs)
+def between_x(array, first, second):
+    pairs = []
+    for x in range(X):
+        pairs.append((x * 2, (x ^ first) * 2))
+        pairs.append((x * 2 + 1, (x ^ second) * 2 + 1))
+    return lax.ppermute(array, ("x", "core"), pairs)
 
 
 def offsets(steps):
@@ -37,6 +40,10 @@
         dz, dy = (shift, 0) if axis == "z" else (0, shift)
         laid = laid + [(z + dz, y + dy) for z, y in laid]
     return laid
+
+
+def shifted(steps, dz, dy):
+    return [(z + dz, y + dy) for z, y in offsets(steps)]
 
 
 def kernel_call(kernel, outs, n_vmem, scratch=(), smem=True, mib=8, flops=0, **rest):
@@ -110,10 +117,9 @@
 THEIRS, OWN = slice(0, 256), slice(256, 512)
 
 
-def up_kernel(where, normed, u0, u1, hidden, up):
-    laid = offsets(UP_STEPS)
-    place(where, u0, laid[:32], up, False)
-    place(where, u1, laid[32:], up, False)
+def up_kernel(where, normed, u0, uz, uy, uzy, hidden, up):
+    for piece, shift in ((u0, (0, 0)), (uz, (1, 0)), (uy, (0, 1)), (uzy, (1, 1))):
+        place(where, piece, shifted(UP_STEPS, *shift), up, False)
     core = where[2]
 
     @pl.loop(0, 2)
@@ -130,14 +136,16 @@
             hidden[rows, columns] = active[j * 64 : (j + 1) * 64]
 
 
-def early_kernel(where, hidden, d0, theirs, own, down):
-    place(where, d0, offsets(DOWN_STEPS)[:32], down, True)
+def early_kernel(where, hidden, d0, dy, theirs, own, down):
+    place(where, d0, offsets(DOWN_STEPS), down, True)
+    place(where, dy, shifted(DOWN_STEPS, 0, 1), down, True)
     down_product(hidden, THEIRS, down, theirs, 0)
     down_product(hidden, OWN, down, own, 0)
 
 
-def late_kernel(where, hidden, d1, theirs_in, theirs, down):
-    place(where, d1, offsets(DOWN_STEPS)[32:], down, True)
+def late_kernel(where, hidden, dz, dyz, theirs_in, theirs, down):
+    place(where, dz, shifted(DOWN_STEPS, 1, 0), down, True)
+    place(where, dyz, shifted(DOWN_STEPS, 1, 1), down, True)
     down_product(hidden, THEIRS, down, theirs, 1)
 
 
@@ -145,17 +153,28 @@
     down_product(hidden, OWN, down, own, 1)
 
 
-def add_kernel(where, own, beside, keep, ahead, back, far):
-    x = where[3]
-    for out, step in ((far, 2), (ahead, 1), (back, 3), (keep, 0)):
-        rows = pl.ds(pl.multiple_of(((x + step) & (X - 1)) * 64, 64), 64)
+def add_kernel(where, own, beside, keep, send):
+    x, core = where[3], where[2]
+    first, second = 1 + 2 * core, 3 - 2 * core
+    for out, k, chunk in (
+        (send, 0, x ^ first),
+        (send, 1, x ^ 2),
+        (keep, 0, x),
+        (keep, 1, x ^ second),
+    ):
+        rows = pl.ds(pl.multiple_of(chunk * 64, 64), 64)
         for part in range(2):
             total = own[part, rows].astype(jnp.float32)
             total = total + beside[part, rows].astype(jnp.float32)
-            out[part] = total.astype(jnp.bfloat16)
-
-
-def last_kernel(where, residual, a, b, c, d, out):
+            out[k, part] = total.astype(jnp.bfloat16)
+
+
+def pass_kernel(keep, came, out):
+    total = keep[1].astype(jnp.float32) + came[1].astype(jnp.float32)
+    out[...] = total.astype(jnp.bfloat16)
+
+
+def last_kernel(where, residual, keep, came, late, out):
     odd = where[0] & 1
     for part in range(2):
         for k in range(4):
@@ -163,13 +182,13 @@
             columns = pl.ds(pl.multiple_of(at, 256), 256)
             here = slice(k * 256, (k + 1) * 256)
             total = residual[:, columns].astype(jnp.float32)
-            for term in (a, b, c, d):
+            for term in (keep.at[0], came.at[0], late):
                 total = total + term[part, :, here].astype(jnp.float32)
             out[:, columns] = total.astype(jnp.bfloat16)
 
 
 def gathered(where, up, down):
-    for k in range(5):
+    for k in range(4):
         up_in = from_side(up, *UP_STEPS[k])
         down_in = from_side(down, *DOWN_STEPS[k])
         if k == 0:
@@ -177,19 +196,23 @@
             up, down = kernel_call(stage_kernel, (own, own), 2)(where, up, down)
         up = join(up, up_in)
         down = join(down, down_in)
-    up_in = from_side(up, *UP_STEPS[5])
-    down_in = from_side(down, *DOWN_STEPS[5])
-    return (up, up_in), (down, down_in)
+    up_z = from_side(up, "z", 1)
+    up_y = from_side(up, "y", 1)
+    down_y = from_side(down, "y", 1)
+    down_z = from_side(down, "z", 1)
+    up_zy = from_side(up_z, "y", 1)
+    down_yz = from_side(down_y, "z", 1)
+    return (up, up_z, up_y, up_zy), (down, down_y, down_z, down_yz)
 
 
 def over_tp(where, beside, own, residual):
-    piece = bf16(2, 64, 1024)
-    keep, ahead, back, far = kernel_call(add_kernel, (piece,) * 4, 2)(
-        where, own, beside
-    )
-    far, ahead, back = along_x(far, 2), along_x(ahead, 1), along_x(back, 3)
-    return kernel_call(last_kernel, bf16(64, 2048), 5)(
-        where, residual, keep, ahead, back, far
+    two = bf16(2, 2, 64, 1024)
+    keep, send = kernel_call(add_kernel, (two, two), 2)(where, own, beside)
+    came = between_x(send, 1, 3)
+    passed = kernel_call(pass_kernel, bf16(2, 64, 1024), 2, smem=False)(keep, came)
+    late = between_x(passed, 3, 1)
+    return kernel_call(last_kernel, bf16(64, 2048), 4)(
+        where, residual, keep, came, late
     )
 
 
@@ -204,19 +227,19 @@
     )(tokens, norm_gain[None])
     residual = lax.dynamic_slice_in_dim(tokens, (x * CORE + core) * 64, 64, 0)
     hidden = kernel_call(
-        up_kernel, bf16(512, 512), 3, scratch=((2048, 512),), mib=12, flops=2**30
+        up_kernel, bf16(512, 512), 5, scratch=((2048, 512),), mib=12, flops=2**30
     )(where, normed, *up)
     out = bf16(2, 256, 1024)
     theirs, own = kernel_call(
-        early_kernel, (out, out), 2, scratch=((1024, 512),), flops=2**29
-    )(where, hidden, down[0])
+        early_kernel, (out, out), 3, scratch=((1024, 512),), flops=2**29
+    )(where, hidden, *down[:2])
     theirs, rest = kernel_call(
         late_kernel,
         (out, bf16(1024, 512)),
-        3,
+        4,
         flops=2**28,
-        input_output_aliases={3: 0},
-    )(where, hidden, down[1], theirs)
+        input_output_aliases={4: 0},
+    )(where, hidden, *down[2:], theirs)
     beside = lax.ppermute(theirs, "core", [(0, 1), (1, 0)])
     own = kernel_call(
         own_kernel,

time: 139 us -> 139 us (level)
  starting transfers between devices: 72.3 us -> 74 us
    ppermute x12 -> x14, waiting for transfers between devices: 40.5 us -> 34.3 us  [from_side(): return lax.ppermute(array, names, pairs)]
    ppermute x12 -> x14, starting transfers between devices: 55.5 us -> 61.2 us  [from_side(): return lax.ppermute(array, names, pairs)]
    ppermute x3 -> x2, waiting for transfers between devices: 6.86 us -> 12 us  [between_x(): return lax.ppermute(array, ('x', 'core'), pairs)]
    ppermute x3 -> x2, starting transfers between devices: 9.94 us -> 6.57 us  [between_x(): return lax.ppermute(array, ('x', 'core'), pairs)]
    pallas_call x5 -> x6, Pallas kernels: 9.61 us -> 9.28 us  [the longest x1 2.77 us: shards(): kernel_call(early_kernel, (out, out), 3, scratch=((1024, 512),), flops=2...]
  transfers between devices with their start and end apart: 16 -> 17, of which waited for: 12 -> 9; matrix products, arithmetic and copies ran while one was open for 0% -> 0% of each run, Pallas kernels for 7% -> 6%
where the time goes in v3:
time: 139 us; the launch traced here: 137 us
  starting transfers between devices  74 us (53%)
  waiting for transfers between devices  47.5 us (34%)
  Pallas kernels  13.1 us (9%)
  local copies, waits for them, and re-layouts  1.55 us (1%)
    ppermute x14, starting transfers between devices, from_side(): return lax.ppermute(array, names, pairs)  61.2 us
    ppermute x14, waiting for transfers between devices, from_side(): return lax.ppermute(array, names, pairs)  34.3 us
    ppermute x2, waiting for transfers between devices, between_x(): return lax.ppermute(array, ('x', 'core'), pairs)  12 us
    ppermute x2, starting transfers between devices, between_x(): return lax.ppermute(array, ('x', 'core'), pairs)  6.57 us
    ppermute x1, starting transfers between devices, shards(): beside = lax.ppermute(theirs, 'core', [(0, 1), (1, 0)])  6.24 us
  transfers between devices with their start and end apart: 17, of which 9 were waited for; matrix products, arithmetic and copies ran while one was open for 0% of the time, Pallas kernels for 6%

profile of v3, /device:TPU:1, one launch (start us, length us, event | category | flops | bytes accessed | tf_op | source)
XLA Modules:
  0.0 136.6 jit_solution(9906695399965490564)
XLA Ops:
  0.0 8.4 %collective-permute-start = (bf16[1,32,512]{2,1,0:T(8,128)(2,1)}, bf16[1,32,512]{2,1,0:T(8,128)(2,1)S(1)}, u32[]{:S(2)}, u32[]{:S(2)}) collective-permute-start(bf16[1,32,512]{2,1,0:T(8,128)(2,1)} %bitcast.9), channel_id=1, source_target_pairs={{32,0},{33,1},{40,8},{41,9},{48,16},{49,17},{56,24},{57,25},{0,32}... | collective-permute-start | bytes 98312 | tf_op jit(solution)/shard_map/ppermute | solution.py:26
  10.6 10.6 %collective-permute-start.1 = (bf16[2,32,512]{2,1,0:T(8,128)(2,1)S(1)}, bf16[2,32,512]{2,1,0:T(8,128)(2,1)S(1)}, u32[]{:S(2)}, u32[]{:S(2)}) collective-permute-start(bf16[2,32,512]{2,1,0:T(8,128)(2,1)S(1)} %shard_map.48.a), channel_id=1, source_target_pairs={{256,0},{769,1},{320,64},{833,65},{384,128},{897,129},{448,192},{9... | collective-permute-start | bytes 196616 | tf_op jit(solution)/shard_map/ppermute | solution.py:26
  21.2 9.2 %collective-permute-done.1.b = bf16[2,32,512]{2,1,0:T(8,128)(2,1)S(1)} collective-permute-done((bf16[2,32,512]{2,1,0:T(8,128)(2,1)S(1)}, bf16[2,32,512]{2,1,0:T(8,128)(2,1)S(1)}, u32[]{:S(2)}, u32[]{:S(2)}) %collective-permute-start.1) | collective-permute-done | bytes 65568 | tf_op jit(solution)/shard_map/ppermute | solution.py:26
  30.4 3.8 %collective-permute-start.2 = (bf16[4,32,512]{2,1,0:T(8,128)(2,1)S(1)}, bf16[4,32,512]{2,1,0:T(8,128)(2,1)S(1)}, u32[]{:S(2)}, u32[]{:S(2)}) collective-permute-start(bf16[4,32,512]{2,1,0:T(8,128)(2,1)S(1)} %shard_map.49.a), channel_id=1, source_target_pairs={{16,0},{49,1},{24,8},{57,9},{32,16},{1,17},{40,24},{9,25},{48,32},... | collective-permute-start | bytes 393224 | tf_op jit(solution)/shard_map/ppermute | solution.py:26
  34.2 2.8 %collective-permute-start.7 = (bf16[1,32,512]{2,1,0:T(8,128)(2,1)}, bf16[1,32,512]{2,1,0:T(8,128)(2,1)S(1)}, u32[]{:S(2)}, u32[]{:S(2)}) collective-permute-start(bf16[1,32,512]{2,1,0:T(8,128)(2,1)} %bitcast.11), channel_id=1, source_target_pairs={{256,0},{769,1},{320,64},{833,65},{384,128},{897,129},{448,192},{9... | collective-permute-start | bytes 98312 | tf_op jit(solution)/shard_map/ppermute | solution.py:26
  37.0 6.0 %collective-permute-done.7.b = bf16[1,32,512]{2,1,0:T(8,128)(2,1)S(1)} collective-permute-done((bf16[1,32,512]{2,1,0:T(8,128)(2,1)}, bf16[1,32,512]{2,1,0:T(8,128)(2,1)S(1)}, u32[]{:S(2)}, u32[]{:S(2)}) %collective-permute-start.7) | collective-permute-done | bytes 32800 | tf_op jit(solution)/shard_map/ppermute | solution.py:26
  42.9 5.2 %collective-permute-start.8 = (bf16[2,32,512]{2,1,0:T(8,128)(2,1)S(1)}, bf16[2,32,512]{2,1,0:T(8,128)(2,1)S(1)}, u32[]{:S(2)}, u32[]{:S(2)}) collective-permute-start(bf16[2,32,512]{2,1,0:T(8,128)(2,1)S(1)} %shard_map.53.a), channel_id=1, source_target_pairs={{32,0},{33,1},{40,8},{41,9},{48,16},{49,17},{56,24},{57,25},{0,32}... | collective-permute-start | bytes 196616 | tf_op jit(solution)/shard_map/ppermute | solution.py:26
  48.2 5.3 %collective-permute-start.3 = (bf16[8,32,512]{2,1,0:T(8,128)(2,1)S(1)}, bf16[8,32,512]{2,1,0:T(8,128)(2,1)S(1)}, u32[]{:S(2)}, u32[]{:S(2)}) collective-permute-start(bf16[8,32,512]{2,1,0:T(8,128)(2,1)S(1)} %shard_map.50.a), channel_id=1, source_target_pairs={{128,0},{897,1},{192,64},{961,65},{256,128},{1,129},{320,192},{65,... | collective-permute-start | bytes 786440 | tf_op jit(solution)/shard_map/ppermute | solution.py:26
  53.5 3.9 %collective-permute-start.9 = (bf16[4,32,512]{2,1,0:T(8,128)(2,1)S(1)}, bf16[4,32,512]{2,1,0:T(8,128)(2,1)S(1)}, u32[]{:S(2)}, u32[]{:S(2)}) collective-permute-start(bf16[4,32,512]{2,1,0:T(8,128)(2,1)S(1)} %shard_map.54.a), channel_id=1, source_target_pairs={{128,0},{897,1},{192,64},{961,65},{256,128},{1,129},{320,192},{65,... | collective-permute-start | bytes 393224 | tf_op jit(solution)/shard_map/ppermute | solution.py:26
  57.4 8.5 %collective-permute-done.9.b = bf16[4,32,512]{2,1,0:T(8,128)(2,1)S(1)} collective-permute-done((bf16[4,32,512]{2,1,0:T(8,128)(2,1)S(1)}, bf16[4,32,512]{2,1,0:T(8,128)(2,1)S(1)}, u32[]{:S(2)}, u32[]{:S(2)}) %collective-permute-start.9) | collective-permute-done | bytes 131104 | tf_op jit(solution)/shard_map/ppermute | solution.py:26
  65.9 3.4 %collective-permute-start.10 = (bf16[8,32,512]{2,1,0:T(8,128)(2,1)S(1)}, bf16[8,32,512]{2,1,0:T(8,128)(2,1)S(1)}, u32[]{:S(2)}, u32[]{:S(2)}) collective-permute-start(bf16[8,32,512]{2,1,0:T(8,128)(2,1)S(1)} %shard_map.55.a), channel_id=1, source_target_pairs={{16,0},{49,1},{24,8},{57,9},{32,16},{1,17},{40,24},{9,25},{48,32},... | collective-permute-start | bytes 786440 | tf_op jit(solution)/shard_map/ppermute | solution.py:26
  69.4 4.2 %collective-permute-start.4 = (bf16[16,32,512]{2,1,0:T(8,128)(2,1)S(1)}, bf16[16,32,512]{2,1,0:T(8,128)(2,1)S(1)}, u32[]{:S(2)}, u32[]{:S(2)}) collective-permute-start(bf16[16,32,512]{2,1,0:T(8,128)(2,1)S(1)} %shard_map.51.u0), channel_id=1, source_target_pairs={{64,0},{961,1},{128,64},{1,65},{192,128},{65,129},{256,192},{129,1... | collective-permute-start | bytes 1572872 | tf_op jit(solution)/shard_map/ppermute | solution.py:26
  73.6 4.1 %collective-permute-done.10.b = bf16[8,32,512]{2,1,0:T(8,128)(2,1)S(1)} collective-permute-done((bf16[8,32,512]{2,1,0:T(8,128)(2,1)S(1)}, bf16[8,32,512]{2,1,0:T(8,128)(2,1)S(1)}, u32[]{:S(2)}, u32[]{:S(2)}) %collective-permute-start.10) | collective-permute-done | bytes 262176 | tf_op jit(solution)/shard_map/ppermute | solution.py:26
  77.7 2.7 %collective-permute-start.12 = (bf16[16,32,512]{2,1,0:T(8,128)(2,1)S(1)}, bf16[16,32,512]{2,1,0:T(8,128)(2,1)S(1)}, u32[]{:S(2)}, u32[]{:S(2)}) collective-permute-start(bf16[16,32,512]{2,1,0:T(8,128)(2,1)S(1)} %shard_map.56.d0), channel_id=1, source_target_pairs={{8,0},{57,1},{16,8},{1,9},{24,16},{9,17},{32,24},{17,25},{40,32},{... | collective-permute-start | bytes 1572872 | tf_op jit(solution)/shard_map/ppermute | solution.py:26
  80.5 1.9 %collective-permute-start.5 = (bf16[16,32,512]{2,1,0:T(8,128)(2,1)S(1)}, bf16[16,32,512]{2,1,0:T(8,128)(2,1)S(1)}, u32[]{:S(2)}, u32[]{:S(2)}) collective-permute-start(bf16[16,32,512]{2,1,0:T(8,128)(2,1)S(1)} %shard_map.51.u0), channel_id=1, source_target_pairs={{8,0},{57,1},{16,8},{1,9},{24,16},{9,17},{32,24},{17,25},{40,32},{... | collective-permute-start | bytes 1572872 | tf_op jit(solution)/shard_map/ppermute | solution.py:26
  82.4 2.5 %collective-permute-start.6 = (bf16[16,32,512]{2,1,0:T(8,128)(2,1)S(1)}, bf16[16,32,512]{2,1,0:T(8,128)(2,1)S(1)}, u32[]{:S(2)}, u32[]{:S(2)}) collective-permute-start(bf16[16,32,512]{2,1,0:T(8,128)(2,1)S(1)} %collective-permute-done.4.uz), channel_id=1, source_target_pairs={{8,0},{57,1},{16,8},{1,9},{24,16},{9,17},{32,24},{17,25},{40,32},{... | collective-permute-start | bytes 1572872 | tf_op jit(solution)/shard_map/ppermute | solution.py:26
  84.9 4.6 %collective-permute-start.11 = (bf16[16,32,512]{2,1,0:T(8,128)(2,1)S(1)}, bf16[16,32,512]{2,1,0:T(8,128)(2,1)S(1)}, u32[]{:S(2)}, u32[]{:S(2)}) collective-permute-start(bf16[16,32,512]{2,1,0:T(8,128)(2,1)S(1)} %shard_map.56.d0), channel_id=1, source_target_pairs={{64,0},{961,1},{128,64},{1,65},{192,128},{65,129},{256,192},{129,1... | collective-permute-start | bytes 1572872 | tf_op jit(solution)/shard_map/ppermute | solution.py:26
  89.5 1.9 %collective-permute-start.13 = (bf16[16,32,512]{2,1,0:T(8,128)(2,1)S(1)}, bf16[16,32,512]{2,1,0:T(8,128)(2,1)S(1)}, u32[]{:S(2)}, u32[]{:S(2)}) collective-permute-start(bf16[16,32,512]{2,1,0:T(8,128)(2,1)S(1)} %collective-permute-done.12.dy), channel_id=1, source_target_pairs={{64,0},{961,1},{128,64},{1,65},{192,128},{65,129},{256,192},{129,1... | collective-permute-start | bytes 1572872 | tf_op jit(solution)/shard_map/ppermute | solution.py:26
  91.5 2.1 %shard_map.46.normed = bf16[512,2048]{1,0:T(8,128)(2,1)S(1)} custom-call(bf16[512,2048]{1,0:T(8,128)(2,1)S(1)} %copy-done, f32[1,2048]{1,0:T(1,128)S(1)} %bitcast.13), custom_call_target="tpu_custom_call" | custom-call | flops 16777216 | bytes 1048576 | tf_op jit(solution)/shard_map/pallas_call | solution.py:225
  93.6 0.9 collective-permute-done.5.uy
  94.5 5.6 %collective-permute-done.6.uzy = bf16[16,32,512]{2,1,0:T(8,128)(2,1)S(1)} collective-permute-done((bf16[16,32,512]{2,1,0:T(8,128)(2,1)S(1)}, bf16[16,32,512]{2,1,0:T(8,128)(2,1)S(1)}, u32[]{:S(2)}, u32[]{:S(2)}) %collective-permute-start.6) | collective-permute-done | bytes 524320 | tf_op jit(solution)/shard_map/ppermute | solution.py:26
  100.1 2.2 %shard_map.52.hidden = bf16[512,512]{1,0:T(8,128)(2,1)S(1)} custom-call(s32[4]{0:T(128)S(1)} %pad_add_fusion.where, bf16[512,2048]{1,0:T(8,128)(2,1)S(1)} %shard_map.46.normed, bf16[16,32,512]{2,1,0:T(8,128)(2,1)S(1)} %shard_map.51.u0, bf16[16,32,512]{2,1,0:T(8,128)(2,1)S(1)} %collective-permute-done.4.uz, ...), custom_call_target="tpu_custom_call" | custom-call | flops 1073741824 | bytes 1048576 | tf_op jit(solution)/shard_map/pallas_call | solution.py:229
  102.3 2.8 %shard_map.57 = (bf16[2,256,1024]{2,1,0:T(8,128)(2,1)S(1)}, bf16[2,256,1024]{2,1,0:T(8,128)(2,1)S(1)}) custom-call(s32[4]{0:T(128)S(1)} %pad_add_fusion.where, bf16[512,512]{1,0:T(8,128)(2,1)S(1)} %shard_map.52.hidden, bf16[16,32,512]{2,1,0:T(8,128)(2,1)S(1)} %shard_map.56.d0, bf16[16,32,512]{2,1,0:T(8,128)(2,1)S(1)} %collective-permute-done.12.dy), custom_call_target="tpu_custom_call" | custom-call | flops 536870912 | bytes 1048576 | tf_op jit(solution)/shard_map/pallas_call | solution.py:233
  105.1 1.7 %shard_map.58 = (bf16[2,256,1024]{2,1,0:T(8,128)(2,1)S(1)}, bf16[1024,512]{1,0:T(8,128)(2,1)S(1)}) custom-call(s32[4]{0:T(128)S(1)} %pad_add_fusion.where, bf16[512,512]{1,0:T(8,128)(2,1)S(1)} %shard_map.52.hidden, bf16[16,32,512]{2,1,0:T(8,128)(2,1)S(1)} %collective-permute-done.11.dz, ...), custom_call_target="tpu_custom_call", output_to_operand_aliasing={{0}: (4, {})} | custom-call | flops 268435456 | bytes 1048576 | tf_op jit(solution)/shard_map/pallas_call | solution.py:236
  106.8 6.2 %collective-permute-start.14 = (bf16[2,256,1024]{2,1,0:T(8,128)(2,1)S(1)}, bf16[2,256,1024]{2,1,0:T(8,128)(2,1)S(1)}, u32[]{:S(2)}, u32[]{:S(2)}) collective-permute-start(bf16[2,256,1024]{2,1,0:T(8,128)(2,1)S(1)} %get-tuple-element.18), channel_id=1, source_target_pairs={{0,1},{1,0},{2,3},{3,2},{4,5},{5,4},{6,7},{7,6},{8,9},{9,8},{10,11... | collective-permute-start | bytes 3145736 | tf_op jit(solution)/shard_map/ppermute | solution.py:243
  113.0 1.1 shard_map.59.own
  114.1 1.2 collective-permute-done.14.beside
  116.1 4.4 %collective-permute-start.15 = (bf16[2,2,64,1024]{3,2,1,0:T(8,128)(2,1)S(1)}, bf16[2,2,64,1024]{3,2,1,0:T(8,128)(2,1)S(1)}, u32[]{:S(2)}, u32[]{:S(2)}) collective-permute-start(bf16[2,2,64,1024]{3,2,1,0:T(8,128)(2,1)S(1)} %get-tuple-element.20), channel_id=1, source_target_pairs={{0,2},{1,7},{2,0},{3,5},{4,6},{5,3},{6,4},{7,1},{8,10},{9,15},{10,... | collective-permute-start | bytes 1572872 | tf_op jit(solution)/shard_map/ppermute | solution.py:34
  120.5 6.7 %collective-permute-done.15.came = bf16[2,2,64,1024]{3,2,1,0:T(8,128)(2,1)S(1)} collective-permute-done((bf16[2,2,64,1024]{3,2,1,0:T(8,128)(2,1)S(1)}, bf16[2,2,64,1024]{3,2,1,0:T(8,128)(2,1)S(1)}, u32[]{:S(2)}, u32[]{:S(2)}) %collective-permute-start.15) | collective-permute-done | bytes 524320 | tf_op jit(solution)/shard_map/ppermute | solution.py:34
  127.3 2.2 %collective-permute-start.16 = (bf16[2,64,1024]{2,1,0:T(8,128)(2,1)S(1)}, bf16[2,64,1024]{2,1,0:T(8,128)(2,1)}, u32[]{:S(2)}, u32[]{:S(2)}) collective-permute-start(bf16[2,64,1024]{2,1,0:T(8,128)(2,1)S(1)} %shard_map.61), channel_id=1, source_target_pairs={{0,6},{1,3},{2,4},{3,1},{4,2},{5,7},{6,0},{7,5},{8,14},{9,11},{10,... | collective-permute-start | bytes 786440 | tf_op jit(solution)/shard_map/ppermute | solution.py:34
  129.5 5.3 %collective-permute-done.16.late = bf16[2,64,1024]{2,1,0:T(8,128)(2,1)} collective-permute-done((bf16[2,64,1024]{2,1,0:T(8,128)(2,1)S(1)}, bf16[2,64,1024]{2,1,0:T(8,128)(2,1)}, u32[]{:S(2)}, u32[]{:S(2)}) %collective-permute-start.16) | collective-permute-done | bytes 262176 | tf_op jit(solution)/shard_map/ppermute | solution.py:34
  134.8 1.8 %shard_map.62 = bf16[64,2048]{1,0:T(8,128)(2,1)} custom-call(s32[4]{0:T(128)S(1)} %pad_add_fusion.where, bf16[64,2048]{1,0:T(8,128)(2,1)S(1)} %constant_dynamic-slice_fusion.residual, bf16[2,2,64,1024]{3,2,1,0:T(8,128)(2,1)S(1)} %get-tuple-element.19.keep, bf16[2,2,64,1024]{3,2,1,0:T(8,128)(2,1)S(1)} %collective-permute-done.15.came, ...), custom_call_target="tpu_custom_call" | custom-call | tf_op jit(solution)/shard_map/pallas_call | solution.py:214
  (29 shorter events, 3.2 us)
Async XLA Ops:
  0.0 91.4 %copy-start = (bf16[512,2048]{1,0:T(8,128)(2,1)S(1)}, bf16[512,2048]{1,0:T(8,128)(2,1)}, u32[]{:S(2)}) copy-start(bf16[512,2048]{1,0:T(8,128)(2,1)} %tokens.1) | copy-start | bytes 6291460
  0.0 10.6 %collective-permute-start = (bf16[1,32,512]{2,1,0:T(8,128)(2,1)}, bf16[1,32,512]{2,1,0:T(8,128)(2,1)S(1)}, u32[]{:S(2)}, u32[]{:S(2)}) collective-permute-start(bf16[1,32,512]{2,1,0:T(8,128)(2,1)} %bitcast.9), channel_id=1, source_target_pairs={{32,0},{33,1},{40,8},{41,9},{48,16},{49,17},{56,24},{57,25},{0,32}... | collective-permute-start | bytes 98312 | tf_op jit(solution)/shard_map/ppermute | solution.py:26
  8.5 0.8 copy-start.1
  9.2 0.8 copy-start.2
  10.0 81.4 %copy-start.3 = (f32[2048]{0:T(1024)S(1)}, f32[2048]{0:T(1024)}, u32[]{:S(2)}) copy-start(f32[2048]{0:T(1024)} %param.5) | copy-start | bytes 24580
  10.6 19.8 %collective-permute-start.1 = (bf16[2,32,512]{2,1,0:T(8,128)(2,1)S(1)}, bf16[2,32,512]{2,1,0:T(8,128)(2,1)S(1)}, u32[]{:S(2)}, u32[]{:S(2)}) collective-permute-start(bf16[2,32,512]{2,1,0:T(8,128)(2,1)S(1)} %shard_map.48.a), channel_id=1, source_target_pairs={{256,0},{769,1},{320,64},{833,65},{384,128},{897,129},{448,192},{9... | collective-permute-start | bytes 196616 | tf_op jit(solution)/shard_map/ppermute | solution.py:26
  30.4 17.8 %collective-permute-start.2 = (bf16[4,32,512]{2,1,0:T(8,128)(2,1)S(1)}, bf16[4,32,512]{2,1,0:T(8,128)(2,1)S(1)}, u32[]{:S(2)}, u32[]{:S(2)}) collective-permute-start(bf16[4,32,512]{2,1,0:T(8,128)(2,1)S(1)} %shard_map.49.a), channel_id=1, source_target_pairs={{16,0},{49,1},{24,8},{57,9},{32,16},{1,17},{40,24},{9,25},{48,32},... | collective-permute-start | bytes 393224 | tf_op jit(solution)/shard_map/ppermute | solution.py:26
  34.2 8.8 %collective-permute-start.7 = (bf16[1,32,512]{2,1,0:T(8,128)(2,1)}, bf16[1,32,512]{2,1,0:T(8,128)(2,1)S(1)}, u32[]{:S(2)}, u32[]{:S(2)}) collective-permute-start(bf16[1,32,512]{2,1,0:T(8,128)(2,1)} %bitcast.11), channel_id=1, source_target_pairs={{256,0},{769,1},{320,64},{833,65},{384,128},{897,129},{448,192},{9... | collective-permute-start | bytes 98312 | tf_op jit(solution)/shard_map/ppermute | solution.py:26
  42.9 10.5 %collective-permute-start.8 = (bf16[2,32,512]{2,1,0:T(8,128)(2,1)S(1)}, bf16[2,32,512]{2,1,0:T(8,128)(2,1)S(1)}, u32[]{:S(2)}, u32[]{:S(2)}) collective-permute-start(bf16[2,32,512]{2,1,0:T(8,128)(2,1)S(1)} %shard_map.53.a), channel_id=1, source_target_pairs={{32,0},{33,1},{40,8},{41,9},{48,16},{49,17},{56,24},{57,25},{0,32}... | collective-permute-start | bytes 196616 | tf_op jit(solution)/shard_map/ppermute | solution.py:26
  48.2 21.1 %collective-permute-start.3 = (bf16[8,32,512]{2,1,0:T(8,128)(2,1)S(1)}, bf16[8,32,512]{2,1,0:T(8,128)(2,1)S(1)}, u32[]{:S(2)}, u32[]{:S(2)}) collective-permute-start(bf16[8,32,512]{2,1,0:T(8,128)(2,1)S(1)} %shard_map.50.a), channel_id=1, source_target_pairs={{128,0},{897,1},{192,64},{961,65},{256,128},{1,129},{320,192},{65,... | collective-permute-start | bytes 786440 | tf_op jit(solution)/shard_map/ppermute | solution.py:26
  53.5 12.4 %collective-permute-start.9 = (bf16[4,32,512]{2,1,0:T(8,128)(2,1)S(1)}, bf16[4,32,512]{2,1,0:T(8,128)(2,1)S(1)}, u32[]{:S(2)}, u32[]{:S(2)}) collective-permute-start(bf16[4,32,512]{2,1,0:T(8,128)(2,1)S(1)} %shard_map.54.a), channel_id=1, source_target_pairs={{128,0},{897,1},{192,64},{961,65},{256,128},{1,129},{320,192},{65,... | collective-permute-start | bytes 393224 | tf_op jit(solution)/shard_map/ppermute | solution.py:26
  65.9 11.8 %collective-permute-start.10 = (bf16[8,32,512]{2,1,0:T(8,128)(2,1)S(1)}, bf16[8,32,512]{2,1,0:T(8,128)(2,1)S(1)}, u32[]{:S(2)}, u32[]{:S(2)}) collective-permute-start(bf16[8,32,512]{2,1,0:T(8,128)(2,1)S(1)} %shard_map.55.a), channel_id=1, source_target_pairs={{16,0},{49,1},{24,8},{57,9},{32,16},{1,17},{40,24},{9,25},{48,32},... | collective-permute-start | bytes 786440 | tf_op jit(solution)/shard_map/ppermute | solution.py:26
  69.4 13.0 %collective-permute-start.4 = (bf16[16,32,512]{2,1,0:T(8,128)(2,1)S(1)}, bf16[16,32,512]{2,1,0:T(8,128)(2,1)S(1)}, u32[]{:S(2)}, u32[]{:S(2)}) collective-permute-start(bf16[16,32,512]{2,1,0:T(8,128)(2,1)S(1)} %shard_map.51.u0), channel_id=1, source_target_pairs={{64,0},{961,1},{128,64},{1,65},{192,128},{65,129},{256,192},{129,1... | collective-permute-start | bytes 1572872 | tf_op jit(solution)/shard_map/ppermute | solution.py:26
  77.7 11.8 %collective-permute-start.12 = (bf16[16,32,512]{2,1,0:T(8,128)(2,1)S(1)}, bf16[16,32,512]{2,1,0:T(8,128)(2,1)S(1)}, u32[]{:S(2)}, u32[]{:S(2)}) collective-permute-start(bf16[16,32,512]{2,1,0:T(8,128)(2,1)S(1)} %shard_map.56.d0), channel_id=1, source_target_pairs={{8,0},{57,1},{16,8},{1,9},{24,16},{9,17},{32,24},{17,25},{40,32},{... | collective-permute-start | bytes 1572872 | tf_op jit(solution)/shard_map/ppermute | solution.py:26
  80.5 14.0 %collective-permute-start.5 = (bf16[16,32,512]{2,1,0:T(8,128)(2,1)S(1)}, bf16[16,32,512]{2,1,0:T(8,128)(2,1)S(1)}, u32[]{:S(2)}, u32[]{:S(2)}) collective-permute-start(bf16[16,32,512]{2,1,0:T(8,128)(2,1)S(1)} %shard_map.51.u0), channel_id=1, source_target_pairs={{8,0},{57,1},{16,8},{1,9},{24,16},{9,17},{32,24},{17,25},{40,32},{... | collective-permute-start | bytes 1572872 | tf_op jit(solution)/shard_map/ppermute | solution.py:26
  82.4 17.7 %collective-permute-start.6 = (bf16[16,32,512]{2,1,0:T(8,128)(2,1)S(1)}, bf16[16,32,512]{2,1,0:T(8,128)(2,1)S(1)}, u32[]{:S(2)}, u32[]{:S(2)}) collective-permute-start(bf16[16,32,512]{2,1,0:T(8,128)(2,1)S(1)} %collective-permute-done.4.uz), channel_id=1, source_target_pairs={{8,0},{57,1},{16,8},{1,9},{24,16},{9,17},{32,24},{17,25},{40,32},{... | collective-permute-start | bytes 1572872 | tf_op jit(solution)/shard_map/ppermute | solution.py:26
  84.9 20.1 %collective-permute-start.11 = (bf16[16,32,512]{2,1,0:T(8,128)(2,1)S(1)}, bf16[16,32,512]{2,1,0:T(8,128)(2,1)S(1)}, u32[]{:S(2)}, u32[]{:S(2)}) collective-permute-start(bf16[16,32,512]{2,1,0:T(8,128)(2,1)S(1)} %shard_map.56.d0), channel_id=1, source_target_pairs={{64,0},{961,1},{128,64},{1,65},{192,128},{65,129},{256,192},{129,1... | collective-permute-start | bytes 1572872 | tf_op jit(solution)/shard_map/ppermute | solution.py:26
  89.5 15.5 %collective-permute-start.13 = (bf16[16,32,512]{2,1,0:T(8,128)(2,1)S(1)}, bf16[16,32,512]{2,1,0:T(8,128)(2,1)S(1)}, u32[]{:S(2)}, u32[]{:S(2)}) collective-permute-start(bf16[16,32,512]{2,1,0:T(8,128)(2,1)S(1)} %collective-permute-done.12.dy), channel_id=1, source_target_pairs={{64,0},{961,1},{128,64},{1,65},{192,128},{65,129},{256,192},{129,1... | collective-permute-start | bytes 1572872 | tf_op jit(solution)/shard_map/ppermute | solution.py:26
  106.8 8.5 %collective-permute-start.14 = (bf16[2,256,1024]{2,1,0:T(8,128)(2,1)S(1)}, bf16[2,256,1024]{2,1,0:T(8,128)(2,1)S(1)}, u32[]{:S(2)}, u32[]{:S(2)}) collective-permute-start(bf16[2,256,1024]{2,1,0:T(8,128)(2,1)S(1)} %get-tuple-element.18), channel_id=1, source_target_pairs={{0,1},{1,0},{2,3},{3,2},{4,5},{5,4},{6,7},{7,6},{8,9},{9,8},{10,11... | collective-permute-start | bytes 3145736 | tf_op jit(solution)/shard_map/ppermute | solution.py:243
  116.1 11.1 %collective-permute-start.15 = (bf16[2,2,64,1024]{3,2,1,0:T(8,128)(2,1)S(1)}, bf16[2,2,64,1024]{3,2,1,0:T(8,128)(2,1)S(1)}, u32[]{:S(2)}, u32[]{:S(2)}) collective-permute-start(bf16[2,2,64,1024]{3,2,1,0:T(8,128)(2,1)S(1)} %get-tuple-element.20), channel_id=1, source_target_pairs={{0,2},{1,7},{2,0},{3,5},{4,6},{5,3},{6,4},{7,1},{8,10},{9,15},{10,... | collective-permute-start | bytes 1572872 | tf_op jit(solution)/shard_map/ppermute | solution.py:34
  127.3 7.5 %collective-permute-start.16 = (bf16[2,64,1024]{2,1,0:T(8,128)(2,1)S(1)}, bf16[2,64,1024]{2,1,0:T(8,128)(2,1)}, u32[]{:S(2)}, u32[]{:S(2)}) collective-permute-start(bf16[2,64,1024]{2,1,0:T(8,128)(2,1)S(1)} %shard_map.61), channel_id=1, source_target_pairs={{0,6},{1,3},{2,4},{3,1},{4,2},{5,7},{6,0},{7,5},{8,14},{9,11},{10,... | collective-permute-start | bytes 786440 | tf_op jit(solution)/shard_map/ppermute | solution.py:34

commit v4 on v3

--- a/solution.py
+++ b/solution.py
@@ -84,7 +84,10 @@
     down_out[...] = down[...]
 
 
-def norm_kernel(tokens, gain, normed):
+def norm_kernel(where, tokens, gain, normed, residual):
+    mine = where[3] * CORE + where[2]
+    residual[...] = tokens[pl.ds(pl.multiple_of(mine * 64, 64), 64), :]
+
     @pl.loop(0, 16)
     def _(n):
         rows = pl.ds(pl.multiple_of(n * 32, 32), 32)
@@ -136,11 +139,10 @@
             hidden[rows, columns] = active[j * 64 : (j + 1) * 64]
 
 
-def early_kernel(where, hidden, d0, dy, theirs, own, down):
+def early_kernel(where, hidden, d0, dy, theirs, down):
     place(where, d0, offsets(DOWN_STEPS), down, True)
     place(where, dy, shifted(DOWN_STEPS, 0, 1), down, True)
     down_product(hidden, THEIRS, down, theirs, 0)
-    down_product(hidden, OWN, down, own, 0)
 
 
 def late_kernel(where, hidden, dz, dyz, theirs_in, theirs, down):
@@ -149,8 +151,9 @@
     down_product(hidden, THEIRS, down, theirs, 1)
 
 
-def own_kernel(hidden, down, own_in, own):
-    down_product(hidden, OWN, down, own, 1)
+def own_kernel(hidden, first, second, own):
+    down_product(hidden, OWN, first, own, 0)
+    down_product(hidden, OWN, second, own, 1)
 
 
 def add_kernel(where, own, beside, keep, send):
@@ -222,18 +225,17 @@
         jnp.int32
     )
     up, down = gathered(where, up_weight[None], down_weight.T[None])
-    normed = kernel_call(
-        norm_kernel, bf16(512, 2048), 2, smem=False, mib=12, flops=2**24
-    )(tokens, norm_gain[None])
-    residual = lax.dynamic_slice_in_dim(tokens, (x * CORE + core) * 64, 64, 0)
+    normed, residual = kernel_call(
+        norm_kernel, (bf16(512, 2048), bf16(64, 2048)), 2, mib=12, flops=2**24
+    )(where, tokens, norm_gain[None])
     hidden = kernel_call(
         up_kernel, bf16(512, 512), 5, scratch=((2048, 512),), mib=12, flops=2**30
     )(where, normed, *up)
     out = bf16(2, 256, 1024)
-    theirs, own = kernel_call(
-        early_kernel, (out, out), 3, scratch=((1024, 512),), flops=2**29
+    theirs, first = kernel_call(
+        early_kernel, (out, bf16(1024, 512)), 3, flops=2**28
     )(where, hidden, *down[:2])
-    theirs, rest = kernel_call(
+    theirs, second = kernel_call(
         late_kernel,
         (out, bf16(1024, 512)),
         4,
@@ -241,14 +243,9 @@
         input_output_aliases={4: 0},
     )(where, hidden, *down[2:], theirs)
     beside = lax.ppermute(theirs, "core", [(0, 1), (1, 0)])
-    own = kernel_call(
-        own_kernel,
-        out,
-        3,
-        smem=False,
-        flops=2**28,
-        input_output_aliases={2: 0},
-    )(hidden, rest, own)
+    own = kernel_call(own_kernel, out, 3, smem=False, flops=2**29)(
+        hidden, first, second
+    )
     return over_tp(where, beside, own, residual)
 
 

time: 139 us -> 138 us (level)
  waiting for transfers between devices: 47.5 us -> 40.4 us
  starting transfers between devices: 74 us -> 80.5 us
    ppermute x14, waiting for transfers between devices: 34.3 us -> 28.3 us  [from_side(): return lax.ppermute(array, names, pairs)]
    ppermute x14, starting transfers between devices: 61.2 us -> 65.3 us  [from_side(): return lax.ppermute(array, names, pairs)]
    ppermute x1, starting transfers between devices: 6.24 us -> 8.59 us  [shards(): beside = lax.ppermute(theirs, 'core', [(0, 1), (1, 0)])]
  transfers between devices with their start and end apart: 17 -> 17, of which waited for: 9 -> 10; matrix products, arithmetic and copies ran while one was open for 0% -> 0% of each run, Pallas kernels for 6% -> 7%
where the time goes in v4:
time: 138 us; the launch traced here: 136 us
  starting transfers between devices  80.5 us (58%)
  waiting for transfers between devices  40.4 us (29%)
  Pallas kernels  13.3 us (10%)
  local copies, waits for them, and re-layouts  1.52 us (1%)
    ppermute x14, starting transfers between devices, from_side(): return lax.ppermute(array, names, pairs)  65.3 us
    ppermute x14, waiting for transfers between devices, from_side(): return lax.ppermute(array, names, pairs)  28.3 us
    ppermute x2, waiting for transfers between devices, between_x(): return lax.ppermute(array, ('x', 'core'), pairs)  11.9 us
    ppermute x1, starting transfers between devices, shards(): beside = lax.ppermute(theirs, 'core', [(0, 1), (1, 0)])  8.59 us
    ppermute x2, starting transfers between devices, between_x(): return lax.ppermute(array, ('x', 'core'), pairs)  6.6 us
  transfers between devices with their start and end apart: 17, of which 10 were waited for; matrix products, arithmetic and copies ran while one was open for 0% of the time, Pallas kernels for 7%

profile of v4, /device:TPU:1, one launch (start us, length us, event | category | flops | bytes accessed | tf_op | source)
XLA Modules:
  0.0 136.1 jit_solution(5555371882565126135)
XLA Ops:
  0.0 8.4 %collective-permute-start = (bf16[1,32,512]{2,1,0:T(8,128)(2,1)}, bf16[1,32,512]{2,1,0:T(8,128)(2,1)S(1)}, u32[]{:S(2)}, u32[]{:S(2)}) collective-permute-start(bf16[1,32,512]{2,1,0:T(8,128)(2,1)} %bitcast.9), channel_id=1, source_target_pairs={{32,0},{33,1},{40,8},{41,9},{48,16},{49,17},{56,24},{57,25},{0,32}... | collective-permute-start | bytes 98312 | tf_op jit(solution)/shard_map/ppermute | solution.py:26
  10.6 10.6 %collective-permute-start.1 = (bf16[2,32,512]{2,1,0:T(8,128)(2,1)S(1)}, bf16[2,32,512]{2,1,0:T(8,128)(2,1)S(1)}, u32[]{:S(2)}, u32[]{:S(2)}) collective-permute-start(bf16[2,32,512]{2,1,0:T(8,128)(2,1)S(1)} %shard_map.48.a), channel_id=1, source_target_pairs={{256,0},{769,1},{320,64},{833,65},{384,128},{897,129},{448,192},{9... | collective-permute-start | bytes 196616 | tf_op jit(solution)/shard_map/ppermute | solution.py:26
  21.2 9.2 %collective-permute-done.1.b = bf16[2,32,512]{2,1,0:T(8,128)(2,1)S(1)} collective-permute-done((bf16[2,32,512]{2,1,0:T(8,128)(2,1)S(1)}, bf16[2,32,512]{2,1,0:T(8,128)(2,1)S(1)}, u32[]{:S(2)}, u32[]{:S(2)}) %collective-permute-start.1) | collective-permute-done | bytes 65568 | tf_op jit(solution)/shard_map/ppermute | solution.py:26
  30.4 3.8 %collective-permute-start.2 = (bf16[4,32,512]{2,1,0:T(8,128)(2,1)S(1)}, bf16[4,32,512]{2,1,0:T(8,128)(2,1)S(1)}, u32[]{:S(2)}, u32[]{:S(2)}) collective-permute-start(bf16[4,32,512]{2,1,0:T(8,128)(2,1)S(1)} %shard_map.49.a), channel_id=1, source_target_pairs={{16,0},{49,1},{24,8},{57,9},{32,16},{1,17},{40,24},{9,25},{48,32},... | collective-permute-start | bytes 393224 | tf_op jit(solution)/shard_map/ppermute | solution.py:26
  34.2 2.8 %collective-permute-start.7 = (bf16[1,32,512]{2,1,0:T(8,128)(2,1)}, bf16[1,32,512]{2,1,0:T(8,128)(2,1)S(1)}, u32[]{:S(2)}, u32[]{:S(2)}) collective-permute-start(bf16[1,32,512]{2,1,0:T(8,128)(2,1)} %bitcast.11), channel_id=1, source_target_pairs={{256,0},{769,1},{320,64},{833,65},{384,128},{897,129},{448,192},{9... | collective-permute-start | bytes 98312 | tf_op jit(solution)/shard_map/ppermute | solution.py:26
  37.0 6.0 %collective-permute-done.7.b = bf16[1,32,512]{2,1,0:T(8,128)(2,1)S(1)} collective-permute-done((bf16[1,32,512]{2,1,0:T(8,128)(2,1)}, bf16[1,32,512]{2,1,0:T(8,128)(2,1)S(1)}, u32[]{:S(2)}, u32[]{:S(2)}) %collective-permute-start.7) | collective-permute-done | bytes 32800 | tf_op jit(solution)/shard_map/ppermute | solution.py:26
  42.9 5.2 %collective-permute-start.8 = (bf16[2,32,512]{2,1,0:T(8,128)(2,1)S(1)}, bf16[2,32,512]{2,1,0:T(8,128)(2,1)S(1)}, u32[]{:S(2)}, u32[]{:S(2)}) collective-permute-start(bf16[2,32,512]{2,1,0:T(8,128)(2,1)S(1)} %shard_map.53.a), channel_id=1, source_target_pairs={{32,0},{33,1},{40,8},{41,9},{48,16},{49,17},{56,24},{57,25},{0,32}... | collective-permute-start | bytes 196616 | tf_op jit(solution)/shard_map/ppermute | solution.py:26
  48.2 3.7 %collective-permute-done.8.b = bf16[2,32,512]{2,1,0:T(8,128)(2,1)S(1)} collective-permute-done((bf16[2,32,512]{2,1,0:T(8,128)(2,1)S(1)}, bf16[2,32,512]{2,1,0:T(8,128)(2,1)S(1)}, u32[]{:S(2)}, u32[]{:S(2)}) %collective-permute-start.8) | collective-permute-done | bytes 65568 | tf_op jit(solution)/shard_map/ppermute | solution.py:26
  51.9 5.5 %collective-permute-start.9 = (bf16[4,32,512]{2,1,0:T(8,128)(2,1)S(1)}, bf16[4,32,512]{2,1,0:T(8,128)(2,1)S(1)}, u32[]{:S(2)}, u32[]{:S(2)}) collective-permute-start(bf16[4,32,512]{2,1,0:T(8,128)(2,1)S(1)} %shard_map.54.a), channel_id=1, source_target_pairs={{128,0},{897,1},{192,64},{961,65},{256,128},{1,129},{320,192},{65,... | collective-permute-start | bytes 393224 | tf_op jit(solution)/shard_map/ppermute | solution.py:26
  57.5 1.9 %collective-permute-start.3 = (bf16[8,32,512]{2,1,0:T(8,128)(2,1)S(1)}, bf16[8,32,512]{2,1,0:T(8,128)(2,1)S(1)}, u32[]{:S(2)}, u32[]{:S(2)}) collective-permute-start(bf16[8,32,512]{2,1,0:T(8,128)(2,1)S(1)} %shard_map.50.a), channel_id=1, source_target_pairs={{128,0},{897,1},{192,64},{961,65},{256,128},{1,129},{320,192},{65,... | collective-permute-start | bytes 786440 | tf_op jit(solution)/shard_map/ppermute | solution.py:26
  59.4 3.7 %collective-permute-done.9.b = bf16[4,32,512]{2,1,0:T(8,128)(2,1)S(1)} collective-permute-done((bf16[4,32,512]{2,1,0:T(8,128)(2,1)S(1)}, bf16[4,32,512]{2,1,0:T(8,128)(2,1)S(1)}, u32[]{:S(2)}, u32[]{:S(2)}) %collective-permute-start.9) | collective-permute-done | bytes 131104 | tf_op jit(solution)/shard_map/ppermute | solution.py:26
  63.2 5.2 %collective-permute-start.10 = (bf16[8,32,512]{2,1,0:T(8,128)(2,1)S(1)}, bf16[8,32,512]{2,1,0:T(8,128)(2,1)S(1)}, u32[]{:S(2)}, u32[]{:S(2)}) collective-permute-start(bf16[8,32,512]{2,1,0:T(8,128)(2,1)S(1)} %shard_map.55.a), channel_id=1, source_target_pairs={{16,0},{49,1},{24,8},{57,9},{32,16},{1,17},{40,24},{9,25},{48,32},... | collective-permute-start | bytes 786440 | tf_op jit(solution)/shard_map/ppermute | solution.py:26
  68.4 5.2 %collective-permute-start.4 = (bf16[16,32,512]{2,1,0:T(8,128)(2,1)S(1)}, bf16[16,32,512]{2,1,0:T(8,128)(2,1)S(1)}, u32[]{:S(2)}, u32[]{:S(2)}) collective-permute-start(bf16[16,32,512]{2,1,0:T(8,128)(2,1)S(1)} %shard_map.51.u0), channel_id=1, source_target_pairs={{64,0},{961,1},{128,64},{1,65},{192,128},{65,129},{256,192},{129,1... | collective-permute-start | bytes 1572872 | tf_op jit(solution)/shard_map/ppermute | solution.py:26
  73.7 4.0 %collective-permute-start.11 = (bf16[16,32,512]{2,1,0:T(8,128)(2,1)S(1)}, bf16[16,32,512]{2,1,0:T(8,128)(2,1)S(1)}, u32[]{:S(2)}, u32[]{:S(2)}) collective-permute-start(bf16[16,32,512]{2,1,0:T(8,128)(2,1)S(1)} %shard_map.56.d0), channel_id=1, source_target_pairs={{8,0},{57,1},{16,8},{1,9},{24,16},{9,17},{32,24},{17,25},{40,32},{... | collective-permute-start | bytes 1572872 | tf_op jit(solution)/shard_map/ppermute | solution.py:26
  77.7 3.0 %collective-permute-start.5 = (bf16[16,32,512]{2,1,0:T(8,128)(2,1)S(1)}, bf16[16,32,512]{2,1,0:T(8,128)(2,1)S(1)}, u32[]{:S(2)}, u32[]{:S(2)}) collective-permute-start(bf16[16,32,512]{2,1,0:T(8,128)(2,1)S(1)} %shard_map.51.u0), channel_id=1, source_target_pairs={{8,0},{57,1},{16,8},{1,9},{24,16},{9,17},{32,24},{17,25},{40,32},{... | collective-permute-start | bytes 1572872 | tf_op jit(solution)/shard_map/ppermute | solution.py:26
  81.1 3.2 %collective-permute-start.6 = (bf16[16,32,512]{2,1,0:T(8,128)(2,1)S(1)}, bf16[16,32,512]{2,1,0:T(8,128)(2,1)S(1)}, u32[]{:S(2)}, u32[]{:S(2)}) collective-permute-start(bf16[16,32,512]{2,1,0:T(8,128)(2,1)S(1)} %collective-permute-done.4.uz), channel_id=1, source_target_pairs={{8,0},{57,1},{16,8},{1,9},{24,16},{9,17},{32,24},{17,25},{40,32},{... | collective-permute-start | bytes 1572872 | tf_op jit(solution)/shard_map/ppermute | solution.py:26
  84.3 4.5 %collective-permute-start.12 = (bf16[16,32,512]{2,1,0:T(8,128)(2,1)S(1)}, bf16[16,32,512]{2,1,0:T(8,128)(2,1)S(1)}, u32[]{:S(2)}, u32[]{:S(2)}) collective-permute-start(bf16[16,32,512]{2,1,0:T(8,128)(2,1)S(1)} %shard_map.56.d0), channel_id=1, source_target_pairs={{64,0},{961,1},{128,64},{1,65},{192,128},{65,129},{256,192},{129,1... | collective-permute-start | bytes 1572872 | tf_op jit(solution)/shard_map/ppermute | solution.py:26
  88.8 1.9 %collective-permute-start.13 = (bf16[16,32,512]{2,1,0:T(8,128)(2,1)S(1)}, bf16[16,32,512]{2,1,0:T(8,128)(2,1)S(1)}, u32[]{:S(2)}, u32[]{:S(2)}) collective-permute-start(bf16[16,32,512]{2,1,0:T(8,128)(2,1)S(1)} %collective-permute-done.11.dy), channel_id=1, source_target_pairs={{64,0},{961,1},{128,64},{1,65},{192,128},{65,129},{256,192},{129,1... | collective-permute-start | bytes 1572872 | tf_op jit(solution)/shard_map/ppermute | solution.py:26
  90.8 2.7 %shard_map.46 = (bf16[512,2048]{1,0:T(8,128)(2,1)S(1)}, bf16[64,2048]{1,0:T(8,128)(2,1)S(1)}) custom-call(s32[4]{0:T(128)S(1)} %pad_add_fusion.where, bf16[512,2048]{1,0:T(8,128)(2,1)S(1)} %copy-done, f32[1,2048]{1,0:T(1,128)S(1)} %bitcast.13), custom_call_target="tpu_custom_call" | custom-call | flops 16777216 | bytes 1048576 | tf_op jit(solution)/shard_map/pallas_call | solution.py:228
  93.5 2.6 %collective-permute-done.6.uzy = bf16[16,32,512]{2,1,0:T(8,128)(2,1)S(1)} collective-permute-done((bf16[16,32,512]{2,1,0:T(8,128)(2,1)S(1)}, bf16[16,32,512]{2,1,0:T(8,128)(2,1)S(1)}, u32[]{:S(2)}, u32[]{:S(2)}) %collective-permute-start.6) | collective-permute-done | bytes 524320 | tf_op jit(solution)/shard_map/ppermute | solution.py:26
  96.1 2.2 %shard_map.52.hidden = bf16[512,512]{1,0:T(8,128)(2,1)S(1)} custom-call(s32[4]{0:T(128)S(1)} %pad_add_fusion.where, bf16[512,2048]{1,0:T(8,128)(2,1)S(1)} %get-tuple-element.16.normed, bf16[16,32,512]{2,1,0:T(8,128)(2,1)S(1)} %shard_map.51.u0, bf16[16,32,512]{2,1,0:T(8,128)(2,1)S(1)} %collective-permute-done.4.uz, ...), custom_call_target="tpu_custom_call" | custom-call | flops 1073741824 | bytes 1048576 | tf_op jit(solution)/shard_map/pallas_call | solution.py:231
  98.3 1.7 %shard_map.57 = (bf16[2,256,1024]{2,1,0:T(8,128)(2,1)S(1)}, bf16[1024,512]{1,0:T(8,128)(2,1)S(1)}) custom-call(s32[4]{0:T(128)S(1)} %pad_add_fusion.where, bf16[512,512]{1,0:T(8,128)(2,1)S(1)} %shard_map.52.hidden, bf16[16,32,512]{2,1,0:T(8,128)(2,1)S(1)} %shard_map.56.d0, bf16[16,32,512]{2,1,0:T(8,128)(2,1)S(1)} %collective-permute-done.11.dy), custom_call_target="tpu_custom_call" | custom-call | flops 268435456 | bytes 1048576 | tf_op jit(solution)/shard_map/pallas_call | solution.py:235
  100.0 2.7 %collective-permute-done.13.dyz = bf16[16,32,512]{2,1,0:T(8,128)(2,1)S(1)} collective-permute-done((bf16[16,32,512]{2,1,0:T(8,128)(2,1)S(1)}, bf16[16,32,512]{2,1,0:T(8,128)(2,1)S(1)}, u32[]{:S(2)}, u32[]{:S(2)}) %collective-permute-start.13) | collective-permute-done | bytes 524320 | tf_op jit(solution)/shard_map/ppermute | solution.py:26
  102.7 1.7 %shard_map.58 = (bf16[2,256,1024]{2,1,0:T(8,128)(2,1)S(1)}, bf16[1024,512]{1,0:T(8,128)(2,1)S(1)}) custom-call(s32[4]{0:T(128)S(1)} %pad_add_fusion.where, bf16[512,512]{1,0:T(8,128)(2,1)S(1)} %shard_map.52.hidden, bf16[16,32,512]{2,1,0:T(8,128)(2,1)S(1)} %collective-permute-done.12.dz, ...), custom_call_target="tpu_custom_call", output_to_operand_aliasing={{0}: (4, {})} | custom-call | flops 268435456 | bytes 1048576 | tf_op jit(solution)/shard_map/pallas_call | solution.py:238
  104.4 8.6 %collective-permute-start.14 = (bf16[2,256,1024]{2,1,0:T(8,128)(2,1)S(1)}, bf16[2,256,1024]{2,1,0:T(8,128)(2,1)S(1)}, u32[]{:S(2)}, u32[]{:S(2)}) collective-permute-start(bf16[2,256,1024]{2,1,0:T(8,128)(2,1)S(1)} %get-tuple-element.22), channel_id=1, source_target_pairs={{0,1},{1,0},{2,3},{3,2},{4,5},{5,4},{6,7},{7,6},{8,9},{9,8},{10,11... | collective-permute-start | bytes 3145736 | tf_op jit(solution)/shard_map/ppermute | solution.py:245
  113.0 2.1 %shard_map.59.own = bf16[2,256,1024]{2,1,0:T(8,128)(2,1)S(1)} custom-call(bf16[512,512]{1,0:T(8,128)(2,1)S(1)} %shard_map.52.hidden, bf16[1024,512]{1,0:T(8,128)(2,1)S(1)} %get-tuple-element.19.first, bf16[1024,512]{1,0:T(8,128)(2,1)S(1)} %get-tuple-element.21.second), custom_call_target="tpu_custom_call" | custom-call | flops 536870912 | bytes 1048576 | tf_op jit(solution)/shard_map/pallas_call | solution.py:246
  115.3 0.8 shard_map.60
  116.1 4.4 %collective-permute-start.15 = (bf16[2,2,64,1024]{3,2,1,0:T(8,128)(2,1)S(1)}, bf16[2,2,64,1024]{3,2,1,0:T(8,128)(2,1)S(1)}, u32[]{:S(2)}, u32[]{:S(2)}) collective-permute-start(bf16[2,2,64,1024]{3,2,1,0:T(8,128)(2,1)S(1)} %get-tuple-element.24), channel_id=1, source_target_pairs={{0,2},{1,7},{2,0},{3,5},{4,6},{5,3},{6,4},{7,1},{8,10},{9,15},{10,... | collective-permute-start | bytes 1572872 | tf_op jit(solution)/shard_map/ppermute | solution.py:34
  120.5 6.7 %collective-permute-done.15.came = bf16[2,2,64,1024]{3,2,1,0:T(8,128)(2,1)S(1)} collective-permute-done((bf16[2,2,64,1024]{3,2,1,0:T(8,128)(2,1)S(1)}, bf16[2,2,64,1024]{3,2,1,0:T(8,128)(2,1)S(1)}, u32[]{:S(2)}, u32[]{:S(2)}) %collective-permute-start.15) | collective-permute-done | bytes 524320 | tf_op jit(solution)/shard_map/ppermute | solution.py:34
  127.3 2.2 %collective-permute-start.16 = (bf16[2,64,1024]{2,1,0:T(8,128)(2,1)S(1)}, bf16[2,64,1024]{2,1,0:T(8,128)(2,1)S(1)}, u32[]{:S(2)}, u32[]{:S(2)}) collective-permute-start(bf16[2,64,1024]{2,1,0:T(8,128)(2,1)S(1)} %shard_map.61), channel_id=1, source_target_pairs={{0,6},{1,3},{2,4},{3,1},{4,2},{5,7},{6,0},{7,5},{8,14},{9,11},{10,... | collective-permute-start | bytes 786440 | tf_op jit(solution)/shard_map/ppermute | solution.py:34
  129.5 5.2 %collective-permute-done.16.late = bf16[2,64,1024]{2,1,0:T(8,128)(2,1)S(1)} collective-permute-done((bf16[2,64,1024]{2,1,0:T(8,128)(2,1)S(1)}, bf16[2,64,1024]{2,1,0:T(8,128)(2,1)S(1)}, u32[]{:S(2)}, u32[]{:S(2)}) %collective-permute-start.16) | collective-permute-done | bytes 262176 | tf_op jit(solution)/shard_map/ppermute | solution.py:34
  134.7 1.4 %shard_map.62 = bf16[64,2048]{1,0:T(8,128)(2,1)} custom-call(s32[4]{0:T(128)S(1)} %pad_add_fusion.where, bf16[64,2048]{1,0:T(8,128)(2,1)S(1)} %get-tuple-element.15.residual, bf16[2,2,64,1024]{3,2,1,0:T(8,128)(2,1)S(1)} %get-tuple-element.23.keep, bf16[2,2,64,1024]{3,2,1,0:T(8,128)(2,1)S(1)} %collective-permute-done.15.came, ...), custom_call_target="tpu_custom_call" | custom-call | tf_op jit(solution)/shard_map/pallas_call | solution.py:217
  (28 shorter events, 2.9 us)
Async XLA Ops:
  0.0 90.8 %copy-start = (bf16[512,2048]{1,0:T(8,128)(2,1)S(1)}, bf16[512,2048]{1,0:T(8,128)(2,1)}, u32[]{:S(2)}) copy-start(bf16[512,2048]{1,0:T(8,128)(2,1)} %tokens.1) | copy-start | bytes 6291460
  0.0 10.6 %collective-permute-start = (bf16[1,32,512]{2,1,0:T(8,128)(2,1)}, bf16[1,32,512]{2,1,0:T(8,128)(2,1)S(1)}, u32[]{:S(2)}, u32[]{:S(2)}) collective-permute-start(bf16[1,32,512]{2,1,0:T(8,128)(2,1)} %bitcast.9), channel_id=1, source_target_pairs={{32,0},{33,1},{40,8},{41,9},{48,16},{49,17},{56,24},{57,25},{0,32}... | collective-permute-start | bytes 98312 | tf_op jit(solution)/shard_map/ppermute | solution.py:26
  8.5 0.8 copy-start.1
  9.2 0.8 copy-start.2
  10.0 80.8 %copy-start.3 = (f32[2048]{0:T(1024)S(1)}, f32[2048]{0:T(1024)}, u32[]{:S(2)}) copy-start(f32[2048]{0:T(1024)} %param.5) | copy-start | bytes 24580
  10.6 19.8 %collective-permute-start.1 = (bf16[2,32,512]{2,1,0:T(8,128)(2,1)S(1)}, bf16[2,32,512]{2,1,0:T(8,128)(2,1)S(1)}, u32[]{:S(2)}, u32[]{:S(2)}) collective-permute-start(bf16[2,32,512]{2,1,0:T(8,128)(2,1)S(1)} %shard_map.48.a), channel_id=1, source_target_pairs={{256,0},{769,1},{320,64},{833,65},{384,128},{897,129},{448,192},{9... | collective-permute-start | bytes 196616 | tf_op jit(solution)/shard_map/ppermute | solution.py:26
  30.4 27.0 %collective-permute-start.2 = (bf16[4,32,512]{2,1,0:T(8,128)(2,1)S(1)}, bf16[4,32,512]{2,1,0:T(8,128)(2,1)S(1)}, u32[]{:S(2)}, u32[]{:S(2)}) collective-permute-start(bf16[4,32,512]{2,1,0:T(8,128)(2,1)S(1)} %shard_map.49.a), channel_id=1, source_target_pairs={{16,0},{49,1},{24,8},{57,9},{32,16},{1,17},{40,24},{9,25},{48,32},... | collective-permute-start | bytes 393224 | tf_op jit(solution)/shard_map/ppermute | solution.py:26
  34.2 8.8 %collective-permute-start.7 = (bf16[1,32,512]{2,1,0:T(8,128)(2,1)}, bf16[1,32,512]{2,1,0:T(8,128)(2,1)S(1)}, u32[]{:S(2)}, u32[]{:S(2)}) collective-permute-start(bf16[1,32,512]{2,1,0:T(8,128)(2,1)} %bitcast.11), channel_id=1, source_target_pairs={{256,0},{769,1},{320,64},{833,65},{384,128},{897,129},{448,192},{9... | collective-permute-start | bytes 98312 | tf_op jit(solution)/shard_map/ppermute | solution.py:26
  42.9 8.9 %collective-permute-start.8 = (bf16[2,32,512]{2,1,0:T(8,128)(2,1)S(1)}, bf16[2,32,512]{2,1,0:T(8,128)(2,1)S(1)}, u32[]{:S(2)}, u32[]{:S(2)}) collective-permute-start(bf16[2,32,512]{2,1,0:T(8,128)(2,1)S(1)} %shard_map.53.a), channel_id=1, source_target_pairs={{32,0},{33,1},{40,8},{41,9},{48,16},{49,17},{56,24},{57,25},{0,32}... | collective-permute-start | bytes 196616 | tf_op jit(solution)/shard_map/ppermute | solution.py:26
  51.9 11.3 %collective-permute-start.9 = (bf16[4,32,512]{2,1,0:T(8,128)(2,1)S(1)}, bf16[4,32,512]{2,1,0:T(8,128)(2,1)S(1)}, u32[]{:S(2)}, u32[]{:S(2)}) collective-permute-start(bf16[4,32,512]{2,1,0:T(8,128)(2,1)S(1)} %shard_map.54.a), channel_id=1, source_target_pairs={{128,0},{897,1},{192,64},{961,65},{256,128},{1,129},{320,192},{65,... | collective-permute-start | bytes 393224 | tf_op jit(solution)/shard_map/ppermute | solution.py:26
  57.5 10.9 %collective-permute-start.3 = (bf16[8,32,512]{2,1,0:T(8,128)(2,1)S(1)}, bf16[8,32,512]{2,1,0:T(8,128)(2,1)S(1)}, u32[]{:S(2)}, u32[]{:S(2)}) collective-permute-start(bf16[8,32,512]{2,1,0:T(8,128)(2,1)S(1)} %shard_map.50.a), channel_id=1, source_target_pairs={{128,0},{897,1},{192,64},{961,65},{256,128},{1,129},{320,192},{65,... | collective-permute-start | bytes 786440 | tf_op jit(solution)/shard_map/ppermute | solution.py:26
  63.2 10.5 %collective-permute-start.10 = (bf16[8,32,512]{2,1,0:T(8,128)(2,1)S(1)}, bf16[8,32,512]{2,1,0:T(8,128)(2,1)S(1)}, u32[]{:S(2)}, u32[]{:S(2)}) collective-permute-start(bf16[8,32,512]{2,1,0:T(8,128)(2,1)S(1)} %shard_map.55.a), channel_id=1, source_target_pairs={{16,0},{49,1},{24,8},{57,9},{32,16},{1,17},{40,24},{9,25},{48,32},... | collective-permute-start | bytes 786440 | tf_op jit(solution)/shard_map/ppermute | solution.py:26
  68.4 12.7 %collective-permute-start.4 = (bf16[16,32,512]{2,1,0:T(8,128)(2,1)S(1)}, bf16[16,32,512]{2,1,0:T(8,128)(2,1)S(1)}, u32[]{:S(2)}, u32[]{:S(2)}) collective-permute-start(bf16[16,32,512]{2,1,0:T(8,128)(2,1)S(1)} %shard_map.51.u0), channel_id=1, source_target_pairs={{64,0},{961,1},{128,64},{1,65},{192,128},{65,129},{256,192},{129,1... | collective-permute-start | bytes 1572872 | tf_op jit(solution)/shard_map/ppermute | solution.py:26
  73.7 15.1 %collective-permute-start.11 = (bf16[16,32,512]{2,1,0:T(8,128)(2,1)S(1)}, bf16[16,32,512]{2,1,0:T(8,128)(2,1)S(1)}, u32[]{:S(2)}, u32[]{:S(2)}) collective-permute-start(bf16[16,32,512]{2,1,0:T(8,128)(2,1)S(1)} %shard_map.56.d0), channel_id=1, source_target_pairs={{8,0},{57,1},{16,8},{1,9},{24,16},{9,17},{32,24},{17,25},{40,32},{... | collective-permute-start | bytes 1572872 | tf_op jit(solution)/shard_map/ppermute | solution.py:26
  77.7 15.8 %collective-permute-start.5 = (bf16[16,32,512]{2,1,0:T(8,128)(2,1)S(1)}, bf16[16,32,512]{2,1,0:T(8,128)(2,1)S(1)}, u32[]{:S(2)}, u32[]{:S(2)}) collective-permute-start(bf16[16,32,512]{2,1,0:T(8,128)(2,1)S(1)} %shard_map.51.u0), channel_id=1, source_target_pairs={{8,0},{57,1},{16,8},{1,9},{24,16},{9,17},{32,24},{17,25},{40,32},{... | collective-permute-start | bytes 1572872 | tf_op jit(solution)/shard_map/ppermute | solution.py:26
  81.1 15.0 %collective-permute-start.6 = (bf16[16,32,512]{2,1,0:T(8,128)(2,1)S(1)}, bf16[16,32,512]{2,1,0:T(8,128)(2,1)S(1)}, u32[]{:S(2)}, u32[]{:S(2)}) collective-permute-start(bf16[16,32,512]{2,1,0:T(8,128)(2,1)S(1)} %collective-permute-done.4.uz), channel_id=1, source_target_pairs={{8,0},{57,1},{16,8},{1,9},{24,16},{9,17},{32,24},{17,25},{40,32},{... | collective-permute-start | bytes 1572872 | tf_op jit(solution)/shard_map/ppermute | solution.py:26
  84.3 15.7 %collective-permute-start.12 = (bf16[16,32,512]{2,1,0:T(8,128)(2,1)S(1)}, bf16[16,32,512]{2,1,0:T(8,128)(2,1)S(1)}, u32[]{:S(2)}, u32[]{:S(2)}) collective-permute-start(bf16[16,32,512]{2,1,0:T(8,128)(2,1)S(1)} %shard_map.56.d0), channel_id=1, source_target_pairs={{64,0},{961,1},{128,64},{1,65},{192,128},{65,129},{256,192},{129,1... | collective-permute-start | bytes 1572872 | tf_op jit(solution)/shard_map/ppermute | solution.py:26
  88.8 13.9 %collective-permute-start.13 = (bf16[16,32,512]{2,1,0:T(8,128)(2,1)S(1)}, bf16[16,32,512]{2,1,0:T(8,128)(2,1)S(1)}, u32[]{:S(2)}, u32[]{:S(2)}) collective-permute-start(bf16[16,32,512]{2,1,0:T(8,128)(2,1)S(1)} %collective-permute-done.11.dy), channel_id=1, source_target_pairs={{64,0},{961,1},{128,64},{1,65},{192,128},{65,129},{256,192},{129,1... | collective-permute-start | bytes 1572872 | tf_op jit(solution)/shard_map/ppermute | solution.py:26
  104.4 10.9 %collective-permute-start.14 = (bf16[2,256,1024]{2,1,0:T(8,128)(2,1)S(1)}, bf16[2,256,1024]{2,1,0:T(8,128)(2,1)S(1)}, u32[]{:S(2)}, u32[]{:S(2)}) collective-permute-start(bf16[2,256,1024]{2,1,0:T(8,128)(2,1)S(1)} %get-tuple-element.22), channel_id=1, source_target_pairs={{0,1},{1,0},{2,3},{3,2},{4,5},{5,4},{6,7},{7,6},{8,9},{9,8},{10,11... | collective-permute-start | bytes 3145736 | tf_op jit(solution)/shard_map/ppermute | solution.py:245
  116.1 11.1 %collective-permute-start.15 = (bf16[2,2,64,1024]{3,2,1,0:T(8,128)(2,1)S(1)}, bf16[2,2,64,1024]{3,2,1,0:T(8,128)(2,1)S(1)}, u32[]{:S(2)}, u32[]{:S(2)}) collective-permute-start(bf16[2,2,64,1024]{3,2,1,0:T(8,128)(2,1)S(1)} %get-tuple-element.24), channel_id=1, source_target_pairs={{0,2},{1,7},{2,0},{3,5},{4,6},{5,3},{6,4},{7,1},{8,10},{9,15},{10,... | collective-permute-start | bytes 1572872 | tf_op jit(solution)/shard_map/ppermute | solution.py:34
  127.3 7.4 %collective-permute-start.16 = (bf16[2,64,1024]{2,1,0:T(8,128)(2,1)S(1)}, bf16[2,64,1024]{2,1,0:T(8,128)(2,1)S(1)}, u32[]{:S(2)}, u32[]{:S(2)}) collective-permute-start(bf16[2,64,1024]{2,1,0:T(8,128)(2,1)S(1)} %shard_map.61), channel_id=1, source_target_pairs={{0,6},{1,3},{2,4},{3,1},{4,2},{5,7},{6,0},{7,5},{8,14},{9,11},{10,... | collective-permute-start | bytes 786440 | tf_op jit(solution)/shard_map/ppermute | solution.py:34

commit v5 on v4

v5 whole, which is shorter than its diff:
```python
import jax
import jax.numpy as jnp
from jax import lax
from jax.experimental import pallas as pl
from jax.experimental.pallas import tpu as pltpu
from jax.sharding import Mesh
from jax.sharding import PartitionSpec as P


EPS = 1e-06
REP, Z, Y, X, CORE = 2, 8, 8, 4, 2
VMEM = pl.BlockSpec(memory_space=pltpu.VMEM)


UP_STEPS = (("y", 4), ("z", 4), ("y", 2), ("z", 2))
DOWN_STEPS = (("z", 4), ("y", 4), ("z", 2), ("y", 2))


def from_side(array, axis, shift):
    names, size = (("y", "core"), Y) if axis == "y" else (("rep", "z", "core"), REP * Z)
    pairs = []
    for i in range(size):
        pairs.append(((i + shift) % size * 2, i * 2))
        pairs.append(((i - shift) % size * 2 + 1, i * 2 + 1))
    return lax.ppermute(array, names, pairs)


def between_x(array, first, second):
    pairs = []
    for x in range(X):
        pairs.append((x * 2, (x ^ first) * 2))
        pairs.append((x * 2 + 1, (x ^ second) * 2 + 1))
    return lax.ppermute(array, ("x", "core"), pairs)


def offsets(steps):
    laid = [(0, 0)]
    for axis, shift in steps:
        dz, dy = (shift, 0) if axis == "z" else (0, shift)
        laid = laid + [(z + dz, y + dy) for z, y in laid]
    return laid


def shifted(steps, dz, dy):
    return [(z + dz, y + dy) for z, y in offsets(steps)]


def kernel_call(kernel, outs, n_vmem, scratch=(), mib=8, flops=0, **rest):
    single = not isinstance(outs, tuple)
    return pl.pallas_call(
        kernel,
        out_shape=outs,
        in_specs=[VMEM] * n_vmem,
        out_specs=VMEM if single else (VMEM,) * len(outs),
        scratch_shapes=[pltpu.VMEM(s, jnp.bfloat16) for s in scratch],
        compiler_params=pltpu.CompilerParams(vmem_limit_bytes=mib * 2**20),
        cost_estimate=pl.CostEstimate(
            flops=flops, bytes_accessed=2**20, transcendentals=0
        )
        if flops
        else None,
        **rest,
    )


def bf16(*shape):
    return jax.ShapeDtypeStruct(shape, jnp.bfloat16)


def join_kernel(a, b, out):
    n = a.shape[0]
    out[:n] = a[...]
    out[n:] = b[...]


def join(a, b):
    n = a.shape[0]
    return kernel_call(join_kernel, bf16(2 * n, 32, 512), 2)(a, b)


def stage_kernel(up, down, up_out, down_out):
    up_out[...] = up[...]
    down_out[...] = down[...]


def norm_kernel(tokens, gain, normed, residual):
    mine = lax.axis_index("x") * CORE + lax.axis_index("core")
    residual[...] = tokens[pl.ds(pl.multiple_of(mine * 64, 64), 64), :]

    @pl.loop(0, 16)
    def _(n):
        rows = pl.ds(pl.multiple_of(n * 32, 32), 32)
        xf = tokens[rows, :].astype(jnp.float32)
        scale = lax.rsqrt(jnp.mean(xf * xf, axis=-1, keepdims=True) + EPS)
        normed[rows, :] = (xf * scale * gain[...]).astype(jnp.bfloat16)


def place(piece, laid, whole, halved):
    z, y = lax.axis_index("z"), lax.axis_index("y")
    sign = 1 - 2 * lax.axis_index("core")
    for j, (dz, dy) in enumerate(laid):
        at_z = (z + sign * dz) & (Z - 1)
        at_y = (y + sign * dy) & (Y - 1)
        at = ((at_z >> 1) if halved else at_z) * Y + at_y
        whole[pl.ds(pl.multiple_of(at * 32, 32), 32), :] = piece[j]


def down_product(hidden, rows, down, out):
    @pl.loop(0, 4)
    def _(n):
        columns = pl.ds(pl.multiple_of(n * 256, 256), 256)
        out[:, columns] = lax.dot_general(
            hidden[rows, :],
            down[columns, :],
            (((1,), (1,)), ((), ())),
            preferred_element_type=jnp.float32,
        ).astype(jnp.bfloat16)


THEIRS, OWN = slice(0, 256), slice(256, 512)


def up_kernel(normed, u0, uz, uy, uzy, hidden, up):
    for piece, shift in ((u0, (0, 0)), (uz, (1, 0)), (uy, (0, 1)), (uzy, (1, 1))):
        place(piece, shifted(UP_STEPS, *shift), up, False)
    core = lax.axis_index("core")

    @pl.loop(0, 2)
    def _(n):
        columns = pl.ds(pl.multiple_of(n * 256, 256), 256)
        lifted = jnp.dot(
            normed[...], up[:, columns], preferred_element_type=jnp.float32
        )
        active = jnp.square(jnp.maximum(lifted, 0.0)).astype(jnp.bfloat16)
        for j in range(X * CORE):
            x, c = divmod(j, CORE)
            side = jnp.where(core == c, 256, 0)
            rows = pl.ds(pl.multiple_of(side + x * 64, 64), 64)
            hidden[rows, columns] = active[j * 64 : (j + 1) * 64]


def early_kernel(hidden, d0, dy, theirs, down):
    place(d0, offsets(DOWN_STEPS), down, True)
    place(dy, shifted(DOWN_STEPS, 0, 1), down, True)
    down_product(hidden, THEIRS, down, theirs)


def late_kernel(hidden, dz, dyz, theirs, down):
    place(dz, shifted(DOWN_STEPS, 1, 0), down, True)
    place(dyz, shifted(DOWN_STEPS, 1, 1), down, True)
    down_product(hidden, THEIRS, down, theirs)


def own_kernel(hidden, down, own):
    down_product(hidden, OWN, down, own)


def add_kernel(own, beside, keep, send):
    x, core = lax.axis_index("x"), lax.axis_index("core")
    first, second = 1 + 2 * core, 3 - 2 * core
    for out, k, chunk in (
        (send, 0, x ^ first),
        (send, 1, x ^ 2),
        (keep, 0, x),
        (keep, 1, x ^ second),
    ):
        rows = pl.ds(pl.multiple_of(chunk * 64, 64), 64)
        total = own[rows].astype(jnp.float32) + beside[rows].astype(jnp.float32)
        out[k] = total.astype(jnp.bfloat16)


def pass_kernel(keep, came, out):
    total = keep[1].astype(jnp.float32) + came[1].astype(jnp.float32)
    out[...] = total.astype(jnp.bfloat16)


def last_kernel(residual, keep0, came0, late0, keep1, came1, late1, out):
    odd = lax.axis_index("z") & 1
    for part, terms in ((0, (keep0, came0, late0)), (1, (keep1, came1, late1))):
        for k in range(4):
            at = (2 * k + (odd ^ part)) * 256
            columns = pl.ds(pl.multiple_of(at, 256), 256)
            here = slice(k * 256, (k + 1) * 256)
            total = residual[:, columns].astype(jnp.float32)
            keep, came, late = terms
            for term in (keep.at[0], came.at[0], late):
                total = total + term[:, here].astype(jnp.float32)
            out[:, columns] = total.astype(jnp.bfloat16)


def gathered(up, down):
    for k in range(4):
        up_in = from_side(up, *UP_STEPS[k])
        down_in = from_side(down, *DOWN_STEPS[k])
        if k == 0:
            own = bf16(1, 32, 512)
            up, down = kernel_call(stage_kernel, (own, own), 2)(up, down)
        up = join(up, up_in)
        down = join(down, down_in)
    up_z = from_side(up, "z", 1)
    up_y = from_side(up, "y", 1)
    down_y = from_side(down, "y", 1)
    down_z = from_side(down, "z", 1)
    up_zy = from_side(up_z, "y", 1)
    down_yz = from_side(down_y, "z", 1)
    return (up, up_z, up_y, up_zy), (down, down_y, down_z, down_yz)


def over_tp(beside, own):
    two = bf16(2, 64, 1024)
    keep, send = kernel_call(add_kernel, (two, two), 2)(own, beside)
    came = between_x(send, 1, 3)
    passed = kernel_call(pass_kernel, bf16(64, 1024), 2)(keep, came)
    late = between_x(passed, 3, 1)
    return keep, came, late


def shards(tokens, norm_gain, up_weight, down_weight):
    up, down = gathered(up_weight[None], down_weight.T[None])
    normed, residual = kernel_call(
        norm_kernel, (bf16(512, 2048), bf16(64, 2048)), 2, mib=12, flops=2**24
    )(tokens, norm_gain[None])
    hidden = kernel_call(
        up_kernel, bf16(512, 512), 5, scratch=((2048, 512),), mib=12, flops=2**30
    )(normed, *up)
    out, rows = bf16(256, 1024), bf16(1024, 512)
    trades = []
    for part, kernel in ((0, early_kernel), (1, late_kernel)):
        pieces = down[2 * part : 2 * part + 2]
        theirs, placed = kernel_call(kernel, (out, rows), 3, flops=2**28)(
            hidden, *pieces
        )
        beside = lax.ppermute(theirs, "core", [(0, 1), (1, 0)])
        own = kernel_call(own_kernel, out, 2, flops=2**28)(hidden, placed)
        trades += over_tp(beside, own)
    return kernel_call(last_kernel, bf16(64, 2048), 7)(residual, *trades)


def solution(mesh):
    torus = Mesh(
        mesh.devices.reshape(REP, Z, Y, X, CORE), ("rep", "z", "y", "x", "core")
    )
    rep_fs = ("rep", "z", "y")
    tp = ("x", "core")
    in_specs = (P(rep_fs, None), P(), P(("z", "y"), tp), P(tp, ("z", "y")))
    return jax.shard_map(
        shards,
        mesh=torus,
        in_specs=in_specs,
        out_specs=P(rep_fs + tp, None),
        check_vma=False,
    )
```

time: 138 us -> 136 us (0.986)
  starting transfers between devices: 80.5 us -> 86.3 us
  waiting for transfers between devices: 40.4 us -> 36.4 us
  Pallas kernels: 13.3 us -> 9.54 us
    ppermute x2 -> x4, waiting for transfers between devices: 11.9 us -> 7.74 us  [between_x(): return lax.ppermute(array, ('x', 'core'), pairs)]
    ppermute x2 -> x4, starting transfers between devices: 6.6 us -> 10.6 us  [between_x(): return lax.ppermute(array, ('x', 'core'), pairs)]
    pallas_call x15 -> x18, Pallas kernels: 8.47 us -> 5.82 us  [the longest x2 2.38 us: shards(): kernel_call(kernel, (out, rows), 3, flops=2 ** 28)(hidden, *pieces)]
    ppermute x1 -> x2, starting transfers between devices: 8.59 us -> 10.9 us  [shards(): beside = lax.ppermute(theirs, 'core', [(0, 1), (1, 0)])]
  transfers between devices with their start and end apart: 17 -> 20, of which waited for: 10 -> 9; matrix products, arithmetic and copies ran while one was open for 0% -> 0% of each run, Pallas kernels for 7% -> 6%
where the time goes in v5:
time: 136 us; the launch traced here: 134 us
  starting transfers between devices  86.3 us (63%)
  waiting for transfers between devices  36.4 us (27%)
  Pallas kernels  9.54 us (7%)
  local copies, waits for them, and re-layouts  1.53 us (1%)
    ppermute x14, starting transfers between devices, from_side(): return lax.ppermute(array, names, pairs)  64.9 us
    ppermute x14, waiting for transfers between devices, from_side(): return lax.ppermute(array, names, pairs)  28.7 us
    ppermute x2, starting transfers between devices, shards(): beside = lax.ppermute(theirs, 'core', [(0, 1), (1, 0)])  10.9 us
    ppermute x4, starting transfers between devices, between_x(): return lax.ppermute(array, ('x', 'core'), pairs)  10.6 us
    ppermute x4, waiting for transfers between devices, between_x(): return lax.ppermute(array, ('x', 'core'), pairs)  7.74 us
  transfers between devices with their start and end apart: 20, of which 9 were waited for; matrix products, arithmetic and copies ran while one was open for 0% of the time, Pallas kernels for 6%

profile of v5, /device:TPU:1, one launch (start us, length us, event | category | flops | bytes accessed | tf_op | source)
XLA Modules:
  0.0 134.2 jit_solution(16987139879518266226)
XLA Ops:
  0.0 8.4 %collective-permute-start = (bf16[1,32,512]{2,1,0:T(8,128)(2,1)}, bf16[1,32,512]{2,1,0:T(8,128)(2,1)S(1)}, u32[]{:S(2)}, u32[]{:S(2)}) collective-permute-start(bf16[1,32,512]{2,1,0:T(8,128)(2,1)} %bitcast.5), channel_id=1, source_target_pairs={{32,0},{33,1},{40,8},{41,9},{48,16},{49,17},{56,24},{57,25},{0,32}... | collective-permute-start | bytes 98312 | tf_op jit(solution)/shard_map/ppermute | solution.py:25
  10.0 10.6 %collective-permute-start.1 = (bf16[2,32,512]{2,1,0:T(8,128)(2,1)S(1)}, bf16[2,32,512]{2,1,0:T(8,128)(2,1)S(1)}, u32[]{:S(2)}, u32[]{:S(2)}) collective-permute-start(bf16[2,32,512]{2,1,0:T(8,128)(2,1)S(1)} %shard_map.48.a), channel_id=1, source_target_pairs={{256,0},{769,1},{320,64},{833,65},{384,128},{897,129},{448,192},{9... | collective-permute-start | bytes 196616 | tf_op jit(solution)/shard_map/ppermute | solution.py:25
  20.6 9.2 %collective-permute-done.1.b = bf16[2,32,512]{2,1,0:T(8,128)(2,1)S(1)} collective-permute-done((bf16[2,32,512]{2,1,0:T(8,128)(2,1)S(1)}, bf16[2,32,512]{2,1,0:T(8,128)(2,1)S(1)}, u32[]{:S(2)}, u32[]{:S(2)}) %collective-permute-start.1) | collective-permute-done | bytes 65568 | tf_op jit(solution)/shard_map/ppermute | solution.py:25
  29.8 4.4 %collective-permute-start.2 = (bf16[4,32,512]{2,1,0:T(8,128)(2,1)S(1)}, bf16[4,32,512]{2,1,0:T(8,128)(2,1)S(1)}, u32[]{:S(2)}, u32[]{:S(2)}) collective-permute-start(bf16[4,32,512]{2,1,0:T(8,128)(2,1)S(1)} %shard_map.49.a), channel_id=1, source_target_pairs={{16,0},{49,1},{24,8},{57,9},{32,16},{1,17},{40,24},{9,25},{48,32},... | collective-permute-start | bytes 393224 | tf_op jit(solution)/shard_map/ppermute | solution.py:25
  34.2 2.8 %collective-permute-start.7 = (bf16[1,32,512]{2,1,0:T(8,128)(2,1)}, bf16[1,32,512]{2,1,0:T(8,128)(2,1)S(1)}, u32[]{:S(2)}, u32[]{:S(2)}) collective-permute-start(bf16[1,32,512]{2,1,0:T(8,128)(2,1)} %bitcast.7), channel_id=1, source_target_pairs={{256,0},{769,1},{320,64},{833,65},{384,128},{897,129},{448,192},{9... | collective-permute-start | bytes 98312 | tf_op jit(solution)/shard_map/ppermute | solution.py:25
  37.0 6.0 %collective-permute-done.7.b = bf16[1,32,512]{2,1,0:T(8,128)(2,1)S(1)} collective-permute-done((bf16[1,32,512]{2,1,0:T(8,128)(2,1)}, bf16[1,32,512]{2,1,0:T(8,128)(2,1)S(1)}, u32[]{:S(2)}, u32[]{:S(2)}) %collective-permute-start.7) | collective-permute-done | bytes 32800 | tf_op jit(solution)/shard_map/ppermute | solution.py:25
  42.9 5.2 %collective-permute-start.8 = (bf16[2,32,512]{2,1,0:T(8,128)(2,1)S(1)}, bf16[2,32,512]{2,1,0:T(8,128)(2,1)S(1)}, u32[]{:S(2)}, u32[]{:S(2)}) collective-permute-start(bf16[2,32,512]{2,1,0:T(8,128)(2,1)S(1)} %shard_map.53.a), channel_id=1, source_target_pairs={{32,0},{33,1},{40,8},{41,9},{48,16},{49,17},{56,24},{57,25},{0,32}... | collective-permute-start | bytes 196616 | tf_op jit(solution)/shard_map/ppermute | solution.py:25
  48.2 3.7 %collective-permute-done.8.b = bf16[2,32,512]{2,1,0:T(8,128)(2,1)S(1)} collective-permute-done((bf16[2,32,512]{2,1,0:T(8,128)(2,1)S(1)}, bf16[2,32,512]{2,1,0:T(8,128)(2,1)S(1)}, u32[]{:S(2)}, u32[]{:S(2)}) %collective-permute-start.8) | collective-permute-done | bytes 65568 | tf_op jit(solution)/shard_map/ppermute | solution.py:25
  51.9 5.5 %collective-permute-start.9 = (bf16[4,32,512]{2,1,0:T(8,128)(2,1)S(1)}, bf16[4,32,512]{2,1,0:T(8,128)(2,1)S(1)}, u32[]{:S(2)}, u32[]{:S(2)}) collective-permute-start(bf16[4,32,512]{2,1,0:T(8,128)(2,1)S(1)} %shard_map.54.a), channel_id=1, source_target_pairs={{128,0},{897,1},{192,64},{961,65},{256,128},{1,129},{320,192},{65,... | collective-permute-start | bytes 393224 | tf_op jit(solution)/shard_map/ppermute | solution.py:25
  57.5 1.9 %collective-permute-start.3 = (bf16[8,32,512]{2,1,0:T(8,128)(2,1)S(1)}, bf16[8,32,512]{2,1,0:T(8,128)(2,1)S(1)}, u32[]{:S(2)}, u32[]{:S(2)}) collective-permute-start(bf16[8,32,512]{2,1,0:T(8,128)(2,1)S(1)} %shard_map.50.a), channel_id=1, source_target_pairs={{128,0},{897,1},{192,64},{961,65},{256,128},{1,129},{320,192},{65,... | collective-permute-start | bytes 786440 | tf_op jit(solution)/shard_map/ppermute | solution.py:25
  59.4 3.7 %collective-permute-done.9.b = bf16[4,32,512]{2,1,0:T(8,128)(2,1)S(1)} collective-permute-done((bf16[4,32,512]{2,1,0:T(8,128)(2,1)S(1)}, bf16[4,32,512]{2,1,0:T(8,128)(2,1)S(1)}, u32[]{:S(2)}, u32[]{:S(2)}) %collective-permute-start.9) | collective-permute-done | bytes 131104 | tf_op jit(solution)/shard_map/ppermute | solution.py:25
  63.2 5.2 %collective-permute-start.10 = (bf16[8,32,512]{2,1,0:T(8,128)(2,1)S(1)}, bf16[8,32,512]{2,1,0:T(8,128)(2,1)S(1)}, u32[]{:S(2)}, u32[]{:S(2)}) collective-permute-start(bf16[8,32,512]{2,1,0:T(8,128)(2,1)S(1)} %shard_map.55.a), channel_id=1, source_target_pairs={{16,0},{49,1},{24,8},{57,9},{32,16},{1,17},{40,24},{9,25},{48,32},... | collective-permute-start | bytes 786440 | tf_op jit(solution)/shard_map/ppermute | solution.py:25
  68.4 5.2 %collective-permute-start.4 = (bf16[16,32,512]{2,1,0:T(8,128)(2,1)S(1)}, bf16[16,32,512]{2,1,0:T(8,128)(2,1)S(1)}, u32[]{:S(2)}, u32[]{:S(2)}) collective-permute-start(bf16[16,32,512]{2,1,0:T(8,128)(2,1)S(1)} %shard_map.51.u0), channel_id=1, source_target_pairs={{64,0},{961,1},{128,64},{1,65},{192,128},{65,129},{256,192},{129,1... | collective-permute-start | bytes 1572872 | tf_op jit(solution)/shard_map/ppermute | solution.py:25
  73.7 1.5 %collective-permute-done.10.b = bf16[8,32,512]{2,1,0:T(8,128)(2,1)S(1)} collective-permute-done((bf16[8,32,512]{2,1,0:T(8,128)(2,1)S(1)}, bf16[8,32,512]{2,1,0:T(8,128)(2,1)S(1)}, u32[]{:S(2)}, u32[]{:S(2)}) %collective-permute-start.10) | collective-permute-done | bytes 262176 | tf_op jit(solution)/shard_map/ppermute | solution.py:25
  75.2 2.3 %collective-permute-start.11 = (bf16[16,32,512]{2,1,0:T(8,128)(2,1)S(1)}, bf16[16,32,512]{2,1,0:T(8,128)(2,1)S(1)}, u32[]{:S(2)}, u32[]{:S(2)}) collective-permute-start(bf16[16,32,512]{2,1,0:T(8,128)(2,1)S(1)} %shard_map.56.d0), channel_id=1, source_target_pairs={{8,0},{57,1},{16,8},{1,9},{24,16},{9,17},{32,24},{17,25},{40,32},{... | collective-permute-start | bytes 1572872 | tf_op jit(solution)/shard_map/ppermute | solution.py:25
  77.6 3.5 %collective-permute-start.5 = (bf16[16,32,512]{2,1,0:T(8,128)(2,1)S(1)}, bf16[16,32,512]{2,1,0:T(8,128)(2,1)S(1)}, u32[]{:S(2)}, u32[]{:S(2)}) collective-permute-start(bf16[16,32,512]{2,1,0:T(8,128)(2,1)S(1)} %shard_map.51.u0), channel_id=1, source_target_pairs={{8,0},{57,1},{16,8},{1,9},{24,16},{9,17},{32,24},{17,25},{40,32},{... | collective-permute-start | bytes 1572872 | tf_op jit(solution)/shard_map/ppermute | solution.py:25
  81.1 3.0 %collective-permute-start.6 = (bf16[16,32,512]{2,1,0:T(8,128)(2,1)S(1)}, bf16[16,32,512]{2,1,0:T(8,128)(2,1)S(1)}, u32[]{:S(2)}, u32[]{:S(2)}) collective-permute-start(bf16[16,32,512]{2,1,0:T(8,128)(2,1)S(1)} %collective-permute-done.4.uz), channel_id=1, source_target_pairs={{8,0},{57,1},{16,8},{1,9},{24,16},{9,17},{32,24},{17,25},{40,32},{... | collective-permute-start | bytes 1572872 | tf_op jit(solution)/shard_map/ppermute | solution.py:25
  84.1 4.7 %collective-permute-start.15 = (bf16[16,32,512]{2,1,0:T(8,128)(2,1)S(1)}, bf16[16,32,512]{2,1,0:T(8,128)(2,1)S(1)}, u32[]{:S(2)}, u32[]{:S(2)}) collective-permute-start(bf16[16,32,512]{2,1,0:T(8,128)(2,1)S(1)} %shard_map.56.d0), channel_id=1, source_target_pairs={{64,0},{961,1},{128,64},{1,65},{192,128},{65,129},{256,192},{129,1... | collective-permute-start | bytes 1572872 | tf_op jit(solution)/shard_map/ppermute | solution.py:25
  88.9 1.9 %collective-permute-start.16 = (bf16[16,32,512]{2,1,0:T(8,128)(2,1)S(1)}, bf16[16,32,512]{2,1,0:T(8,128)(2,1)S(1)}, u32[]{:S(2)}, u32[]{:S(2)}) collective-permute-start(bf16[16,32,512]{2,1,0:T(8,128)(2,1)S(1)} %collective-permute-done.11.dy), channel_id=1, source_target_pairs={{64,0},{961,1},{128,64},{1,65},{192,128},{65,129},{256,192},{129,1... | collective-permute-start | bytes 1572872 | tf_op jit(solution)/shard_map/ppermute | solution.py:25
  90.8 2.1 %shard_map.46 = (bf16[512,2048]{1,0:T(8,128)(2,1)S(1)}, bf16[64,2048]{1,0:T(8,128)(2,1)S(1)}) custom-call(bf16[512,2048]{1,0:T(8,128)(2,1)S(1)} %copy-done, f32[1,2048]{1,0:T(1,128)S(1)} %bitcast.9), custom_call_target="tpu_custom_call" | custom-call | flops 16777216 | bytes 1048576 | tf_op jit(solution)/shard_map/pallas_call | solution.py:220
  92.9 4.6 %collective-permute-done.6.uzy = bf16[16,32,512]{2,1,0:T(8,128)(2,1)S(1)} collective-permute-done((bf16[16,32,512]{2,1,0:T(8,128)(2,1)S(1)}, bf16[16,32,512]{2,1,0:T(8,128)(2,1)S(1)}, u32[]{:S(2)}, u32[]{:S(2)}) %collective-permute-start.6) | collective-permute-done | bytes 524320 | tf_op jit(solution)/shard_map/ppermute | solution.py:25
  97.6 1.6 %shard_map.52.hidden = bf16[512,512]{1,0:T(8,128)(2,1)S(1)} custom-call(bf16[512,2048]{1,0:T(8,128)(2,1)S(1)} %get-tuple-element.18.normed, bf16[16,32,512]{2,1,0:T(8,128)(2,1)S(1)} %shard_map.51.u0, bf16[16,32,512]{2,1,0:T(8,128)(2,1)S(1)} %collective-permute-done.4.uz, bf16[16,32,512]{2,1,0:T(8,128)(2,1)S(1)} %collective-permute-done.5.uy, ...), custom_call_target="tpu_custom_call" | custom-call | flops 1073741824 | bytes 1048576 | tf_op jit(solution)/shard_map/pallas_call | solution.py:223
  100.4 8.6 %collective-permute-start.12 = (bf16[256,1024]{1,0:T(8,128)(2,1)S(1)}, bf16[256,1024]{1,0:T(8,128)(2,1)S(1)}, u32[]{:S(2)}, u32[]{:S(2)}) collective-permute-start(bf16[256,1024]{1,0:T(8,128)(2,1)S(1)} %get-tuple-element.22), channel_id=1, source_target_pairs={{0,1},{1,0},{2,3},{3,2},{4,5},{5,4},{6,7},{7,6},{8,9},{9,8},{10,11... | collective-permute-start | bytes 1572872 | tf_op jit(solution)/shard_map/ppermute | solution.py:233
  109.0 1.2 shard_map.61
  110.2 2.2 %collective-permute-start.17 = (bf16[256,1024]{1,0:T(8,128)(2,1)S(1)}, bf16[256,1024]{1,0:T(8,128)(2,1)S(1)}, u32[]{:S(2)}, u32[]{:S(2)}) collective-permute-start(bf16[256,1024]{1,0:T(8,128)(2,1)S(1)} %get-tuple-element.26), channel_id=1, source_target_pairs={{0,1},{1,0},{2,3},{3,2},{4,5},{5,4},{6,7},{7,6},{8,9},{9,8},{10,11... | collective-permute-start | bytes 1572872 | tf_op jit(solution)/shard_map/ppermute | solution.py:233
  114.7 4.4 %collective-permute-start.13 = (bf16[2,64,1024]{2,1,0:T(8,128)(2,1)S(1)}, bf16[2,64,1024]{2,1,0:T(8,128)(2,1)S(1)}, u32[]{:S(2)}, u32[]{:S(2)}) collective-permute-start(bf16[2,64,1024]{2,1,0:T(8,128)(2,1)S(1)} %get-tuple-element.24), channel_id=1, source_target_pairs={{0,2},{1,7},{2,0},{3,5},{4,6},{5,3},{6,4},{7,1},{8,10},{9,15},{10,... | collective-permute-start | bytes 786440 | tf_op jit(solution)/shard_map/ppermute | solution.py:33
  119.3 2.1 %collective-permute-start.18 = (bf16[2,64,1024]{2,1,0:T(8,128)(2,1)S(1)}, bf16[2,64,1024]{2,1,0:T(8,128)(2,1)S(1)}, u32[]{:S(2)}, u32[]{:S(2)}) collective-permute-start(bf16[2,64,1024]{2,1,0:T(8,128)(2,1)S(1)} %get-tuple-element.28), channel_id=1, source_target_pairs={{0,2},{1,7},{2,0},{3,5},{4,6},{5,3},{6,4},{7,1},{8,10},{9,15},{10,... | collective-permute-start | bytes 786440 | tf_op jit(solution)/shard_map/ppermute | solution.py:33
  121.4 1.7 %collective-permute-done.13.came.came0 = bf16[2,64,1024]{2,1,0:T(8,128)(2,1)S(1)} collective-permute-done((bf16[2,64,1024]{2,1,0:T(8,128)(2,1)S(1)}, bf16[2,64,1024]{2,1,0:T(8,128)(2,1)S(1)}, u32[]{:S(2)}, u32[]{:S(2)}) %collective-permute-start.13) | collective-permute-done | bytes 262176 | tf_op jit(solution)/shard_map/ppermute | solution.py:33
  123.1 2.2 %collective-permute-start.14 = (bf16[64,1024]{1,0:T(8,128)(2,1)S(1)}, bf16[64,1024]{1,0:T(8,128)(2,1)S(1)}, u32[]{:S(2)}, u32[]{:S(2)}) collective-permute-start(bf16[64,1024]{1,0:T(8,128)(2,1)S(1)} %shard_map.60), channel_id=1, source_target_pairs={{0,6},{1,3},{2,4},{3,1},{4,2},{5,7},{6,0},{7,5},{8,14},{9,11},{10,... | collective-permute-start | bytes 393224 | tf_op jit(solution)/shard_map/ppermute | solution.py:33
  125.3 2.3 %collective-permute-done.18.came.came1 = bf16[2,64,1024]{2,1,0:T(8,128)(2,1)S(1)} collective-permute-done((bf16[2,64,1024]{2,1,0:T(8,128)(2,1)S(1)}, bf16[2,64,1024]{2,1,0:T(8,128)(2,1)S(1)}, u32[]{:S(2)}, u32[]{:S(2)}) %collective-permute-start.18) | collective-permute-done | bytes 262176 | tf_op jit(solution)/shard_map/ppermute | solution.py:33
  127.6 1.9 %collective-permute-start.19 = (bf16[64,1024]{1,0:T(8,128)(2,1)S(1)}, bf16[64,1024]{1,0:T(8,128)(2,1)S(1)}, u32[]{:S(2)}, u32[]{:S(2)}) collective-permute-start(bf16[64,1024]{1,0:T(8,128)(2,1)S(1)} %shard_map.64), channel_id=1, source_target_pairs={{0,6},{1,3},{2,4},{3,1},{4,2},{5,7},{6,0},{7,5},{8,14},{9,11},{10,... | collective-permute-start | bytes 393224 | tf_op jit(solution)/shard_map/ppermute | solution.py:33
  129.6 3.8 %collective-permute-done.19.late1 = bf16[64,1024]{1,0:T(8,128)(2,1)S(1)} collective-permute-done((bf16[64,1024]{1,0:T(8,128)(2,1)S(1)}, bf16[64,1024]{1,0:T(8,128)(2,1)S(1)}, u32[]{:S(2)}, u32[]{:S(2)}) %collective-permute-start.19) | collective-permute-done | bytes 131104 | tf_op jit(solution)/shard_map/ppermute | solution.py:33
  (36 shorter events, 6.2 us)
Async XLA Ops:
  0.0 90.8 %copy-start = (bf16[512,2048]{1,0:T(8,128)(2,1)S(1)}, bf16[512,2048]{1,0:T(8,128)(2,1)}, u32[]{:S(2)}) copy-start(bf16[512,2048]{1,0:T(8,128)(2,1)} %tokens.1) | copy-start | bytes 6291460
  0.0 9.9 %collective-permute-start = (bf16[1,32,512]{2,1,0:T(8,128)(2,1)}, bf16[1,32,512]{2,1,0:T(8,128)(2,1)S(1)}, u32[]{:S(2)}, u32[]{:S(2)}) collective-permute-start(bf16[1,32,512]{2,1,0:T(8,128)(2,1)} %bitcast.5), channel_id=1, source_target_pairs={{32,0},{33,1},{40,8},{41,9},{48,16},{49,17},{56,24},{57,25},{0,32}... | collective-permute-start | bytes 98312 | tf_op jit(solution)/shard_map/ppermute | solution.py:25
  8.4 0.8 copy-start.1
  9.2 0.8 copy-start.2
  9.9 80.9 %copy-start.3 = (f32[2048]{0:T(1024)S(1)}, f32[2048]{0:T(1024)}, u32[]{:S(2)}) copy-start(f32[2048]{0:T(1024)} %param.5) | copy-start | bytes 24580
  10.0 19.8 %collective-permute-start.1 = (bf16[2,32,512]{2,1,0:T(8,128)(2,1)S(1)}, bf16[2,32,512]{2,1,0:T(8,128)(2,1)S(1)}, u32[]{:S(2)}, u32[]{:S(2)}) collective-permute-start(bf16[2,32,512]{2,1,0:T(8,128)(2,1)S(1)} %shard_map.48.a), channel_id=1, source_target_pairs={{256,0},{769,1},{320,64},{833,65},{384,128},{897,129},{448,192},{9... | collective-permute-start | bytes 196616 | tf_op jit(solution)/shard_map/ppermute | solution.py:25
  29.8 27.6 %collective-permute-start.2 = (bf16[4,32,512]{2,1,0:T(8,128)(2,1)S(1)}, bf16[4,32,512]{2,1,0:T(8,128)(2,1)S(1)}, u32[]{:S(2)}, u32[]{:S(2)}) collective-permute-start(bf16[4,32,512]{2,1,0:T(8,128)(2,1)S(1)} %shard_map.49.a), channel_id=1, source_target_pairs={{16,0},{49,1},{24,8},{57,9},{32,16},{1,17},{40,24},{9,25},{48,32},... | collective-permute-start | bytes 393224 | tf_op jit(solution)/shard_map/ppermute | solution.py:25
  34.2 8.8 %collective-permute-start.7 = (bf16[1,32,512]{2,1,0:T(8,128)(2,1)}, bf16[1,32,512]{2,1,0:T(8,128)(2,1)S(1)}, u32[]{:S(2)}, u32[]{:S(2)}) collective-permute-start(bf16[1,32,512]{2,1,0:T(8,128)(2,1)} %bitcast.7), channel_id=1, source_target_pairs={{256,0},{769,1},{320,64},{833,65},{384,128},{897,129},{448,192},{9... | collective-permute-start | bytes 98312 | tf_op jit(solution)/shard_map/ppermute | solution.py:25
  42.9 8.9 %collective-permute-start.8 = (bf16[2,32,512]{2,1,0:T(8,128)(2,1)S(1)}, bf16[2,32,512]{2,1,0:T(8,128)(2,1)S(1)}, u32[]{:S(2)}, u32[]{:S(2)}) collective-permute-start(bf16[2,32,512]{2,1,0:T(8,128)(2,1)S(1)} %shard_map.53.a), channel_id=1, source_target_pairs={{32,0},{33,1},{40,8},{41,9},{48,16},{49,17},{56,24},{57,25},{0,32}... | collective-permute-start | bytes 196616 | tf_op jit(solution)/shard_map/ppermute | solution.py:25
  51.9 11.3 %collective-permute-start.9 = (bf16[4,32,512]{2,1,0:T(8,128)(2,1)S(1)}, bf16[4,32,512]{2,1,0:T(8,128)(2,1)S(1)}, u32[]{:S(2)}, u32[]{:S(2)}) collective-permute-start(bf16[4,32,512]{2,1,0:T(8,128)(2,1)S(1)} %shard_map.54.a), channel_id=1, source_target_pairs={{128,0},{897,1},{192,64},{961,65},{256,128},{1,129},{320,192},{65,... | collective-permute-start | bytes 393224 | tf_op jit(solution)/shard_map/ppermute | solution.py:25
  57.5 10.9 %collective-permute-start.3 = (bf16[8,32,512]{2,1,0:T(8,128)(2,1)S(1)}, bf16[8,32,512]{2,1,0:T(8,128)(2,1)S(1)}, u32[]{:S(2)}, u32[]{:S(2)}) collective-permute-start(bf16[8,32,512]{2,1,0:T(8,128)(2,1)S(1)} %shard_map.50.a), channel_id=1, source_target_pairs={{128,0},{897,1},{192,64},{961,65},{256,128},{1,129},{320,192},{65,... | collective-permute-start | bytes 786440 | tf_op jit(solution)/shard_map/ppermute | solution.py:25
  63.2 12.0 %collective-permute-start.10 = (bf16[8,32,512]{2,1,0:T(8,128)(2,1)S(1)}, bf16[8,32,512]{2,1,0:T(8,128)(2,1)S(1)}, u32[]{:S(2)}, u32[]{:S(2)}) collective-permute-start(bf16[8,32,512]{2,1,0:T(8,128)(2,1)S(1)} %shard_map.55.a), channel_id=1, source_target_pairs={{16,0},{49,1},{24,8},{57,9},{32,16},{1,17},{40,24},{9,25},{48,32},... | collective-permute-start | bytes 786440 | tf_op jit(solution)/shard_map/ppermute | solution.py:25
  68.4 12.7 %collective-permute-start.4 = (bf16[16,32,512]{2,1,0:T(8,128)(2,1)S(1)}, bf16[16,32,512]{2,1,0:T(8,128)(2,1)S(1)}, u32[]{:S(2)}, u32[]{:S(2)}) collective-permute-start(bf16[16,32,512]{2,1,0:T(8,128)(2,1)S(1)} %shard_map.51.u0), channel_id=1, source_target_pairs={{64,0},{961,1},{128,64},{1,65},{192,128},{65,129},{256,192},{129,1... | collective-permute-start | bytes 1572872 | tf_op jit(solution)/shard_map/ppermute | solution.py:25
  75.2 13.6 %collective-permute-start.11 = (bf16[16,32,512]{2,1,0:T(8,128)(2,1)S(1)}, bf16[16,32,512]{2,1,0:T(8,128)(2,1)S(1)}, u32[]{:S(2)}, u32[]{:S(2)}) collective-permute-start(bf16[16,32,512]{2,1,0:T(8,128)(2,1)S(1)} %shard_map.56.d0), channel_id=1, source_target_pairs={{8,0},{57,1},{16,8},{1,9},{24,16},{9,17},{32,24},{17,25},{40,32},{... | collective-permute-start | bytes 1572872 | tf_op jit(solution)/shard_map/ppermute | solution.py:25
  77.6 15.4 %collective-permute-start.5 = (bf16[16,32,512]{2,1,0:T(8,128)(2,1)S(1)}, bf16[16,32,512]{2,1,0:T(8,128)(2,1)S(1)}, u32[]{:S(2)}, u32[]{:S(2)}) collective-permute-start(bf16[16,32,512]{2,1,0:T(8,128)(2,1)S(1)} %shard_map.51.u0), channel_id=1, source_target_pairs={{8,0},{57,1},{16,8},{1,9},{24,16},{9,17},{32,24},{17,25},{40,32},{... | collective-permute-start | bytes 1572872 | tf_op jit(solution)/shard_map/ppermute | solution.py:25
  81.1 16.5 %collective-permute-start.6 = (bf16[16,32,512]{2,1,0:T(8,128)(2,1)S(1)}, bf16[16,32,512]{2,1,0:T(8,128)(2,1)S(1)}, u32[]{:S(2)}, u32[]{:S(2)}) collective-permute-start(bf16[16,32,512]{2,1,0:T(8,128)(2,1)S(1)} %collective-permute-done.4.uz), channel_id=1, source_target_pairs={{8,0},{57,1},{16,8},{1,9},{24,16},{9,17},{32,24},{17,25},{40,32},{... | collective-permute-start | bytes 1572872 | tf_op jit(solution)/shard_map/ppermute | solution.py:25
  84.1 24.9 %collective-permute-start.15 = (bf16[16,32,512]{2,1,0:T(8,128)(2,1)S(1)}, bf16[16,32,512]{2,1,0:T(8,128)(2,1)S(1)}, u32[]{:S(2)}, u32[]{:S(2)}) collective-permute-start(bf16[16,32,512]{2,1,0:T(8,128)(2,1)S(1)} %shard_map.56.d0), channel_id=1, source_target_pairs={{64,0},{961,1},{128,64},{1,65},{192,128},{65,129},{256,192},{129,1... | collective-permute-start | bytes 1572872 | tf_op jit(solution)/shard_map/ppermute | solution.py:25
  88.9 20.2 %collective-permute-start.16 = (bf16[16,32,512]{2,1,0:T(8,128)(2,1)S(1)}, bf16[16,32,512]{2,1,0:T(8,128)(2,1)S(1)}, u32[]{:S(2)}, u32[]{:S(2)}) collective-permute-start(bf16[16,32,512]{2,1,0:T(8,128)(2,1)S(1)} %collective-permute-done.11.dy), channel_id=1, source_target_pairs={{64,0},{961,1},{128,64},{1,65},{192,128},{65,129},{256,192},{129,1... | collective-permute-start | bytes 1572872 | tf_op jit(solution)/shard_map/ppermute | solution.py:25
  100.4 14.2 %collective-permute-start.12 = (bf16[256,1024]{1,0:T(8,128)(2,1)S(1)}, bf16[256,1024]{1,0:T(8,128)(2,1)S(1)}, u32[]{:S(2)}, u32[]{:S(2)}) collective-permute-start(bf16[256,1024]{1,0:T(8,128)(2,1)S(1)} %get-tuple-element.22), channel_id=1, source_target_pairs={{0,1},{1,0},{2,3},{3,2},{4,5},{5,4},{6,7},{7,6},{8,9},{9,8},{10,11... | collective-permute-start | bytes 1572872 | tf_op jit(solution)/shard_map/ppermute | solution.py:233
  110.2 8.9 %collective-permute-start.17 = (bf16[256,1024]{1,0:T(8,128)(2,1)S(1)}, bf16[256,1024]{1,0:T(8,128)(2,1)S(1)}, u32[]{:S(2)}, u32[]{:S(2)}) collective-permute-start(bf16[256,1024]{1,0:T(8,128)(2,1)S(1)} %get-tuple-element.26), channel_id=1, source_target_pairs={{0,1},{1,0},{2,3},{3,2},{4,5},{5,4},{6,7},{7,6},{8,9},{9,8},{10,11... | collective-permute-start | bytes 1572872 | tf_op jit(solution)/shard_map/ppermute | solution.py:233
  114.7 8.3 %collective-permute-start.13 = (bf16[2,64,1024]{2,1,0:T(8,128)(2,1)S(1)}, bf16[2,64,1024]{2,1,0:T(8,128)(2,1)S(1)}, u32[]{:S(2)}, u32[]{:S(2)}) collective-permute-start(bf16[2,64,1024]{2,1,0:T(8,128)(2,1)S(1)} %get-tuple-element.24), channel_id=1, source_target_pairs={{0,2},{1,7},{2,0},{3,5},{4,6},{5,3},{6,4},{7,1},{8,10},{9,15},{10,... | collective-permute-start | bytes 786440 | tf_op jit(solution)/shard_map/ppermute | solution.py:33
  119.3 8.3 %collective-permute-start.18 = (bf16[2,64,1024]{2,1,0:T(8,128)(2,1)S(1)}, bf16[2,64,1024]{2,1,0:T(8,128)(2,1)S(1)}, u32[]{:S(2)}, u32[]{:S(2)}) collective-permute-start(bf16[2,64,1024]{2,1,0:T(8,128)(2,1)S(1)} %get-tuple-element.28), channel_id=1, source_target_pairs={{0,2},{1,7},{2,0},{3,5},{4,6},{5,3},{6,4},{7,1},{8,10},{9,15},{10,... | collective-permute-start | bytes 786440 | tf_op jit(solution)/shard_map/ppermute | solution.py:33
  123.1 6.5 %collective-permute-start.14 = (bf16[64,1024]{1,0:T(8,128)(2,1)S(1)}, bf16[64,1024]{1,0:T(8,128)(2,1)S(1)}, u32[]{:S(2)}, u32[]{:S(2)}) collective-permute-start(bf16[64,1024]{1,0:T(8,128)(2,1)S(1)} %shard_map.60), channel_id=1, source_target_pairs={{0,6},{1,3},{2,4},{3,1},{4,2},{5,7},{6,0},{7,5},{8,14},{9,11},{10,... | collective-permute-start | bytes 393224 | tf_op jit(solution)/shard_map/ppermute | solution.py:33
  127.6 5.7 %collective-permute-start.19 = (bf16[64,1024]{1,0:T(8,128)(2,1)S(1)}, bf16[64,1024]{1,0:T(8,128)(2,1)S(1)}, u32[]{:S(2)}, u32[]{:S(2)}) collective-permute-start(bf16[64,1024]{1,0:T(8,128)(2,1)S(1)} %shard_map.64), channel_id=1, source_target_pairs={{0,6},{1,3},{2,4},{3,1},{4,2},{5,7},{6,0},{7,5},{8,14},{9,11},{10,... | collective-permute-start | bytes 393224 | tf_op jit(solution)/shard_map/ppermute | solution.py:33

commit v6 on v5

--- a/solution.py
+++ b/solution.py
@@ -105,11 +105,11 @@
         whole[pl.ds(pl.multiple_of(at * 32, 32), 32), :] = piece[j]
 
 
-def down_product(hidden, rows, down, out):
+def down_product(hidden, rows, down, out, part):
     @pl.loop(0, 4)
     def _(n):
         columns = pl.ds(pl.multiple_of(n * 256, 256), 256)
-        out[:, columns] = lax.dot_general(
+        out[part, :, columns] = lax.dot_general(
             hidden[rows, :],
             down[columns, :],
             (((1,), (1,)), ((), ())),
@@ -142,17 +142,18 @@
 def early_kernel(hidden, d0, dy, theirs, down):
     place(d0, offsets(DOWN_STEPS), down, True)
     place(dy, shifted(DOWN_STEPS, 0, 1), down, True)
-    down_product(hidden, THEIRS, down, theirs)
-
-
-def late_kernel(hidden, dz, dyz, theirs, down):
+    down_product(hidden, THEIRS, down, theirs, 0)
+
+
+def late_kernel(hidden, dz, dyz, theirs_in, theirs, down):
     place(dz, shifted(DOWN_STEPS, 1, 0), down, True)
     place(dyz, shifted(DOWN_STEPS, 1, 1), down, True)
-    down_product(hidden, THEIRS, down, theirs)
-
-
-def own_kernel(hidden, down, own):
-    down_product(hidden, OWN, down, own)
+    down_product(hidden, THEIRS, down, theirs, 1)
+
+
+def own_kernel(hidden, first, second, own):
+    down_product(hidden, OWN, first, own, 0)
+    down_product(hidden, OWN, second, own, 1)
 
 
 def add_kernel(own, beside, keep, send):
@@ -165,8 +166,10 @@
         (keep, 1, x ^ second),
     ):
         rows = pl.ds(pl.multiple_of(chunk * 64, 64), 64)
-        total = own[rows].astype(jnp.float32) + beside[rows].astype(jnp.float32)
-        out[k] = total.astype(jnp.bfloat16)
+        for part in range(2):
+            total = own[part, rows].astype(jnp.float32)
+            total = total + beside[part, rows].astype(jnp.float32)
+            out[k, part] = total.astype(jnp.bfloat16)
 
 
 def pass_kernel(keep, came, out):
@@ -174,17 +177,16 @@
     out[...] = total.astype(jnp.bfloat16)
 
 
-def last_kernel(residual, keep0, came0, late0, keep1, came1, late1, out):
+def last_kernel(residual, keep, came, late, out):
     odd = lax.axis_index("z") & 1
-    for part, terms in ((0, (keep0, came0, late0)), (1, (keep1, came1, late1))):
+    for part in range(2):
         for k in range(4):
             at = (2 * k + (odd ^ part)) * 256
             columns = pl.ds(pl.multiple_of(at, 256), 256)
             here = slice(k * 256, (k + 1) * 256)
             total = residual[:, columns].astype(jnp.float32)
-            keep, came, late = terms
             for term in (keep.at[0], came.at[0], late):
-                total = total + term[:, here].astype(jnp.float32)
+                total = total + term[part, :, here].astype(jnp.float32)
             out[:, columns] = total.astype(jnp.bfloat16)
 
 
@@ -206,13 +208,13 @@
     return (up, up_z, up_y, up_zy), (down, down_y, down_z, down_yz)
 
 
-def over_tp(beside, own):
-    two = bf16(2, 64, 1024)
+def over_tp(beside, own, residual):
+    two = bf16(2, 2, 64, 1024)
     keep, send = kernel_call(add_kernel, (two, two), 2)(own, beside)
     came = between_x(send, 1, 3)
-    passed = kernel_call(pass_kernel, bf16(64, 1024), 2)(keep, came)
+    passed = kernel_call(pass_kernel, bf16(2, 64, 1024), 2)(keep, came)
     late = between_x(passed, 3, 1)
-    return keep, came, late
+    return kernel_call(last_kernel, bf16(64, 2048), 4)(residual, keep, came, late)
 
 
 def shards(tokens, norm_gain, up_weight, down_weight):
@@ -223,17 +225,20 @@
     hidden = kernel_call(
         up_kernel, bf16(512, 512), 5, scratch=((2048, 512),), mib=12, flops=2**30
     )(normed, *up)
-    out, rows = bf16(256, 1024), bf16(1024, 512)
-    trades = []
-    for part, kernel in ((0, early_kernel), (1, late_kernel)):
-        pieces = down[2 * part : 2 * part + 2]
-        theirs, placed = kernel_call(kernel, (out, rows), 3, flops=2**28)(
-            hidden, *pieces
-        )
-        beside = lax.ppermute(theirs, "core", [(0, 1), (1, 0)])
-        own = kernel_call(own_kernel, out, 2, flops=2**28)(hidden, placed)
-        trades += over_tp(beside, own)
-    return kernel_call(last_kernel, bf16(64, 2048), 7)(residual, *trades)
+    out, rows = bf16(2, 256, 1024), bf16(1024, 512)
+    theirs, first = kernel_call(early_kernel, (out, rows), 3, flops=2**28)(
+        hidden, *down[:2]
+    )
+    theirs, second = kernel_call(
+        late_kernel,
+        (out, rows),
+        4,
+        flops=2**28,
+        input_output_aliases={3: 0},
+    )(hidden, *down[2:], theirs)
+    beside = lax.ppermute(theirs, "core", [(0, 1), (1, 0)])
+    own = kernel_call(own_kernel, out, 3, flops=2**29)(hidden, first, second)
+    return over_tp(beside, own, residual)
 
 
 def solution(mesh):

time: 136 us -> 136 us (level)
  waiting for transfers between devices: 36.4 us -> 43.1 us
  starting transfers between devices: 86.3 us -> 80.1 us
    ppermute x4 -> x2, waiting for transfers between devices: 7.74 us -> 11.9 us  [between_x(): return lax.ppermute(array, ('x', 'core'), pairs)]
    ppermute x4 -> x2, starting transfers between devices: 10.6 us -> 6.59 us  [between_x(): return lax.ppermute(array, ('x', 'core'), pairs)]
    ppermute x14, waiting for transfers between devices: 28.7 us -> 31 us  [from_side(): return lax.ppermute(array, names, pairs)]
    ppermute x2 -> x1, starting transfers between devices: 10.9 us -> 8.59 us  [shards(): beside = lax.ppermute(theirs, 'core', [(0, 1), (1, 0)])]
    pallas_call x7 -> x5, Pallas kernels: 5.4 us -> 5.36 us  [the longest x1 2.11 us: shards(): own = kernel_call(own_kernel, out, 3, flops=2 ** 29)(hidden, first, second)]
  transfers between devices with their start and end apart: 20 -> 17, of which waited for: 9 -> 10; matrix products, arithmetic and copies ran while one was open for 0% -> 0% of each run, Pallas kernels for 6% -> 5%
where the time goes in v6:
time: 136 us; the launch traced here: 134 us
  starting transfers between devices  80.1 us (59%)
  waiting for transfers between devices  43.1 us (32%)
  Pallas kernels  9.47 us (7%)
  local copies, waits for them, and re-layouts  1.53 us (1%)
    ppermute x14, starting transfers between devices, from_side(): return lax.ppermute(array, names, pairs)  64.9 us
    ppermute x14, waiting for transfers between devices, from_side(): return lax.ppermute(array, names, pairs)  31 us
    ppermute x2, waiting for transfers between devices, between_x(): return lax.ppermute(array, ('x', 'core'), pairs)  11.9 us
    ppermute x1, starting transfers between devices, shards(): beside = lax.ppermute(theirs, 'core', [(0, 1), (1, 0)])  8.59 us
    ppermute x2, starting transfers between devices, between_x(): return lax.ppermute(array, ('x', 'core'), pairs)  6.59 us
  transfers between devices with their start and end apart: 17, of which 10 were waited for; matrix products, arithmetic and copies ran while one was open for 0% of the time, Pallas kernels for 5%

profile of v6, /device:TPU:1, one launch (start us, length us, event | category | flops | bytes accessed | tf_op | source)
XLA Modules:
  0.0 134.4 jit_solution(3980365074334854440)
XLA Ops:
  0.0 8.4 %collective-permute-start = (bf16[1,32,512]{2,1,0:T(8,128)(2,1)}, bf16[1,32,512]{2,1,0:T(8,128)(2,1)S(1)}, u32[]{:S(2)}, u32[]{:S(2)}) collective-permute-start(bf16[1,32,512]{2,1,0:T(8,128)(2,1)} %bitcast.5), channel_id=1, source_target_pairs={{32,0},{33,1},{40,8},{41,9},{48,16},{49,17},{56,24},{57,25},{0,32}... | collective-permute-start | bytes 98312 | tf_op jit(solution)/shard_map/ppermute | solution.py:25
  10.0 10.6 %collective-permute-start.1 = (bf16[2,32,512]{2,1,0:T(8,128)(2,1)S(1)}, bf16[2,32,512]{2,1,0:T(8,128)(2,1)S(1)}, u32[]{:S(2)}, u32[]{:S(2)}) collective-permute-start(bf16[2,32,512]{2,1,0:T(8,128)(2,1)S(1)} %shard_map.48.a), channel_id=1, source_target_pairs={{256,0},{769,1},{320,64},{833,65},{384,128},{897,129},{448,192},{9... | collective-permute-start | bytes 196616 | tf_op jit(solution)/shard_map/ppermute | solution.py:25
  20.6 9.2 %collective-permute-done.1.b = bf16[2,32,512]{2,1,0:T(8,128)(2,1)S(1)} collective-permute-done((bf16[2,32,512]{2,1,0:T(8,128)(2,1)S(1)}, bf16[2,32,512]{2,1,0:T(8,128)(2,1)S(1)}, u32[]{:S(2)}, u32[]{:S(2)}) %collective-permute-start.1) | collective-permute-done | bytes 65568 | tf_op jit(solution)/shard_map/ppermute | solution.py:25
  29.8 4.4 %collective-permute-start.2 = (bf16[4,32,512]{2,1,0:T(8,128)(2,1)S(1)}, bf16[4,32,512]{2,1,0:T(8,128)(2,1)S(1)}, u32[]{:S(2)}, u32[]{:S(2)}) collective-permute-start(bf16[4,32,512]{2,1,0:T(8,128)(2,1)S(1)} %shard_map.49.a), channel_id=1, source_target_pairs={{16,0},{49,1},{24,8},{57,9},{32,16},{1,17},{40,24},{9,25},{48,32},... | collective-permute-start | bytes 393224 | tf_op jit(solution)/shard_map/ppermute | solution.py:25
  34.2 2.8 %collective-permute-start.7 = (bf16[1,32,512]{2,1,0:T(8,128)(2,1)}, bf16[1,32,512]{2,1,0:T(8,128)(2,1)S(1)}, u32[]{:S(2)}, u32[]{:S(2)}) collective-permute-start(bf16[1,32,512]{2,1,0:T(8,128)(2,1)} %bitcast.7), channel_id=1, source_target_pairs={{256,0},{769,1},{320,64},{833,65},{384,128},{897,129},{448,192},{9... | collective-permute-start | bytes 98312 | tf_op jit(solution)/shard_map/ppermute | solution.py:25
  37.0 6.0 %collective-permute-done.7.b = bf16[1,32,512]{2,1,0:T(8,128)(2,1)S(1)} collective-permute-done((bf16[1,32,512]{2,1,0:T(8,128)(2,1)}, bf16[1,32,512]{2,1,0:T(8,128)(2,1)S(1)}, u32[]{:S(2)}, u32[]{:S(2)}) %collective-permute-start.7) | collective-permute-done | bytes 32800 | tf_op jit(solution)/shard_map/ppermute | solution.py:25
  42.9 5.2 %collective-permute-start.8 = (bf16[2,32,512]{2,1,0:T(8,128)(2,1)S(1)}, bf16[2,32,512]{2,1,0:T(8,128)(2,1)S(1)}, u32[]{:S(2)}, u32[]{:S(2)}) collective-permute-start(bf16[2,32,512]{2,1,0:T(8,128)(2,1)S(1)} %shard_map.53.a), channel_id=1, source_target_pairs={{32,0},{33,1},{40,8},{41,9},{48,16},{49,17},{56,24},{57,25},{0,32}... | collective-permute-start | bytes 196616 | tf_op jit(solution)/shard_map/ppermute | solution.py:25
  48.2 3.7 %collective-permute-done.8.b = bf16[2,32,512]{2,1,0:T(8,128)(2,1)S(1)} collective-permute-done((bf16[2,32,512]{2,1,0:T(8,128)(2,1)S(1)}, bf16[2,32,512]{2,1,0:T(8,128)(2,1)S(1)}, u32[]{:S(2)}, u32[]{:S(2)}) %collective-permute-start.8) | collective-permute-done | bytes 65568 | tf_op jit(solution)/shard_map/ppermute | solution.py:25
  51.9 5.5 %collective-permute-start.9 = (bf16[4,32,512]{2,1,0:T(8,128)(2,1)S(1)}, bf16[4,32,512]{2,1,0:T(8,128)(2,1)S(1)}, u32[]{:S(2)}, u32[]{:S(2)}) collective-permute-start(bf16[4,32,512]{2,1,0:T(8,128)(2,1)S(1)} %shard_map.54.a), channel_id=1, source_target_pairs={{128,0},{897,1},{192,64},{961,65},{256,128},{1,129},{320,192},{65,... | collective-permute-start | bytes 393224 | tf_op jit(solution)/shard_map/ppermute | solution.py:25
  57.5 1.9 %collective-permute-start.3 = (bf16[8,32,512]{2,1,0:T(8,128)(2,1)S(1)}, bf16[8,32,512]{2,1,0:T(8,128)(2,1)S(1)}, u32[]{:S(2)}, u32[]{:S(2)}) collective-permute-start(bf16[8,32,512]{2,1,0:T(8,128)(2,1)S(1)} %shard_map.50.a), channel_id=1, source_target_pairs={{128,0},{897,1},{192,64},{961,65},{256,128},{1,129},{320,192},{65,... | collective-permute-start | bytes 786440 | tf_op jit(solution)/shard_map/ppermute | solution.py:25
  59.4 3.7 %collective-permute-done.9.b = bf16[4,32,512]{2,1,0:T(8,128)(2,1)S(1)} collective-permute-done((bf16[4,32,512]{2,1,0:T(8,128)(2,1)S(1)}, bf16[4,32,512]{2,1,0:T(8,128)(2,1)S(1)}, u32[]{:S(2)}, u32[]{:S(2)}) %collective-permute-start.9) | collective-permute-done | bytes 131104 | tf_op jit(solution)/shard_map/ppermute | solution.py:25
  63.2 5.2 %collective-permute-start.10 = (bf16[8,32,512]{2,1,0:T(8,128)(2,1)S(1)}, bf16[8,32,512]{2,1,0:T(8,128)(2,1)S(1)}, u32[]{:S(2)}, u32[]{:S(2)}) collective-permute-start(bf16[8,32,512]{2,1,0:T(8,128)(2,1)S(1)} %shard_map.55.a), channel_id=1, source_target_pairs={{16,0},{49,1},{24,8},{57,9},{32,16},{1,17},{40,24},{9,25},{48,32},... | collective-permute-start | bytes 786440 | tf_op jit(solution)/shard_map/ppermute | solution.py:25
  68.4 5.2 %collective-permute-start.4 = (bf16[16,32,512]{2,1,0:T(8,128)(2,1)S(1)}, bf16[16,32,512]{2,1,0:T(8,128)(2,1)S(1)}, u32[]{:S(2)}, u32[]{:S(2)}) collective-permute-start(bf16[16,32,512]{2,1,0:T(8,128)(2,1)S(1)} %shard_map.51.u0), channel_id=1, source_target_pairs={{64,0},{961,1},{128,64},{1,65},{192,128},{65,129},{256,192},{129,1... | collective-permute-start | bytes 1572872 | tf_op jit(solution)/shard_map/ppermute | solution.py:25
  73.7 1.5 %collective-permute-done.10.b = bf16[8,32,512]{2,1,0:T(8,128)(2,1)S(1)} collective-permute-done((bf16[8,32,512]{2,1,0:T(8,128)(2,1)S(1)}, bf16[8,32,512]{2,1,0:T(8,128)(2,1)S(1)}, u32[]{:S(2)}, u32[]{:S(2)}) %collective-permute-start.10) | collective-permute-done | bytes 262176 | tf_op jit(solution)/shard_map/ppermute | solution.py:25
  75.2 2.3 %collective-permute-start.11 = (bf16[16,32,512]{2,1,0:T(8,128)(2,1)S(1)}, bf16[16,32,512]{2,1,0:T(8,128)(2,1)S(1)}, u32[]{:S(2)}, u32[]{:S(2)}) collective-permute-start(bf16[16,32,512]{2,1,0:T(8,128)(2,1)S(1)} %shard_map.56.d0), channel_id=1, source_target_pairs={{8,0},{57,1},{16,8},{1,9},{24,16},{9,17},{32,24},{17,25},{40,32},{... | collective-permute-start | bytes 1572872 | tf_op jit(solution)/shard_map/ppermute | solution.py:25
  77.6 3.5 %collective-permute-start.5 = (bf16[16,32,512]{2,1,0:T(8,128)(2,1)S(1)}, bf16[16,32,512]{2,1,0:T(8,128)(2,1)S(1)}, u32[]{:S(2)}, u32[]{:S(2)}) collective-permute-start(bf16[16,32,512]{2,1,0:T(8,128)(2,1)S(1)} %shard_map.51.u0), channel_id=1, source_target_pairs={{8,0},{57,1},{16,8},{1,9},{24,16},{9,17},{32,24},{17,25},{40,32},{... | collective-permute-start | bytes 1572872 | tf_op jit(solution)/shard_map/ppermute | solution.py:25
  81.1 3.0 %collective-permute-start.6 = (bf16[16,32,512]{2,1,0:T(8,128)(2,1)S(1)}, bf16[16,32,512]{2,1,0:T(8,128)(2,1)S(1)}, u32[]{:S(2)}, u32[]{:S(2)}) collective-permute-start(bf16[16,32,512]{2,1,0:T(8,128)(2,1)S(1)} %collective-permute-done.4.uz), channel_id=1, source_target_pairs={{8,0},{57,1},{16,8},{1,9},{24,16},{9,17},{32,24},{17,25},{40,32},{... | collective-permute-start | bytes 1572872 | tf_op jit(solution)/shard_map/ppermute | solution.py:25
  84.1 4.7 %collective-permute-start.12 = (bf16[16,32,512]{2,1,0:T(8,128)(2,1)S(1)}, bf16[16,32,512]{2,1,0:T(8,128)(2,1)S(1)}, u32[]{:S(2)}, u32[]{:S(2)}) collective-permute-start(bf16[16,32,512]{2,1,0:T(8,128)(2,1)S(1)} %shard_map.56.d0), channel_id=1, source_target_pairs={{64,0},{961,1},{128,64},{1,65},{192,128},{65,129},{256,192},{129,1... | collective-permute-start | bytes 1572872 | tf_op jit(solution)/shard_map/ppermute | solution.py:25
  88.9 1.9 %collective-permute-start.13 = (bf16[16,32,512]{2,1,0:T(8,128)(2,1)S(1)}, bf16[16,32,512]{2,1,0:T(8,128)(2,1)S(1)}, u32[]{:S(2)}, u32[]{:S(2)}) collective-permute-start(bf16[16,32,512]{2,1,0:T(8,128)(2,1)S(1)} %collective-permute-done.11.dy), channel_id=1, source_target_pairs={{64,0},{961,1},{128,64},{1,65},{192,128},{65,129},{256,192},{129,1... | collective-permute-start | bytes 1572872 | tf_op jit(solution)/shard_map/ppermute | solution.py:25
  90.8 2.1 %shard_map.46 = (bf16[512,2048]{1,0:T(8,128)(2,1)S(1)}, bf16[64,2048]{1,0:T(8,128)(2,1)S(1)}) custom-call(bf16[512,2048]{1,0:T(8,128)(2,1)S(1)} %copy-done, f32[1,2048]{1,0:T(1,128)S(1)} %bitcast.9), custom_call_target="tpu_custom_call" | custom-call | flops 16777216 | bytes 1048576 | tf_op jit(solution)/shard_map/pallas_call | solution.py:222
  92.9 4.6 %collective-permute-done.6.uzy = bf16[16,32,512]{2,1,0:T(8,128)(2,1)S(1)} collective-permute-done((bf16[16,32,512]{2,1,0:T(8,128)(2,1)S(1)}, bf16[16,32,512]{2,1,0:T(8,128)(2,1)S(1)}, u32[]{:S(2)}, u32[]{:S(2)}) %collective-permute-start.6) | collective-permute-done | bytes 524320 | tf_op jit(solution)/shard_map/ppermute | solution.py:25
  97.6 1.6 %shard_map.52.hidden = bf16[512,512]{1,0:T(8,128)(2,1)S(1)} custom-call(bf16[512,2048]{1,0:T(8,128)(2,1)S(1)} %get-tuple-element.16.normed, bf16[16,32,512]{2,1,0:T(8,128)(2,1)S(1)} %shard_map.51.u0, bf16[16,32,512]{2,1,0:T(8,128)(2,1)S(1)} %collective-permute-done.4.uz, bf16[16,32,512]{2,1,0:T(8,128)(2,1)S(1)} %collective-permute-done.5.uy, ...), custom_call_target="tpu_custom_call" | custom-call | flops 1073741824 | bytes 1048576 | tf_op jit(solution)/shard_map/pallas_call | solution.py:225
  99.2 1.2 shard_map.57
  100.4 2.3 %collective-permute-done.13.dyz = bf16[16,32,512]{2,1,0:T(8,128)(2,1)S(1)} collective-permute-done((bf16[16,32,512]{2,1,0:T(8,128)(2,1)S(1)}, bf16[16,32,512]{2,1,0:T(8,128)(2,1)S(1)}, u32[]{:S(2)}, u32[]{:S(2)}) %collective-permute-start.13) | collective-permute-done | bytes 524320 | tf_op jit(solution)/shard_map/ppermute | solution.py:25
  102.7 1.1 shard_map.58
  103.9 8.6 %collective-permute-start.14 = (bf16[2,256,1024]{2,1,0:T(8,128)(2,1)S(1)}, bf16[2,256,1024]{2,1,0:T(8,128)(2,1)S(1)}, u32[]{:S(2)}, u32[]{:S(2)}) collective-permute-start(bf16[2,256,1024]{2,1,0:T(8,128)(2,1)S(1)} %get-tuple-element.22), channel_id=1, source_target_pairs={{0,1},{1,0},{2,3},{3,2},{4,5},{5,4},{6,7},{7,6},{8,9},{9,8},{10,11... | collective-permute-start | bytes 3145736 | tf_op jit(solution)/shard_map/ppermute | solution.py:239
  112.5 2.1 %shard_map.59.own = bf16[2,256,1024]{2,1,0:T(8,128)(2,1)S(1)} custom-call(bf16[512,512]{1,0:T(8,128)(2,1)S(1)} %shard_map.52.hidden, bf16[1024,512]{1,0:T(8,128)(2,1)S(1)} %get-tuple-element.19.first, bf16[1024,512]{1,0:T(8,128)(2,1)S(1)} %get-tuple-element.21.second), custom_call_target="tpu_custom_call" | custom-call | flops 536870912 | bytes 1048576 | tf_op jit(solution)/shard_map/pallas_call | solution.py:240
  115.0 4.4 %collective-permute-start.15 = (bf16[2,2,64,1024]{3,2,1,0:T(8,128)(2,1)S(1)}, bf16[2,2,64,1024]{3,2,1,0:T(8,128)(2,1)S(1)}, u32[]{:S(2)}, u32[]{:S(2)}) collective-permute-start(bf16[2,2,64,1024]{3,2,1,0:T(8,128)(2,1)S(1)} %get-tuple-element.24), channel_id=1, source_target_pairs={{0,2},{1,7},{2,0},{3,5},{4,6},{5,3},{6,4},{7,1},{8,10},{9,15},{10,... | collective-permute-start | bytes 1572872 | tf_op jit(solution)/shard_map/ppermute | solution.py:33
  119.4 6.7 %collective-permute-done.15.came = bf16[2,2,64,1024]{3,2,1,0:T(8,128)(2,1)S(1)} collective-permute-done((bf16[2,2,64,1024]{3,2,1,0:T(8,128)(2,1)S(1)}, bf16[2,2,64,1024]{3,2,1,0:T(8,128)(2,1)S(1)}, u32[]{:S(2)}, u32[]{:S(2)}) %collective-permute-start.15) | collective-permute-done | bytes 524320 | tf_op jit(solution)/shard_map/ppermute | solution.py:33
  126.2 2.2 %collective-permute-start.16 = (bf16[2,64,1024]{2,1,0:T(8,128)(2,1)S(1)}, bf16[2,64,1024]{2,1,0:T(8,128)(2,1)S(1)}, u32[]{:S(2)}, u32[]{:S(2)}) collective-permute-start(bf16[2,64,1024]{2,1,0:T(8,128)(2,1)S(1)} %shard_map.61), channel_id=1, source_target_pairs={{0,6},{1,3},{2,4},{3,1},{4,2},{5,7},{6,0},{7,5},{8,14},{9,11},{10,... | collective-permute-start | bytes 786440 | tf_op jit(solution)/shard_map/ppermute | solution.py:33
  128.4 5.2 %collective-permute-done.16.late = bf16[2,64,1024]{2,1,0:T(8,128)(2,1)S(1)} collective-permute-done((bf16[2,64,1024]{2,1,0:T(8,128)(2,1)S(1)}, bf16[2,64,1024]{2,1,0:T(8,128)(2,1)S(1)}, u32[]{:S(2)}, u32[]{:S(2)}) %collective-permute-start.16) | collective-permute-done | bytes 262176 | tf_op jit(solution)/shard_map/ppermute | solution.py:33
  133.6 0.9 shard_map.62
  (27 shorter events, 2.1 us)
Async XLA Ops:
  0.0 90.8 %copy-start = (bf16[512,2048]{1,0:T(8,128)(2,1)S(1)}, bf16[512,2048]{1,0:T(8,128)(2,1)}, u32[]{:S(2)}) copy-start(bf16[512,2048]{1,0:T(8,128)(2,1)} %tokens.1) | copy-start | bytes 6291460
  0.0 9.9 %collective-permute-start = (bf16[1,32,512]{2,1,0:T(8,128)(2,1)}, bf16[1,32,512]{2,1,0:T(8,128)(2,1)S(1)}, u32[]{:S(2)}, u32[]{:S(2)}) collective-permute-start(bf16[1,32,512]{2,1,0:T(8,128)(2,1)} %bitcast.5), channel_id=1, source_target_pairs={{32,0},{33,1},{40,8},{41,9},{48,16},{49,17},{56,24},{57,25},{0,32}... | collective-permute-start | bytes 98312 | tf_op jit(solution)/shard_map/ppermute | solution.py:25
  8.4 0.8 copy-start.1
  9.2 0.8 copy-start.2
  9.9 80.9 %copy-start.3 = (f32[2048]{0:T(1024)S(1)}, f32[2048]{0:T(1024)}, u32[]{:S(2)}) copy-start(f32[2048]{0:T(1024)} %param.5) | copy-start | bytes 24580
  10.0 19.8 %collective-permute-start.1 = (bf16[2,32,512]{2,1,0:T(8,128)(2,1)S(1)}, bf16[2,32,512]{2,1,0:T(8,128)(2,1)S(1)}, u32[]{:S(2)}, u32[]{:S(2)}) collective-permute-start(bf16[2,32,512]{2,1,0:T(8,128)(2,1)S(1)} %shard_map.48.a), channel_id=1, source_target_pairs={{256,0},{769,1},{320,64},{833,65},{384,128},{897,129},{448,192},{9... | collective-permute-start | bytes 196616 | tf_op jit(solution)/shard_map/ppermute | solution.py:25
  29.8 27.6 %collective-permute-start.2 = (bf16[4,32,512]{2,1,0:T(8,128)(2,1)S(1)}, bf16[4,32,512]{2,1,0:T(8,128)(2,1)S(1)}, u32[]{:S(2)}, u32[]{:S(2)}) collective-permute-start(bf16[4,32,512]{2,1,0:T(8,128)(2,1)S(1)} %shard_map.49.a), channel_id=1, source_target_pairs={{16,0},{49,1},{24,8},{57,9},{32,16},{1,17},{40,24},{9,25},{48,32},... | collective-permute-start | bytes 393224 | tf_op jit(solution)/shard_map/ppermute | solution.py:25
  34.2 8.8 %collective-permute-start.7 = (bf16[1,32,512]{2,1,0:T(8,128)(2,1)}, bf16[1,32,512]{2,1,0:T(8,128)(2,1)S(1)}, u32[]{:S(2)}, u32[]{:S(2)}) collective-permute-start(bf16[1,32,512]{2,1,0:T(8,128)(2,1)} %bitcast.7), channel_id=1, source_target_pairs={{256,0},{769,1},{320,64},{833,65},{384,128},{897,129},{448,192},{9... | collective-permute-start | bytes 98312 | tf_op jit(solution)/shard_map/ppermute | solution.py:25
  42.9 8.9 %collective-permute-start.8 = (bf16[2,32,512]{2,1,0:T(8,128)(2,1)S(1)}, bf16[2,32,512]{2,1,0:T(8,128)(2,1)S(1)}, u32[]{:S(2)}, u32[]{:S(2)}) collective-permute-start(bf16[2,32,512]{2,1,0:T(8,128)(2,1)S(1)} %shard_map.53.a), channel_id=1, source_target_pairs={{32,0},{33,1},{40,8},{41,9},{48,16},{49,17},{56,24},{57,25},{0,32}... | collective-permute-start | bytes 196616 | tf_op jit(solution)/shard_map/ppermute | solution.py:25
  51.9 11.3 %collective-permute-start.9 = (bf16[4,32,512]{2,1,0:T(8,128)(2,1)S(1)}, bf16[4,32,512]{2,1,0:T(8,128)(2,1)S(1)}, u32[]{:S(2)}, u32[]{:S(2)}) collective-permute-start(bf16[4,32,512]{2,1,0:T(8,128)(2,1)S(1)} %shard_map.54.a), channel_id=1, source_target_pairs={{128,0},{897,1},{192,64},{961,65},{256,128},{1,129},{320,192},{65,... | collective-permute-start | bytes 393224 | tf_op jit(solution)/shard_map/ppermute | solution.py:25
  57.5 10.9 %collective-permute-start.3 = (bf16[8,32,512]{2,1,0:T(8,128)(2,1)S(1)}, bf16[8,32,512]{2,1,0:T(8,128)(2,1)S(1)}, u32[]{:S(2)}, u32[]{:S(2)}) collective-permute-start(bf16[8,32,512]{2,1,0:T(8,128)(2,1)S(1)} %shard_map.50.a), channel_id=1, source_target_pairs={{128,0},{897,1},{192,64},{961,65},{256,128},{1,129},{320,192},{65,... | collective-permute-start | bytes 786440 | tf_op jit(solution)/shard_map/ppermute | solution.py:25
  63.2 12.0 %collective-permute-start.10 = (bf16[8,32,512]{2,1,0:T(8,128)(2,1)S(1)}, bf16[8,32,512]{2,1,0:T(8,128)(2,1)S(1)}, u32[]{:S(2)}, u32[]{:S(2)}) collective-permute-start(bf16[8,32,512]{2,1,0:T(8,128)(2,1)S(1)} %shard_map.55.a), channel_id=1, source_target_pairs={{16,0},{49,1},{24,8},{57,9},{32,16},{1,17},{40,24},{9,25},{48,32},... | collective-permute-start | bytes 786440 | tf_op jit(solution)/shard_map/ppermute | solution.py:25
  68.4 12.7 %collective-permute-start.4 = (bf16[16,32,512]{2,1,0:T(8,128)(2,1)S(1)}, bf16[16,32,512]{2,1,0:T(8,128)(2,1)S(1)}, u32[]{:S(2)}, u32[]{:S(2)}) collective-permute-start(bf16[16,32,512]{2,1,0:T(8,128)(2,1)S(1)} %shard_map.51.u0), channel_id=1, source_target_pairs={{64,0},{961,1},{128,64},{1,65},{192,128},{65,129},{256,192},{129,1... | collective-permute-start | bytes 1572872 | tf_op jit(solution)/shard_map/ppermute | solution.py:25
  75.2 13.6 %collective-permute-start.11 = (bf16[16,32,512]{2,1,0:T(8,128)(2,1)S(1)}, bf16[16,32,512]{2,1,0:T(8,128)(2,1)S(1)}, u32[]{:S(2)}, u32[]{:S(2)}) collective-permute-start(bf16[16,32,512]{2,1,0:T(8,128)(2,1)S(1)} %shard_map.56.d0), channel_id=1, source_target_pairs={{8,0},{57,1},{16,8},{1,9},{24,16},{9,17},{32,24},{17,25},{40,32},{... | collective-permute-start | bytes 1572872 | tf_op jit(solution)/shard_map/ppermute | solution.py:25
  77.6 15.4 %collective-permute-start.5 = (bf16[16,32,512]{2,1,0:T(8,128)(2,1)S(1)}, bf16[16,32,512]{2,1,0:T(8,128)(2,1)S(1)}, u32[]{:S(2)}, u32[]{:S(2)}) collective-permute-start(bf16[16,32,512]{2,1,0:T(8,128)(2,1)S(1)} %shard_map.51.u0), channel_id=1, source_target_pairs={{8,0},{57,1},{16,8},{1,9},{24,16},{9,17},{32,24},{17,25},{40,32},{... | collective-permute-start | bytes 1572872 | tf_op jit(solution)/shard_map/ppermute | solution.py:25
  81.1 16.5 %collective-permute-start.6 = (bf16[16,32,512]{2,1,0:T(8,128)(2,1)S(1)}, bf16[16,32,512]{2,1,0:T(8,128)(2,1)S(1)}, u32[]{:S(2)}, u32[]{:S(2)}) collective-permute-start(bf16[16,32,512]{2,1,0:T(8,128)(2,1)S(1)} %collective-permute-done.4.uz), channel_id=1, source_target_pairs={{8,0},{57,1},{16,8},{1,9},{24,16},{9,17},{32,24},{17,25},{40,32},{... | collective-permute-start | bytes 1572872 | tf_op jit(solution)/shard_map/ppermute | solution.py:25
  84.1 16.2 %collective-permute-start.12 = (bf16[16,32,512]{2,1,0:T(8,128)(2,1)S(1)}, bf16[16,32,512]{2,1,0:T(8,128)(2,1)S(1)}, u32[]{:S(2)}, u32[]{:S(2)}) collective-permute-start(bf16[16,32,512]{2,1,0:T(8,128)(2,1)S(1)} %shard_map.56.d0), channel_id=1, source_target_pairs={{64,0},{961,1},{128,64},{1,65},{192,128},{65,129},{256,192},{129,1... | collective-permute-start | bytes 1572872 | tf_op jit(solution)/shard_map/ppermute | solution.py:25
  88.9 13.9 %collective-permute-start.13 = (bf16[16,32,512]{2,1,0:T(8,128)(2,1)S(1)}, bf16[16,32,512]{2,1,0:T(8,128)(2,1)S(1)}, u32[]{:S(2)}, u32[]{:S(2)}) collective-permute-start(bf16[16,32,512]{2,1,0:T(8,128)(2,1)S(1)} %collective-permute-done.11.dy), channel_id=1, source_target_pairs={{64,0},{961,1},{128,64},{1,65},{192,128},{65,129},{256,192},{129,1... | collective-permute-start | bytes 1572872 | tf_op jit(solution)/shard_map/ppermute | solution.py:25
  103.9 10.9 %collective-permute-start.14 = (bf16[2,256,1024]{2,1,0:T(8,128)(2,1)S(1)}, bf16[2,256,1024]{2,1,0:T(8,128)(2,1)S(1)}, u32[]{:S(2)}, u32[]{:S(2)}) collective-permute-start(bf16[2,256,1024]{2,1,0:T(8,128)(2,1)S(1)} %get-tuple-element.22), channel_id=1, source_target_pairs={{0,1},{1,0},{2,3},{3,2},{4,5},{5,4},{6,7},{7,6},{8,9},{9,8},{10,11... | collective-permute-start | bytes 3145736 | tf_op jit(solution)/shard_map/ppermute | solution.py:239
  115.0 11.1 %collective-permute-start.15 = (bf16[2,2,64,1024]{3,2,1,0:T(8,128)(2,1)S(1)}, bf16[2,2,64,1024]{3,2,1,0:T(8,128)(2,1)S(1)}, u32[]{:S(2)}, u32[]{:S(2)}) collective-permute-start(bf16[2,2,64,1024]{3,2,1,0:T(8,128)(2,1)S(1)} %get-tuple-element.24), channel_id=1, source_target_pairs={{0,2},{1,7},{2,0},{3,5},{4,6},{5,3},{6,4},{7,1},{8,10},{9,15},{10,... | collective-permute-start | bytes 1572872 | tf_op jit(solution)/shard_map/ppermute | solution.py:33
  126.2 7.4 %collective-permute-start.16 = (bf16[2,64,1024]{2,1,0:T(8,128)(2,1)S(1)}, bf16[2,64,1024]{2,1,0:T(8,128)(2,1)S(1)}, u32[]{:S(2)}, u32[]{:S(2)}) collective-permute-start(bf16[2,64,1024]{2,1,0:T(8,128)(2,1)S(1)} %shard_map.61), channel_id=1, source_target_pairs={{0,6},{1,3},{2,4},{3,1},{4,2},{5,7},{6,0},{7,5},{8,14},{9,11},{10,... | collective-permute-start | bytes 786440 | tf_op jit(solution)/shard_map/ppermute | solution.py:33

commit v7 on v6

--- a/solution.py
+++ b/solution.py
@@ -156,24 +156,24 @@
     down_product(hidden, OWN, second, own, 1)
 
 
-def add_kernel(own, beside, keep, send):
+def add_kernel(own, beside, ahead, near, keep, hold):
     x, core = lax.axis_index("x"), lax.axis_index("core")
     first, second = 1 + 2 * core, 3 - 2 * core
-    for out, k, chunk in (
-        (send, 0, x ^ first),
-        (send, 1, x ^ 2),
-        (keep, 0, x),
-        (keep, 1, x ^ second),
+    for out, chunk in (
+        (ahead, x ^ 2),
+        (near, x ^ first),
+        (keep, x),
+        (hold, x ^ second),
     ):
         rows = pl.ds(pl.multiple_of(chunk * 64, 64), 64)
         for part in range(2):
             total = own[part, rows].astype(jnp.float32)
             total = total + beside[part, rows].astype(jnp.float32)
-            out[k, part] = total.astype(jnp.bfloat16)
-
-
-def pass_kernel(keep, came, out):
-    total = keep[1].astype(jnp.float32) + came[1].astype(jnp.float32)
+            out[part] = total.astype(jnp.bfloat16)
+
+
+def pass_kernel(hold, came, out):
+    total = hold[...].astype(jnp.float32) + came[...].astype(jnp.float32)
     out[...] = total.astype(jnp.bfloat16)
 
 
@@ -185,7 +185,7 @@
             columns = pl.ds(pl.multiple_of(at, 256), 256)
             here = slice(k * 256, (k + 1) * 256)
             total = residual[:, columns].astype(jnp.float32)
-            for term in (keep.at[0], came.at[0], late):
+            for term in (keep, came, late):
                 total = total + term[part, :, here].astype(jnp.float32)
             out[:, columns] = total.astype(jnp.bfloat16)
 
@@ -209,10 +209,11 @@
 
 
 def over_tp(beside, own, residual):
-    two = bf16(2, 2, 64, 1024)
-    keep, send = kernel_call(add_kernel, (two, two), 2)(own, beside)
-    came = between_x(send, 1, 3)
-    passed = kernel_call(pass_kernel, bf16(2, 64, 1024), 2)(keep, came)
+    piece = bf16(2, 64, 1024)
+    ahead, near, keep, hold = kernel_call(add_kernel, (piece,) * 4, 2)(own, beside)
+    through = between_x(ahead, 1, 3)
+    came = between_x(near, 1, 3)
+    passed = kernel_call(pass_kernel, piece, 2)(hold, through)
     late = between_x(passed, 3, 1)
     return kernel_call(last_kernel, bf16(64, 2048), 4)(residual, keep, came, late)
 

time: 136 us -> 134 us (0.985)
  waiting for transfers between devices: 43.1 us -> 38.2 us
  starting transfers between devices: 80.1 us -> 82.2 us
    ppermute x2 -> x3, waiting for transfers between devices: 11.9 us -> 7.02 us  [between_x(): return lax.ppermute(array, ('x', 'core'), pairs)]
    ppermute x2 -> x3, starting transfers between devices: 6.59 us -> 8.69 us  [between_x(): return lax.ppermute(array, ('x', 'core'), pairs)]
  transfers between devices with their start and end apart: 17 -> 18, of which waited for: 10 -> 11; matrix products, arithmetic and copies ran while one was open for 0% -> 0% of each run, Pallas kernels for 5% -> 5%
where the time goes in v7:
time: 134 us; the launch traced here: 132 us
  starting transfers between devices  82.2 us (61%)
  waiting for transfers between devices  38.2 us (29%)
  Pallas kernels  9.47 us (7%)
  local copies, waits for them, and re-layouts  1.53 us (1%)
    ppermute x14, starting transfers between devices, from_side(): return lax.ppermute(array, names, pairs)  64.9 us
    ppermute x14, waiting for transfers between devices, from_side(): return lax.ppermute(array, names, pairs)  31 us
    ppermute x3, starting transfers between devices, between_x(): return lax.ppermute(array, ('x', 'core'), pairs)  8.69 us
    ppermute x1, starting transfers between devices, shards(): beside = lax.ppermute(theirs, 'core', [(0, 1), (1, 0)])  8.59 us
    ppermute x3, waiting for transfers between devices, between_x(): return lax.ppermute(array, ('x', 'core'), pairs)  7.02 us
  transfers between devices with their start and end apart: 18, of which 11 were waited for; matrix products, arithmetic and copies ran while one was open for 0% of the time, Pallas kernels for 5%

profile of v7, /device:TPU:1, one launch (start us, length us, event | category | flops | bytes accessed | tf_op | source)
XLA Modules:
  0.0 131.6 jit_solution(12340807054605359011)
XLA Ops:
  0.0 8.4 %collective-permute-start = (bf16[1,32,512]{2,1,0:T(8,128)(2,1)}, bf16[1,32,512]{2,1,0:T(8,128)(2,1)S(1)}, u32[]{:S(2)}, u32[]{:S(2)}) collective-permute-start(bf16[1,32,512]{2,1,0:T(8,128)(2,1)} %bitcast.5), channel_id=1, source_target_pairs={{32,0},{33,1},{40,8},{41,9},{48,16},{49,17},{56,24},{57,25},{0,32}... | collective-permute-start | bytes 98312 | tf_op jit(solution)/shard_map/ppermute | solution.py:25
  10.0 10.6 %collective-permute-start.1 = (bf16[2,32,512]{2,1,0:T(8,128)(2,1)S(1)}, bf16[2,32,512]{2,1,0:T(8,128)(2,1)S(1)}, u32[]{:S(2)}, u32[]{:S(2)}) collective-permute-start(bf16[2,32,512]{2,1,0:T(8,128)(2,1)S(1)} %shard_map.48.a), channel_id=1, source_target_pairs={{256,0},{769,1},{320,64},{833,65},{384,128},{897,129},{448,192},{9... | collective-permute-start | bytes 196616 | tf_op jit(solution)/shard_map/ppermute | solution.py:25
  20.6 9.2 %collective-permute-done.1.b = bf16[2,32,512]{2,1,0:T(8,128)(2,1)S(1)} collective-permute-done((bf16[2,32,512]{2,1,0:T(8,128)(2,1)S(1)}, bf16[2,32,512]{2,1,0:T(8,128)(2,1)S(1)}, u32[]{:S(2)}, u32[]{:S(2)}) %collective-permute-start.1) | collective-permute-done | bytes 65568 | tf_op jit(solution)/shard_map/ppermute | solution.py:25
  29.8 4.4 %collective-permute-start.2 = (bf16[4,32,512]{2,1,0:T(8,128)(2,1)S(1)}, bf16[4,32,512]{2,1,0:T(8,128)(2,1)S(1)}, u32[]{:S(2)}, u32[]{:S(2)}) collective-permute-start(bf16[4,32,512]{2,1,0:T(8,128)(2,1)S(1)} %shard_map.49.a), channel_id=1, source_target_pairs={{16,0},{49,1},{24,8},{57,9},{32,16},{1,17},{40,24},{9,25},{48,32},... | collective-permute-start | bytes 393224 | tf_op jit(solution)/shard_map/ppermute | solution.py:25
  34.2 2.8 %collective-permute-start.7 = (bf16[1,32,512]{2,1,0:T(8,128)(2,1)}, bf16[1,32,512]{2,1,0:T(8,128)(2,1)S(1)}, u32[]{:S(2)}, u32[]{:S(2)}) collective-permute-start(bf16[1,32,512]{2,1,0:T(8,128)(2,1)} %bitcast.7), channel_id=1, source_target_pairs={{256,0},{769,1},{320,64},{833,65},{384,128},{897,129},{448,192},{9... | collective-permute-start | bytes 98312 | tf_op jit(solution)/shard_map/ppermute | solution.py:25
  37.0 6.0 %collective-permute-done.7.b = bf16[1,32,512]{2,1,0:T(8,128)(2,1)S(1)} collective-permute-done((bf16[1,32,512]{2,1,0:T(8,128)(2,1)}, bf16[1,32,512]{2,1,0:T(8,128)(2,1)S(1)}, u32[]{:S(2)}, u32[]{:S(2)}) %collective-permute-start.7) | collective-permute-done | bytes 32800 | tf_op jit(solution)/shard_map/ppermute | solution.py:25
  42.9 5.2 %collective-permute-start.8 = (bf16[2,32,512]{2,1,0:T(8,128)(2,1)S(1)}, bf16[2,32,512]{2,1,0:T(8,128)(2,1)S(1)}, u32[]{:S(2)}, u32[]{:S(2)}) collective-permute-start(bf16[2,32,512]{2,1,0:T(8,128)(2,1)S(1)} %shard_map.53.a), channel_id=1, source_target_pairs={{32,0},{33,1},{40,8},{41,9},{48,16},{49,17},{56,24},{57,25},{0,32}... | collective-permute-start | bytes 196616 | tf_op jit(solution)/shard_map/ppermute | solution.py:25
  48.2 3.7 %collective-permute-done.8.b = bf16[2,32,512]{2,1,0:T(8,128)(2,1)S(1)} collective-permute-done((bf16[2,32,512]{2,1,0:T(8,128)(2,1)S(1)}, bf16[2,32,512]{2,1,0:T(8,128)(2,1)S(1)}, u32[]{:S(2)}, u32[]{:S(2)}) %collective-permute-start.8) | collective-permute-done | bytes 65568 | tf_op jit(solution)/shard_map/ppermute | solution.py:25
  51.9 5.5 %collective-permute-start.9 = (bf16[4,32,512]{2,1,0:T(8,128)(2,1)S(1)}, bf16[4,32,512]{2,1,0:T(8,128)(2,1)S(1)}, u32[]{:S(2)}, u32[]{:S(2)}) collective-permute-start(bf16[4,32,512]{2,1,0:T(8,128)(2,1)S(1)} %shard_map.54.a), channel_id=1, source_target_pairs={{128,0},{897,1},{192,64},{961,65},{256,128},{1,129},{320,192},{65,... | collective-permute-start | bytes 393224 | tf_op jit(solution)/shard_map/ppermute | solution.py:25
  57.5 1.9 %collective-permute-start.3 = (bf16[8,32,512]{2,1,0:T(8,128)(2,1)S(1)}, bf16[8,32,512]{2,1,0:T(8,128)(2,1)S(1)}, u32[]{:S(2)}, u32[]{:S(2)}) collective-permute-start(bf16[8,32,512]{2,1,0:T(8,128)(2,1)S(1)} %shard_map.50.a), channel_id=1, source_target_pairs={{128,0},{897,1},{192,64},{961,65},{256,128},{1,129},{320,192},{65,... | collective-permute-start | bytes 786440 | tf_op jit(solution)/shard_map/ppermute | solution.py:25
  59.4 3.7 %collective-permute-done.9.b = bf16[4,32,512]{2,1,0:T(8,128)(2,1)S(1)} collective-permute-done((bf16[4,32,512]{2,1,0:T(8,128)(2,1)S(1)}, bf16[4,32,512]{2,1,0:T(8,128)(2,1)S(1)}, u32[]{:S(2)}, u32[]{:S(2)}) %collective-permute-start.9) | collective-permute-done | bytes 131104 | tf_op jit(solution)/shard_map/ppermute | solution.py:25
  63.2 5.2 %collective-permute-start.10 = (bf16[8,32,512]{2,1,0:T(8,128)(2,1)S(1)}, bf16[8,32,512]{2,1,0:T(8,128)(2,1)S(1)}, u32[]{:S(2)}, u32[]{:S(2)}) collective-permute-start(bf16[8,32,512]{2,1,0:T(8,128)(2,1)S(1)} %shard_map.55.a), channel_id=1, source_target_pairs={{16,0},{49,1},{24,8},{57,9},{32,16},{1,17},{40,24},{9,25},{48,32},... | collective-permute-start | bytes 786440 | tf_op jit(solution)/shard_map/ppermute | solution.py:25
  68.4 5.2 %collective-permute-start.4 = (bf16[16,32,512]{2,1,0:T(8,128)(2,1)S(1)}, bf16[16,32,512]{2,1,0:T(8,128)(2,1)S(1)}, u32[]{:S(2)}, u32[]{:S(2)}) collective-permute-start(bf16[16,32,512]{2,1,0:T(8,128)(2,1)S(1)} %shard_map.51.u0), channel_id=1, source_target_pairs={{64,0},{961,1},{128,64},{1,65},{192,128},{65,129},{256,192},{129,1... | collective-permute-start | bytes 1572872 | tf_op jit(solution)/shard_map/ppermute | solution.py:25
  73.7 1.5 %collective-permute-done.10.b = bf16[8,32,512]{2,1,0:T(8,128)(2,1)S(1)} collective-permute-done((bf16[8,32,512]{2,1,0:T(8,128)(2,1)S(1)}, bf16[8,32,512]{2,1,0:T(8,128)(2,1)S(1)}, u32[]{:S(2)}, u32[]{:S(2)}) %collective-permute-start.10) | collective-permute-done | bytes 262176 | tf_op jit(solution)/shard_map/ppermute | solution.py:25
  75.2 2.3 %collective-permute-start.11 = (bf16[16,32,512]{2,1,0:T(8,128)(2,1)S(1)}, bf16[16,32,512]{2,1,0:T(8,128)(2,1)S(1)}, u32[]{:S(2)}, u32[]{:S(2)}) collective-permute-start(bf16[16,32,512]{2,1,0:T(8,128)(2,1)S(1)} %shard_map.56.d0), channel_id=1, source_target_pairs={{8,0},{57,1},{16,8},{1,9},{24,16},{9,17},{32,24},{17,25},{40,32},{... | collective-permute-start | bytes 1572872 | tf_op jit(solution)/shard_map/ppermute | solution.py:25
  77.6 3.5 %collective-permute-start.5 = (bf16[16,32,512]{2,1,0:T(8,128)(2,1)S(1)}, bf16[16,32,512]{2,1,0:T(8,128)(2,1)S(1)}, u32[]{:S(2)}, u32[]{:S(2)}) collective-permute-start(bf16[16,32,512]{2,1,0:T(8,128)(2,1)S(1)} %shard_map.51.u0), channel_id=1, source_target_pairs={{8,0},{57,1},{16,8},{1,9},{24,16},{9,17},{32,24},{17,25},{40,32},{... | collective-permute-start | bytes 1572872 | tf_op jit(solution)/shard_map/ppermute | solution.py:25
  81.1 3.0 %collective-permute-start.6 = (bf16[16,32,512]{2,1,0:T(8,128)(2,1)S(1)}, bf16[16,32,512]{2,1,0:T(8,128)(2,1)S(1)}, u32[]{:S(2)}, u32[]{:S(2)}) collective-permute-start(bf16[16,32,512]{2,1,0:T(8,128)(2,1)S(1)} %collective-permute-done.4.uz), channel_id=1, source_target_pairs={{8,0},{57,1},{16,8},{1,9},{24,16},{9,17},{32,24},{17,25},{40,32},{... | collective-permute-start | bytes 1572872 | tf_op jit(solution)/shard_map/ppermute | solution.py:25
  84.1 4.7 %collective-permute-start.12 = (bf16[16,32,512]{2,1,0:T(8,128)(2,1)S(1)}, bf16[16,32,512]{2,1,0:T(8,128)(2,1)S(1)}, u32[]{:S(2)}, u32[]{:S(2)}) collective-permute-start(bf16[16,32,512]{2,1,0:T(8,128)(2,1)S(1)} %shard_map.56.d0), channel_id=1, source_target_pairs={{64,0},{961,1},{128,64},{1,65},{192,128},{65,129},{256,192},{129,1... | collective-permute-start | bytes 1572872 | tf_op jit(solution)/shard_map/ppermute | solution.py:25
  88.9 1.9 %collective-permute-start.13 = (bf16[16,32,512]{2,1,0:T(8,128)(2,1)S(1)}, bf16[16,32,512]{2,1,0:T(8,128)(2,1)S(1)}, u32[]{:S(2)}, u32[]{:S(2)}) collective-permute-start(bf16[16,32,512]{2,1,0:T(8,128)(2,1)S(1)} %collective-permute-done.11.dy), channel_id=1, source_target_pairs={{64,0},{961,1},{128,64},{1,65},{192,128},{65,129},{256,192},{129,1... | collective-permute-start | bytes 1572872 | tf_op jit(solution)/shard_map/ppermute | solution.py:25
  90.8 2.1 %shard_map.46 = (bf16[512,2048]{1,0:T(8,128)(2,1)S(1)}, bf16[64,2048]{1,0:T(8,128)(2,1)S(1)}) custom-call(bf16[512,2048]{1,0:T(8,128)(2,1)S(1)} %copy-done, f32[1,2048]{1,0:T(1,128)S(1)} %bitcast.9), custom_call_target="tpu_custom_call" | custom-call | flops 16777216 | bytes 1048576 | tf_op jit(solution)/shard_map/pallas_call | solution.py:223
  92.9 4.6 %collective-permute-done.6.uzy = bf16[16,32,512]{2,1,0:T(8,128)(2,1)S(1)} collective-permute-done((bf16[16,32,512]{2,1,0:T(8,128)(2,1)S(1)}, bf16[16,32,512]{2,1,0:T(8,128)(2,1)S(1)}, u32[]{:S(2)}, u32[]{:S(2)}) %collective-permute-start.6) | collective-permute-done | bytes 524320 | tf_op jit(solution)/shard_map/ppermute | solution.py:25
  97.6 1.6 %shard_map.52.hidden = bf16[512,512]{1,0:T(8,128)(2,1)S(1)} custom-call(bf16[512,2048]{1,0:T(8,128)(2,1)S(1)} %get-tuple-element.18.normed, bf16[16,32,512]{2,1,0:T(8,128)(2,1)S(1)} %shard_map.51.u0, bf16[16,32,512]{2,1,0:T(8,128)(2,1)S(1)} %collective-permute-done.4.uz, bf16[16,32,512]{2,1,0:T(8,128)(2,1)S(1)} %collective-permute-done.5.uy, ...), custom_call_target="tpu_custom_call" | custom-call | flops 1073741824 | bytes 1048576 | tf_op jit(solution)/shard_map/pallas_call | solution.py:226
  99.2 1.2 shard_map.57
  100.4 2.3 %collective-permute-done.13.dyz = bf16[16,32,512]{2,1,0:T(8,128)(2,1)S(1)} collective-permute-done((bf16[16,32,512]{2,1,0:T(8,128)(2,1)S(1)}, bf16[16,32,512]{2,1,0:T(8,128)(2,1)S(1)}, u32[]{:S(2)}, u32[]{:S(2)}) %collective-permute-start.13) | collective-permute-done | bytes 524320 | tf_op jit(solution)/shard_map/ppermute | solution.py:25
  103.9 8.6 %collective-permute-start.14 = (bf16[2,256,1024]{2,1,0:T(8,128)(2,1)S(1)}, bf16[2,256,1024]{2,1,0:T(8,128)(2,1)S(1)}, u32[]{:S(2)}, u32[]{:S(2)}) collective-permute-start(bf16[2,256,1024]{2,1,0:T(8,128)(2,1)S(1)} %get-tuple-element.24), channel_id=1, source_target_pairs={{0,1},{1,0},{2,3},{3,2},{4,5},{5,4},{6,7},{7,6},{8,9},{9,8},{10,11... | collective-permute-start | bytes 3145736 | tf_op jit(solution)/shard_map/ppermute | solution.py:240
  112.5 2.1 %shard_map.59.own = bf16[2,256,1024]{2,1,0:T(8,128)(2,1)S(1)} custom-call(bf16[512,512]{1,0:T(8,128)(2,1)S(1)} %shard_map.52.hidden, bf16[1024,512]{1,0:T(8,128)(2,1)S(1)} %get-tuple-element.21.first, bf16[1024,512]{1,0:T(8,128)(2,1)S(1)} %get-tuple-element.23.second), custom_call_target="tpu_custom_call" | custom-call | flops 536870912 | bytes 1048576 | tf_op jit(solution)/shard_map/pallas_call | solution.py:241
  115.0 4.4 %collective-permute-start.16 = (bf16[2,64,1024]{2,1,0:T(8,128)(2,1)S(1)}, bf16[2,64,1024]{2,1,0:T(8,128)(2,1)S(1)}, u32[]{:S(2)}, u32[]{:S(2)}) collective-permute-start(bf16[2,64,1024]{2,1,0:T(8,128)(2,1)S(1)} %get-tuple-element.28), channel_id=1, source_target_pairs={{0,2},{1,7},{2,0},{3,5},{4,6},{5,3},{6,4},{7,1},{8,10},{9,15},{10,... | collective-permute-start | bytes 786440 | tf_op jit(solution)/shard_map/ppermute | solution.py:33
  119.4 2.1 %collective-permute-start.15 = (bf16[2,64,1024]{2,1,0:T(8,128)(2,1)S(1)}, bf16[2,64,1024]{2,1,0:T(8,128)(2,1)S(1)}, u32[]{:S(2)}, u32[]{:S(2)}) collective-permute-start(bf16[2,64,1024]{2,1,0:T(8,128)(2,1)S(1)} %get-tuple-element.26), channel_id=1, source_target_pairs={{0,2},{1,7},{2,0},{3,5},{4,6},{5,3},{6,4},{7,1},{8,10},{9,15},{10,... | collective-permute-start | bytes 786440 | tf_op jit(solution)/shard_map/ppermute | solution.py:33
  121.5 1.8 %collective-permute-done.16.came = bf16[2,64,1024]{2,1,0:T(8,128)(2,1)S(1)} collective-permute-done((bf16[2,64,1024]{2,1,0:T(8,128)(2,1)S(1)}, bf16[2,64,1024]{2,1,0:T(8,128)(2,1)S(1)}, u32[]{:S(2)}, u32[]{:S(2)}) %collective-permute-start.16) | collective-permute-done | bytes 262176 | tf_op jit(solution)/shard_map/ppermute | solution.py:33
  123.4 2.2 %collective-permute-start.17 = (bf16[2,64,1024]{2,1,0:T(8,128)(2,1)S(1)}, bf16[2,64,1024]{2,1,0:T(8,128)(2,1)S(1)}, u32[]{:S(2)}, u32[]{:S(2)}) collective-permute-start(bf16[2,64,1024]{2,1,0:T(8,128)(2,1)S(1)} %shard_map.61), channel_id=1, source_target_pairs={{0,6},{1,3},{2,4},{3,1},{4,2},{5,7},{6,0},{7,5},{8,14},{9,11},{10,... | collective-permute-start | bytes 786440 | tf_op jit(solution)/shard_map/ppermute | solution.py:33
  125.6 2.1 %collective-permute-done.15.came = bf16[2,64,1024]{2,1,0:T(8,128)(2,1)S(1)} collective-permute-done((bf16[2,64,1024]{2,1,0:T(8,128)(2,1)S(1)}, bf16[2,64,1024]{2,1,0:T(8,128)(2,1)S(1)}, u32[]{:S(2)}, u32[]{:S(2)}) %collective-permute-start.15) | collective-permute-done | bytes 262176 | tf_op jit(solution)/shard_map/ppermute | solution.py:33
  127.7 3.1 %collective-permute-done.17.late = bf16[2,64,1024]{2,1,0:T(8,128)(2,1)S(1)} collective-permute-done((bf16[2,64,1024]{2,1,0:T(8,128)(2,1)S(1)}, bf16[2,64,1024]{2,1,0:T(8,128)(2,1)S(1)}, u32[]{:S(2)}, u32[]{:S(2)}) %collective-permute-start.17) | collective-permute-done | bytes 262176 | tf_op jit(solution)/shard_map/ppermute | solution.py:33
  (29 shorter events, 4.1 us)
Async XLA Ops:
  0.0 90.8 %copy-start = (bf16[512,2048]{1,0:T(8,128)(2,1)S(1)}, bf16[512,2048]{1,0:T(8,128)(2,1)}, u32[]{:S(2)}) copy-start(bf16[512,2048]{1,0:T(8,128)(2,1)} %tokens.1) | copy-start | bytes 6291460
  0.0 9.9 %collective-permute-start = (bf16[1,32,512]{2,1,0:T(8,128)(2,1)}, bf16[1,32,512]{2,1,0:T(8,128)(2,1)S(1)}, u32[]{:S(2)}, u32[]{:S(2)}) collective-permute-start(bf16[1,32,512]{2,1,0:T(8,128)(2,1)} %bitcast.5), channel_id=1, source_target_pairs={{32,0},{33,1},{40,8},{41,9},{48,16},{49,17},{56,24},{57,25},{0,32}... | collective-permute-start | bytes 98312 | tf_op jit(solution)/shard_map/ppermute | solution.py:25
  8.4 0.8 copy-start.1
  9.2 0.8 copy-start.2
  9.9 80.9 %copy-start.3 = (f32[2048]{0:T(1024)S(1)}, f32[2048]{0:T(1024)}, u32[]{:S(2)}) copy-start(f32[2048]{0:T(1024)} %param.5) | copy-start | bytes 24580
  10.0 19.8 %collective-permute-start.1 = (bf16[2,32,512]{2,1,0:T(8,128)(2,1)S(1)}, bf16[2,32,512]{2,1,0:T(8,128)(2,1)S(1)}, u32[]{:S(2)}, u32[]{:S(2)}) collective-permute-start(bf16[2,32,512]{2,1,0:T(8,128)(2,1)S(1)} %shard_map.48.a), channel_id=1, source_target_pairs={{256,0},{769,1},{320,64},{833,65},{384,128},{897,129},{448,192},{9... | collective-permute-start | bytes 196616 | tf_op jit(solution)/shard_map/ppermute | solution.py:25
  29.8 27.6 %collective-permute-start.2 = (bf16[4,32,512]{2,1,0:T(8,128)(2,1)S(1)}, bf16[4,32,512]{2,1,0:T(8,128)(2,1)S(1)}, u32[]{:S(2)}, u32[]{:S(2)}) collective-permute-start(bf16[4,32,512]{2,1,0:T(8,128)(2,1)S(1)} %shard_map.49.a), channel_id=1, source_target_pairs={{16,0},{49,1},{24,8},{57,9},{32,16},{1,17},{40,24},{9,25},{48,32},... | collective-permute-start | bytes 393224 | tf_op jit(solution)/shard_map/ppermute | solution.py:25
  34.2 8.8 %collective-permute-start.7 = (bf16[1,32,512]{2,1,0:T(8,128)(2,1)}, bf16[1,32,512]{2,1,0:T(8,128)(2,1)S(1)}, u32[]{:S(2)}, u32[]{:S(2)}) collective-permute-start(bf16[1,32,512]{2,1,0:T(8,128)(2,1)} %bitcast.7), channel_id=1, source_target_pairs={{256,0},{769,1},{320,64},{833,65},{384,128},{897,129},{448,192},{9... | collective-permute-start | bytes 98312 | tf_op jit(solution)/shard_map/ppermute | solution.py:25
  42.9 8.9 %collective-permute-start.8 = (bf16[2,32,512]{2,1,0:T(8,128)(2,1)S(1)}, bf16[2,32,512]{2,1,0:T(8,128)(2,1)S(1)}, u32[]{:S(2)}, u32[]{:S(2)}) collective-permute-start(bf16[2,32,512]{2,1,0:T(8,128)(2,1)S(1)} %shard_map.53.a), channel_id=1, source_target_pairs={{32,0},{33,1},{40,8},{41,9},{48,16},{49,17},{56,24},{57,25},{0,32}... | collective-permute-start | bytes 196616 | tf_op jit(solution)/shard_map/ppermute | solution.py:25
  51.9 11.3 %collective-permute-start.9 = (bf16[4,32,512]{2,1,0:T(8,128)(2,1)S(1)}, bf16[4,32,512]{2,1,0:T(8,128)(2,1)S(1)}, u32[]{:S(2)}, u32[]{:S(2)}) collective-permute-start(bf16[4,32,512]{2,1,0:T(8,128)(2,1)S(1)} %shard_map.54.a), channel_id=1, source_target_pairs={{128,0},{897,1},{192,64},{961,65},{256,128},{1,129},{320,192},{65,... | collective-permute-start | bytes 393224 | tf_op jit(solution)/shard_map/ppermute | solution.py:25
  57.5 10.9 %collective-permute-start.3 = (bf16[8,32,512]{2,1,0:T(8,128)(2,1)S(1)}, bf16[8,32,512]{2,1,0:T(8,128)(2,1)S(1)}, u32[]{:S(2)}, u32[]{:S(2)}) collective-permute-start(bf16[8,32,512]{2,1,0:T(8,128)(2,1)S(1)} %shard_map.50.a), channel_id=1, source_target_pairs={{128,0},{897,1},{192,64},{961,65},{256,128},{1,129},{320,192},{65,... | collective-permute-start | bytes 786440 | tf_op jit(solution)/shard_map/ppermute | solution.py:25
  63.2 12.0 %collective-permute-start.10 = (bf16[8,32,512]{2,1,0:T(8,128)(2,1)S(1)}, bf16[8,32,512]{2,1,0:T(8,128)(2,1)S(1)}, u32[]{:S(2)}, u32[]{:S(2)}) collective-permute-start(bf16[8,32,512]{2,1,0:T(8,128)(2,1)S(1)} %shard_map.55.a), channel_id=1, source_target_pairs={{16,0},{49,1},{24,8},{57,9},{32,16},{1,17},{40,24},{9,25},{48,32},... | collective-permute-start | bytes 786440 | tf_op jit(solution)/shard_map/ppermute | solution.py:25
  68.4 12.7 %collective-permute-start.4 = (bf16[16,32,512]{2,1,0:T(8,128)(2,1)S(1)}, bf16[16,32,512]{2,1,0:T(8,128)(2,1)S(1)}, u32[]{:S(2)}, u32[]{:S(2)}) collective-permute-start(bf16[16,32,512]{2,1,0:T(8,128)(2,1)S(1)} %shard_map.51.u0), channel_id=1, source_target_pairs={{64,0},{961,1},{128,64},{1,65},{192,128},{65,129},{256,192},{129,1... | collective-permute-start | bytes 1572872 | tf_op jit(solution)/shard_map/ppermute | solution.py:25
  75.2 13.6 %collective-permute-start.11 = (bf16[16,32,512]{2,1,0:T(8,128)(2,1)S(1)}, bf16[16,32,512]{2,1,0:T(8,128)(2,1)S(1)}, u32[]{:S(2)}, u32[]{:S(2)}) collective-permute-start(bf16[16,32,512]{2,1,0:T(8,128)(2,1)S(1)} %shard_map.56.d0), channel_id=1, source_target_pairs={{8,0},{57,1},{16,8},{1,9},{24,16},{9,17},{32,24},{17,25},{40,32},{... | collective-permute-start | bytes 1572872 | tf_op jit(solution)/shard_map/ppermute | solution.py:25
  77.6 15.4 %collective-permute-start.5 = (bf16[16,32,512]{2,1,0:T(8,128)(2,1)S(1)}, bf16[16,32,512]{2,1,0:T(8,128)(2,1)S(1)}, u32[]{:S(2)}, u32[]{:S(2)}) collective-permute-start(bf16[16,32,512]{2,1,0:T(8,128)(2,1)S(1)} %shard_map.51.u0), channel_id=1, source_target_pairs={{8,0},{57,1},{16,8},{1,9},{24,16},{9,17},{32,24},{17,25},{40,32},{... | collective-permute-start | bytes 1572872 | tf_op jit(solution)/shard_map/ppermute | solution.py:25
  81.1 16.5 %collective-permute-start.6 = (bf16[16,32,512]{2,1,0:T(8,128)(2,1)S(1)}, bf16[16,32,512]{2,1,0:T(8,128)(2,1)S(1)}, u32[]{:S(2)}, u32[]{:S(2)}) collective-permute-start(bf16[16,32,512]{2,1,0:T(8,128)(2,1)S(1)} %collective-permute-done.4.uz), channel_id=1, source_target_pairs={{8,0},{57,1},{16,8},{1,9},{24,16},{9,17},{32,24},{17,25},{40,32},{... | collective-permute-start | bytes 1572872 | tf_op jit(solution)/shard_map/ppermute | solution.py:25
  84.1 16.2 %collective-permute-start.12 = (bf16[16,32,512]{2,1,0:T(8,128)(2,1)S(1)}, bf16[16,32,512]{2,1,0:T(8,128)(2,1)S(1)}, u32[]{:S(2)}, u32[]{:S(2)}) collective-permute-start(bf16[16,32,512]{2,1,0:T(8,128)(2,1)S(1)} %shard_map.56.d0), channel_id=1, source_target_pairs={{64,0},{961,1},{128,64},{1,65},{192,128},{65,129},{256,192},{129,1... | collective-permute-start | bytes 1572872 | tf_op jit(solution)/shard_map/ppermute | solution.py:25
  88.9 13.9 %collective-permute-start.13 = (bf16[16,32,512]{2,1,0:T(8,128)(2,1)S(1)}, bf16[16,32,512]{2,1,0:T(8,128)(2,1)S(1)}, u32[]{:S(2)}, u32[]{:S(2)}) collective-permute-start(bf16[16,32,512]{2,1,0:T(8,128)(2,1)S(1)} %collective-permute-done.11.dy), channel_id=1, source_target_pairs={{64,0},{961,1},{128,64},{1,65},{192,128},{65,129},{256,192},{129,1... | collective-permute-start | bytes 1572872 | tf_op jit(solution)/shard_map/ppermute | solution.py:25
  103.9 10.9 %collective-permute-start.14 = (bf16[2,256,1024]{2,1,0:T(8,128)(2,1)S(1)}, bf16[2,256,1024]{2,1,0:T(8,128)(2,1)S(1)}, u32[]{:S(2)}, u32[]{:S(2)}) collective-permute-start(bf16[2,256,1024]{2,1,0:T(8,128)(2,1)S(1)} %get-tuple-element.24), channel_id=1, source_target_pairs={{0,1},{1,0},{2,3},{3,2},{4,5},{5,4},{6,7},{7,6},{8,9},{9,8},{10,11... | collective-permute-start | bytes 3145736 | tf_op jit(solution)/shard_map/ppermute | solution.py:240
  115.0 8.3 %collective-permute-start.16 = (bf16[2,64,1024]{2,1,0:T(8,128)(2,1)S(1)}, bf16[2,64,1024]{2,1,0:T(8,128)(2,1)S(1)}, u32[]{:S(2)}, u32[]{:S(2)}) collective-permute-start(bf16[2,64,1024]{2,1,0:T(8,128)(2,1)S(1)} %get-tuple-element.28), channel_id=1, source_target_pairs={{0,2},{1,7},{2,0},{3,5},{4,6},{5,3},{6,4},{7,1},{8,10},{9,15},{10,... | collective-permute-start | bytes 786440 | tf_op jit(solution)/shard_map/ppermute | solution.py:33
  119.4 8.3 %collective-permute-start.15 = (bf16[2,64,1024]{2,1,0:T(8,128)(2,1)S(1)}, bf16[2,64,1024]{2,1,0:T(8,128)(2,1)S(1)}, u32[]{:S(2)}, u32[]{:S(2)}) collective-permute-start(bf16[2,64,1024]{2,1,0:T(8,128)(2,1)S(1)} %get-tuple-element.26), channel_id=1, source_target_pairs={{0,2},{1,7},{2,0},{3,5},{4,6},{5,3},{6,4},{7,1},{8,10},{9,15},{10,... | collective-permute-start | bytes 786440 | tf_op jit(solution)/shard_map/ppermute | solution.py:33
  123.4 7.4 %collective-permute-start.17 = (bf16[2,64,1024]{2,1,0:T(8,128)(2,1)S(1)}, bf16[2,64,1024]{2,1,0:T(8,128)(2,1)S(1)}, u32[]{:S(2)}, u32[]{:S(2)}) collective-permute-start(bf16[2,64,1024]{2,1,0:T(8,128)(2,1)S(1)} %shard_map.61), channel_id=1, source_target_pairs={{0,6},{1,3},{2,4},{3,1},{4,2},{5,7},{6,0},{7,5},{8,14},{9,11},{10,... | collective-permute-start | bytes 786440 | tf_op jit(solution)/shard_map/ppermute | solution.py:33

commit v8 on v7

--- a/solution.py
+++ b/solution.py
@@ -20,8 +20,8 @@
     names, size = (("y", "core"), Y) if axis == "y" else (("rep", "z", "core"), REP * Z)
     pairs = []
     for i in range(size):
-        pairs.append(((i + shift) % size * 2, i * 2))
-        pairs.append(((i - shift) % size * 2 + 1, i * 2 + 1))
+        pairs.append(((i - shift) % size * 2, i * 2))
+        pairs.append(((i + shift) % size * 2 + 1, i * 2 + 1))
     return lax.ppermute(array, names, pairs)
 
 
@@ -78,9 +78,8 @@
     return kernel_call(join_kernel, bf16(2 * n, 32, 512), 2)(a, b)
 
 
-def stage_kernel(up, down, up_out, down_out):
-    up_out[...] = up[...]
-    down_out[...] = down[...]
+def stage_kernel(array, out):
+    out[...] = array[...]
 
 
 def norm_kernel(tokens, gain, normed, residual):
@@ -97,7 +96,7 @@
 
 def place(piece, laid, whole, halved):
     z, y = lax.axis_index("z"), lax.axis_index("y")
-    sign = 1 - 2 * lax.axis_index("core")
+    sign = 2 * lax.axis_index("core") - 1
     for j, (dz, dy) in enumerate(laid):
         at_z = (z + sign * dz) & (Z - 1)
         at_y = (y + sign * dy) & (Y - 1)
@@ -195,8 +194,9 @@
         up_in = from_side(up, *UP_STEPS[k])
         down_in = from_side(down, *DOWN_STEPS[k])
         if k == 0:
-            own = bf16(1, 32, 512)
-            up, down = kernel_call(stage_kernel, (own, own), 2)(up, down)
+            stage = kernel_call(stage_kernel, bf16(1, 32, 512), 1)
+            up = stage(up)
+            down = stage(down)
         up = join(up, up_in)
         down = join(down, down_in)
     up_z = from_side(up, "z", 1)

time: 134 us -> 135 us (level)
  starting transfers between devices: 82.2 us -> 99.5 us
  waiting for transfers between devices: 38.2 us -> 22.2 us
    ppermute x14, waiting for transfers between devices: 31 us -> 15 us  [from_side(): return lax.ppermute(array, names, pairs)]
    ppermute x14, starting transfers between devices: 64.9 us -> 78.9 us  [from_side(): return lax.ppermute(array, names, pairs)]
    ppermute x1, starting transfers between devices: 8.59 us -> 11.9 us  [shards(): beside = lax.ppermute(theirs, 'core', [(0, 1), (1, 0)])]
  transfers between devices with their start and end apart: 18 -> 18, of which waited for: 11 -> 13; matrix products, arithmetic and copies ran while one was open for 0% -> 0% of each run, Pallas kernels for 5% -> 5%
where the time goes in v8:
time: 135 us; the launch traced here: 133 us
  starting transfers between devices  99.5 us (74%)
  waiting for transfers between devices  22.2 us (16%)
  Pallas kernels  9.44 us (7%)
  local copies, waits for them, and re-layouts  1.53 us (1%)
    ppermute x14, starting transfers between devices, from_side(): return lax.ppermute(array, names, pairs)  78.9 us
    ppermute x14, waiting for transfers between devices, from_side(): return lax.ppermute(array, names, pairs)  15 us
    ppermute x1, starting transfers between devices, shards(): beside = lax.ppermute(theirs, 'core', [(0, 1), (1, 0)])  11.9 us
    ppermute x3, starting transfers between devices, between_x(): return lax.ppermute(array, ('x', 'core'), pairs)  8.7 us
    ppermute x3, waiting for transfers between devices, between_x(): return lax.ppermute(array, ('x', 'core'), pairs)  7.01 us
  transfers between devices with their start and end apart: 18, of which 13 were waited for; matrix products, arithmetic and copies ran while one was open for 0% of the time, Pallas kernels for 5%

profile of v8, /device:TPU:1, one launch (start us, length us, event | category | flops | bytes accessed | tf_op | source)
XLA Modules:
  0.0 132.9 jit_solution(9549131558153095945)
XLA Ops:
  0.0 8.4 %collective-permute-start = (bf16[1,32,512]{2,1,0:T(8,128)(2,1)}, bf16[1,32,512]{2,1,0:T(8,128)(2,1)S(1)}, u32[]{:S(2)}, u32[]{:S(2)}) collective-permute-start(bf16[1,32,512]{2,1,0:T(8,128)(2,1)} %bitcast.5), channel_id=1, source_target_pairs={{32,0},{33,1},{40,8},{41,9},{48,16},{49,17},{56,24},{57,25},{0,32}... | collective-permute-start | bytes 98312 | tf_op jit(solution)/shard_map/ppermute | solution.py:25
  9.9 17.9 %collective-permute-start.1 = (bf16[2,32,512]{2,1,0:T(8,128)(2,1)S(1)}, bf16[2,32,512]{2,1,0:T(8,128)(2,1)S(1)}, u32[]{:S(2)}, u32[]{:S(2)}) collective-permute-start(bf16[2,32,512]{2,1,0:T(8,128)(2,1)S(1)} %shard_map.48.a), channel_id=1, source_target_pairs={{768,0},{257,1},{832,64},{321,65},{896,128},{385,129},{960,192},{4... | collective-permute-start | bytes 196616 | tf_op jit(solution)/shard_map/ppermute | solution.py:25
  27.8 1.3 collective-permute-done.1.b
  29.2 5.7 %collective-permute-start.2 = (bf16[4,32,512]{2,1,0:T(8,128)(2,1)S(1)}, bf16[4,32,512]{2,1,0:T(8,128)(2,1)S(1)}, u32[]{:S(2)}, u32[]{:S(2)}) collective-permute-start(bf16[4,32,512]{2,1,0:T(8,128)(2,1)S(1)} %shard_map.49.a), channel_id=1, source_target_pairs={{48,0},{17,1},{56,8},{25,9},{0,16},{33,17},{8,24},{41,25},{16,32},... | collective-permute-start | bytes 393224 | tf_op jit(solution)/shard_map/ppermute | solution.py:25
  34.8 7.6 %collective-permute-start.7 = (bf16[1,32,512]{2,1,0:T(8,128)(2,1)}, bf16[1,32,512]{2,1,0:T(8,128)(2,1)S(1)}, u32[]{:S(2)}, u32[]{:S(2)}) collective-permute-start(bf16[1,32,512]{2,1,0:T(8,128)(2,1)} %bitcast.7), channel_id=1, source_target_pairs={{768,0},{257,1},{832,64},{321,65},{896,128},{385,129},{960,192},{4... | collective-permute-start | bytes 98312 | tf_op jit(solution)/shard_map/ppermute | solution.py:25
  43.8 3.9 %collective-permute-start.8 = (bf16[2,32,512]{2,1,0:T(8,128)(2,1)S(1)}, bf16[2,32,512]{2,1,0:T(8,128)(2,1)S(1)}, u32[]{:S(2)}, u32[]{:S(2)}) collective-permute-start(bf16[2,32,512]{2,1,0:T(8,128)(2,1)S(1)} %shard_map.54.a), channel_id=1, source_target_pairs={{32,0},{33,1},{40,8},{41,9},{48,16},{49,17},{56,24},{57,25},{0,32}... | collective-permute-start | bytes 196616 | tf_op jit(solution)/shard_map/ppermute | solution.py:25
  47.7 5.0 %collective-permute-done.8.b = bf16[2,32,512]{2,1,0:T(8,128)(2,1)S(1)} collective-permute-done((bf16[2,32,512]{2,1,0:T(8,128)(2,1)S(1)}, bf16[2,32,512]{2,1,0:T(8,128)(2,1)S(1)}, u32[]{:S(2)}, u32[]{:S(2)}) %collective-permute-start.8) | collective-permute-done | bytes 65568 | tf_op jit(solution)/shard_map/ppermute | solution.py:25
  52.7 7.5 %collective-permute-start.9 = (bf16[4,32,512]{2,1,0:T(8,128)(2,1)S(1)}, bf16[4,32,512]{2,1,0:T(8,128)(2,1)S(1)}, u32[]{:S(2)}, u32[]{:S(2)}) collective-permute-start(bf16[4,32,512]{2,1,0:T(8,128)(2,1)S(1)} %shard_map.55.a), channel_id=1, source_target_pairs={{896,0},{129,1},{960,64},{193,65},{0,128},{257,129},{64,192},{321,... | collective-permute-start | bytes 393224 | tf_op jit(solution)/shard_map/ppermute | solution.py:25
  60.2 2.2 %collective-permute-start.3 = (bf16[8,32,512]{2,1,0:T(8,128)(2,1)S(1)}, bf16[8,32,512]{2,1,0:T(8,128)(2,1)S(1)}, u32[]{:S(2)}, u32[]{:S(2)}) collective-permute-start(bf16[8,32,512]{2,1,0:T(8,128)(2,1)S(1)} %shard_map.50.a), channel_id=1, source_target_pairs={{896,0},{129,1},{960,64},{193,65},{0,128},{257,129},{64,192},{321,... | collective-permute-start | bytes 786440 | tf_op jit(solution)/shard_map/ppermute | solution.py:25
  62.4 1.1 collective-permute-done.9.b
  63.5 4.8 %collective-permute-start.10 = (bf16[8,32,512]{2,1,0:T(8,128)(2,1)S(1)}, bf16[8,32,512]{2,1,0:T(8,128)(2,1)S(1)}, u32[]{:S(2)}, u32[]{:S(2)}) collective-permute-start(bf16[8,32,512]{2,1,0:T(8,128)(2,1)S(1)} %shard_map.56.a), channel_id=1, source_target_pairs={{48,0},{17,1},{56,8},{25,9},{0,16},{33,17},{8,24},{41,25},{16,32},... | collective-permute-start | bytes 786440 | tf_op jit(solution)/shard_map/ppermute | solution.py:25
  68.3 3.1 %collective-permute-done.3.b = bf16[8,32,512]{2,1,0:T(8,128)(2,1)S(1)} collective-permute-done((bf16[8,32,512]{2,1,0:T(8,128)(2,1)S(1)}, bf16[8,32,512]{2,1,0:T(8,128)(2,1)S(1)}, u32[]{:S(2)}, u32[]{:S(2)}) %collective-permute-start.3) | collective-permute-done | bytes 262176 | tf_op jit(solution)/shard_map/ppermute | solution.py:25
  71.4 2.8 %collective-permute-start.4 = (bf16[16,32,512]{2,1,0:T(8,128)(2,1)S(1)}, bf16[16,32,512]{2,1,0:T(8,128)(2,1)S(1)}, u32[]{:S(2)}, u32[]{:S(2)}) collective-permute-start(bf16[16,32,512]{2,1,0:T(8,128)(2,1)S(1)} %shard_map.51.u0), channel_id=1, source_target_pairs={{960,0},{65,1},{0,64},{129,65},{64,128},{193,129},{128,192},{257,1... | collective-permute-start | bytes 1572872 | tf_op jit(solution)/shard_map/ppermute | solution.py:25
  74.4 3.1 %collective-permute-start.11 = (bf16[16,32,512]{2,1,0:T(8,128)(2,1)S(1)}, bf16[16,32,512]{2,1,0:T(8,128)(2,1)S(1)}, u32[]{:S(2)}, u32[]{:S(2)}) collective-permute-start(bf16[16,32,512]{2,1,0:T(8,128)(2,1)S(1)} %shard_map.57.d0), channel_id=1, source_target_pairs={{56,0},{9,1},{0,8},{17,9},{8,16},{25,17},{16,24},{33,25},{24,32},{... | collective-permute-start | bytes 1572872 | tf_op jit(solution)/shard_map/ppermute | solution.py:25
  77.5 4.9 %collective-permute-start.5 = (bf16[16,32,512]{2,1,0:T(8,128)(2,1)S(1)}, bf16[16,32,512]{2,1,0:T(8,128)(2,1)S(1)}, u32[]{:S(2)}, u32[]{:S(2)}) collective-permute-start(bf16[16,32,512]{2,1,0:T(8,128)(2,1)S(1)} %shard_map.51.u0), channel_id=1, source_target_pairs={{56,0},{9,1},{0,8},{17,9},{8,16},{25,17},{16,24},{33,25},{24,32},{... | collective-permute-start | bytes 1572872 | tf_op jit(solution)/shard_map/ppermute | solution.py:25
  82.4 2.2 %collective-permute-start.6 = (bf16[16,32,512]{2,1,0:T(8,128)(2,1)S(1)}, bf16[16,32,512]{2,1,0:T(8,128)(2,1)S(1)}, u32[]{:S(2)}, u32[]{:S(2)}) collective-permute-start(bf16[16,32,512]{2,1,0:T(8,128)(2,1)S(1)} %collective-permute-done.4.uz), channel_id=1, source_target_pairs={{56,0},{9,1},{0,8},{17,9},{8,16},{25,17},{16,24},{33,25},{24,32},{... | collective-permute-start | bytes 1572872 | tf_op jit(solution)/shard_map/ppermute | solution.py:25
  84.6 4.4 %collective-permute-start.12 = (bf16[16,32,512]{2,1,0:T(8,128)(2,1)S(1)}, bf16[16,32,512]{2,1,0:T(8,128)(2,1)S(1)}, u32[]{:S(2)}, u32[]{:S(2)}) collective-permute-start(bf16[16,32,512]{2,1,0:T(8,128)(2,1)S(1)} %shard_map.57.d0), channel_id=1, source_target_pairs={{960,0},{65,1},{0,64},{129,65},{64,128},{193,129},{128,192},{257,1... | collective-permute-start | bytes 1572872 | tf_op jit(solution)/shard_map/ppermute | solution.py:25
  89.0 3.7 %collective-permute-start.13 = (bf16[16,32,512]{2,1,0:T(8,128)(2,1)S(1)}, bf16[16,32,512]{2,1,0:T(8,128)(2,1)S(1)}, u32[]{:S(2)}, u32[]{:S(2)}) collective-permute-start(bf16[16,32,512]{2,1,0:T(8,128)(2,1)S(1)} %collective-permute-done.11.dy), channel_id=1, source_target_pairs={{960,0},{65,1},{0,64},{129,65},{64,128},{193,129},{128,192},{257,1... | collective-permute-start | bytes 1572872 | tf_op jit(solution)/shard_map/ppermute | solution.py:25
  92.7 2.1 %shard_map.46 = (bf16[512,2048]{1,0:T(8,128)(2,1)S(1)}, bf16[64,2048]{1,0:T(8,128)(2,1)S(1)}) custom-call(bf16[512,2048]{1,0:T(8,128)(2,1)S(1)} %copy-done, f32[1,2048]{1,0:T(1,128)S(1)} %bitcast.9), custom_call_target="tpu_custom_call" | custom-call | flops 16777216 | bytes 1048576 | tf_op jit(solution)/shard_map/pallas_call | solution.py:223
  94.8 1.0 collective-permute-done.6.uzy
  95.9 1.6 %shard_map.52.hidden = bf16[512,512]{1,0:T(8,128)(2,1)S(1)} custom-call(bf16[512,2048]{1,0:T(8,128)(2,1)S(1)} %get-tuple-element.16.normed, bf16[16,32,512]{2,1,0:T(8,128)(2,1)S(1)} %shard_map.51.u0, bf16[16,32,512]{2,1,0:T(8,128)(2,1)S(1)} %collective-permute-done.4.uz, bf16[16,32,512]{2,1,0:T(8,128)(2,1)S(1)} %collective-permute-done.5.uy, ...), custom_call_target="tpu_custom_call" | custom-call | flops 1073741824 | bytes 1048576 | tf_op jit(solution)/shard_map/pallas_call | solution.py:226
  97.5 1.2 shard_map.58
  98.7 2.1 %collective-permute-done.13.dyz = bf16[16,32,512]{2,1,0:T(8,128)(2,1)S(1)} collective-permute-done((bf16[16,32,512]{2,1,0:T(8,128)(2,1)S(1)}, bf16[16,32,512]{2,1,0:T(8,128)(2,1)S(1)}, u32[]{:S(2)}, u32[]{:S(2)}) %collective-permute-start.13) | collective-permute-done | bytes 524320 | tf_op jit(solution)/shard_map/ppermute | solution.py:25
  100.7 1.1 shard_map.59
  101.9 11.9 %collective-permute-start.14 = (bf16[2,256,1024]{2,1,0:T(8,128)(2,1)S(1)}, bf16[2,256,1024]{2,1,0:T(8,128)(2,1)S(1)}, u32[]{:S(2)}, u32[]{:S(2)}) collective-permute-start(bf16[2,256,1024]{2,1,0:T(8,128)(2,1)S(1)} %get-tuple-element.20), channel_id=1, source_target_pairs={{0,1},{1,0},{2,3},{3,2},{4,5},{5,4},{6,7},{7,6},{8,9},{9,8},{10,11... | collective-permute-start | bytes 3145736 | tf_op jit(solution)/shard_map/ppermute | solution.py:240
  113.7 2.1 %shard_map.60.own = bf16[2,256,1024]{2,1,0:T(8,128)(2,1)S(1)} custom-call(bf16[512,512]{1,0:T(8,128)(2,1)S(1)} %shard_map.52.hidden, bf16[1024,512]{1,0:T(8,128)(2,1)S(1)} %get-tuple-element.17.first, bf16[1024,512]{1,0:T(8,128)(2,1)S(1)} %get-tuple-element.19.second), custom_call_target="tpu_custom_call" | custom-call | flops 536870912 | bytes 1048576 | tf_op jit(solution)/shard_map/pallas_call | solution.py:241
  116.2 4.4 %collective-permute-start.16 = (bf16[2,64,1024]{2,1,0:T(8,128)(2,1)S(1)}, bf16[2,64,1024]{2,1,0:T(8,128)(2,1)S(1)}, u32[]{:S(2)}, u32[]{:S(2)}) collective-permute-start(bf16[2,64,1024]{2,1,0:T(8,128)(2,1)S(1)} %get-tuple-element.24), channel_id=1, source_target_pairs={{0,2},{1,7},{2,0},{3,5},{4,6},{5,3},{6,4},{7,1},{8,10},{9,15},{10,... | collective-permute-start | bytes 786440 | tf_op jit(solution)/shard_map/ppermute | solution.py:33
  120.6 2.1 %collective-permute-start.15 = (bf16[2,64,1024]{2,1,0:T(8,128)(2,1)S(1)}, bf16[2,64,1024]{2,1,0:T(8,128)(2,1)S(1)}, u32[]{:S(2)}, u32[]{:S(2)}) collective-permute-start(bf16[2,64,1024]{2,1,0:T(8,128)(2,1)S(1)} %get-tuple-element.22), channel_id=1, source_target_pairs={{0,2},{1,7},{2,0},{3,5},{4,6},{5,3},{6,4},{7,1},{8,10},{9,15},{10,... | collective-permute-start | bytes 786440 | tf_op jit(solution)/shard_map/ppermute | solution.py:33
  122.7 1.8 %collective-permute-done.16.came = bf16[2,64,1024]{2,1,0:T(8,128)(2,1)S(1)} collective-permute-done((bf16[2,64,1024]{2,1,0:T(8,128)(2,1)S(1)}, bf16[2,64,1024]{2,1,0:T(8,128)(2,1)S(1)}, u32[]{:S(2)}, u32[]{:S(2)}) %collective-permute-start.16) | collective-permute-done | bytes 262176 | tf_op jit(solution)/shard_map/ppermute | solution.py:33
  124.6 2.2 %collective-permute-start.17 = (bf16[2,64,1024]{2,1,0:T(8,128)(2,1)S(1)}, bf16[2,64,1024]{2,1,0:T(8,128)(2,1)S(1)}, u32[]{:S(2)}, u32[]{:S(2)}) collective-permute-start(bf16[2,64,1024]{2,1,0:T(8,128)(2,1)S(1)} %shard_map.62), channel_id=1, source_target_pairs={{0,6},{1,3},{2,4},{3,1},{4,2},{5,7},{6,0},{7,5},{8,14},{9,11},{10,... | collective-permute-start | bytes 786440 | tf_op jit(solution)/shard_map/ppermute | solution.py:33
  126.8 2.1 %collective-permute-done.15.came = bf16[2,64,1024]{2,1,0:T(8,128)(2,1)S(1)} collective-permute-done((bf16[2,64,1024]{2,1,0:T(8,128)(2,1)S(1)}, bf16[2,64,1024]{2,1,0:T(8,128)(2,1)S(1)}, u32[]{:S(2)}, u32[]{:S(2)}) %collective-permute-start.15) | collective-permute-done | bytes 262176 | tf_op jit(solution)/shard_map/ppermute | solution.py:33
  128.9 3.1 %collective-permute-done.17.late = bf16[2,64,1024]{2,1,0:T(8,128)(2,1)S(1)} collective-permute-done((bf16[2,64,1024]{2,1,0:T(8,128)(2,1)S(1)}, bf16[2,64,1024]{2,1,0:T(8,128)(2,1)S(1)}, u32[]{:S(2)}, u32[]{:S(2)}) %collective-permute-start.17) | collective-permute-done | bytes 262176 | tf_op jit(solution)/shard_map/ppermute | solution.py:33
  (30 shorter events, 4.5 us)
Async XLA Ops:
  0.0 92.7 %copy-start = (bf16[512,2048]{1,0:T(8,128)(2,1)S(1)}, bf16[512,2048]{1,0:T(8,128)(2,1)}, u32[]{:S(2)}) copy-start(bf16[512,2048]{1,0:T(8,128)(2,1)} %tokens.1) | copy-start | bytes 6291460
  0.0 9.9 %collective-permute-start = (bf16[1,32,512]{2,1,0:T(8,128)(2,1)}, bf16[1,32,512]{2,1,0:T(8,128)(2,1)S(1)}, u32[]{:S(2)}, u32[]{:S(2)}) collective-permute-start(bf16[1,32,512]{2,1,0:T(8,128)(2,1)} %bitcast.5), channel_id=1, source_target_pairs={{32,0},{33,1},{40,8},{41,9},{48,16},{49,17},{56,24},{57,25},{0,32}... | collective-permute-start | bytes 98312 | tf_op jit(solution)/shard_map/ppermute | solution.py:25
  8.4 0.8 copy-start.1
  9.9 19.2 %collective-permute-start.1 = (bf16[2,32,512]{2,1,0:T(8,128)(2,1)S(1)}, bf16[2,32,512]{2,1,0:T(8,128)(2,1)S(1)}, u32[]{:S(2)}, u32[]{:S(2)}) collective-permute-start(bf16[2,32,512]{2,1,0:T(8,128)(2,1)S(1)} %shard_map.48.a), channel_id=1, source_target_pairs={{768,0},{257,1},{832,64},{321,65},{896,128},{385,129},{960,192},{4... | collective-permute-start | bytes 196616 | tf_op jit(solution)/shard_map/ppermute | solution.py:25
  29.2 31.0 %collective-permute-start.2 = (bf16[4,32,512]{2,1,0:T(8,128)(2,1)S(1)}, bf16[4,32,512]{2,1,0:T(8,128)(2,1)S(1)}, u32[]{:S(2)}, u32[]{:S(2)}) collective-permute-start(bf16[4,32,512]{2,1,0:T(8,128)(2,1)S(1)} %shard_map.49.a), channel_id=1, source_target_pairs={{48,0},{17,1},{56,8},{25,9},{0,16},{33,17},{8,24},{41,25},{16,32},... | collective-permute-start | bytes 393224 | tf_op jit(solution)/shard_map/ppermute | solution.py:25
  34.8 8.9 %collective-permute-start.7 = (bf16[1,32,512]{2,1,0:T(8,128)(2,1)}, bf16[1,32,512]{2,1,0:T(8,128)(2,1)S(1)}, u32[]{:S(2)}, u32[]{:S(2)}) collective-permute-start(bf16[1,32,512]{2,1,0:T(8,128)(2,1)} %bitcast.7), channel_id=1, source_target_pairs={{768,0},{257,1},{832,64},{321,65},{896,128},{385,129},{960,192},{4... | collective-permute-start | bytes 98312 | tf_op jit(solution)/shard_map/ppermute | solution.py:25
  42.5 0.8 copy-start.2
  43.2 49.5 %copy-start.3 = (f32[2048]{0:T(1024)S(1)}, f32[2048]{0:T(1024)}, u32[]{:S(2)}) copy-start(f32[2048]{0:T(1024)} %param.5) | copy-start | bytes 24580
  43.8 8.9 %collective-permute-start.8 = (bf16[2,32,512]{2,1,0:T(8,128)(2,1)S(1)}, bf16[2,32,512]{2,1,0:T(8,128)(2,1)S(1)}, u32[]{:S(2)}, u32[]{:S(2)}) collective-permute-start(bf16[2,32,512]{2,1,0:T(8,128)(2,1)S(1)} %shard_map.54.a), channel_id=1, source_target_pairs={{32,0},{33,1},{40,8},{41,9},{48,16},{49,17},{56,24},{57,25},{0,32}... | collective-permute-start | bytes 196616 | tf_op jit(solution)/shard_map/ppermute | solution.py:25
  52.7 10.8 %collective-permute-start.9 = (bf16[4,32,512]{2,1,0:T(8,128)(2,1)S(1)}, bf16[4,32,512]{2,1,0:T(8,128)(2,1)S(1)}, u32[]{:S(2)}, u32[]{:S(2)}) collective-permute-start(bf16[4,32,512]{2,1,0:T(8,128)(2,1)S(1)} %shard_map.55.a), channel_id=1, source_target_pairs={{896,0},{129,1},{960,64},{193,65},{0,128},{257,129},{64,192},{321,... | collective-permute-start | bytes 393224 | tf_op jit(solution)/shard_map/ppermute | solution.py:25
  60.2 11.1 %collective-permute-start.3 = (bf16[8,32,512]{2,1,0:T(8,128)(2,1)S(1)}, bf16[8,32,512]{2,1,0:T(8,128)(2,1)S(1)}, u32[]{:S(2)}, u32[]{:S(2)}) collective-permute-start(bf16[8,32,512]{2,1,0:T(8,128)(2,1)S(1)} %shard_map.50.a), channel_id=1, source_target_pairs={{896,0},{129,1},{960,64},{193,65},{0,128},{257,129},{64,192},{321,... | collective-permute-start | bytes 786440 | tf_op jit(solution)/shard_map/ppermute | solution.py:25
  63.5 10.9 %collective-permute-start.10 = (bf16[8,32,512]{2,1,0:T(8,128)(2,1)S(1)}, bf16[8,32,512]{2,1,0:T(8,128)(2,1)S(1)}, u32[]{:S(2)}, u32[]{:S(2)}) collective-permute-start(bf16[8,32,512]{2,1,0:T(8,128)(2,1)S(1)} %shard_map.56.a), channel_id=1, source_target_pairs={{48,0},{17,1},{56,8},{25,9},{0,16},{33,17},{8,24},{41,25},{16,32},... | collective-permute-start | bytes 786440 | tf_op jit(solution)/shard_map/ppermute | solution.py:25
  71.4 11.0 %collective-permute-start.4 = (bf16[16,32,512]{2,1,0:T(8,128)(2,1)S(1)}, bf16[16,32,512]{2,1,0:T(8,128)(2,1)S(1)}, u32[]{:S(2)}, u32[]{:S(2)}) collective-permute-start(bf16[16,32,512]{2,1,0:T(8,128)(2,1)S(1)} %shard_map.51.u0), channel_id=1, source_target_pairs={{960,0},{65,1},{0,64},{129,65},{64,128},{193,129},{128,192},{257,1... | collective-permute-start | bytes 1572872 | tf_op jit(solution)/shard_map/ppermute | solution.py:25
  74.4 14.6 %collective-permute-start.11 = (bf16[16,32,512]{2,1,0:T(8,128)(2,1)S(1)}, bf16[16,32,512]{2,1,0:T(8,128)(2,1)S(1)}, u32[]{:S(2)}, u32[]{:S(2)}) collective-permute-start(bf16[16,32,512]{2,1,0:T(8,128)(2,1)S(1)} %shard_map.57.d0), channel_id=1, source_target_pairs={{56,0},{9,1},{0,8},{17,9},{8,16},{25,17},{16,24},{33,25},{24,32},{... | collective-permute-start | bytes 1572872 | tf_op jit(solution)/shard_map/ppermute | solution.py:25
  77.5 17.3 %collective-permute-start.5 = (bf16[16,32,512]{2,1,0:T(8,128)(2,1)S(1)}, bf16[16,32,512]{2,1,0:T(8,128)(2,1)S(1)}, u32[]{:S(2)}, u32[]{:S(2)}) collective-permute-start(bf16[16,32,512]{2,1,0:T(8,128)(2,1)S(1)} %shard_map.51.u0), channel_id=1, source_target_pairs={{56,0},{9,1},{0,8},{17,9},{8,16},{25,17},{16,24},{33,25},{24,32},{... | collective-permute-start | bytes 1572872 | tf_op jit(solution)/shard_map/ppermute | solution.py:25
  82.4 13.4 %collective-permute-start.6 = (bf16[16,32,512]{2,1,0:T(8,128)(2,1)S(1)}, bf16[16,32,512]{2,1,0:T(8,128)(2,1)S(1)}, u32[]{:S(2)}, u32[]{:S(2)}) collective-permute-start(bf16[16,32,512]{2,1,0:T(8,128)(2,1)S(1)} %collective-permute-done.4.uz), channel_id=1, source_target_pairs={{56,0},{9,1},{0,8},{17,9},{8,16},{25,17},{16,24},{33,25},{24,32},{... | collective-permute-start | bytes 1572872 | tf_op jit(solution)/shard_map/ppermute | solution.py:25
  84.6 14.0 %collective-permute-start.12 = (bf16[16,32,512]{2,1,0:T(8,128)(2,1)S(1)}, bf16[16,32,512]{2,1,0:T(8,128)(2,1)S(1)}, u32[]{:S(2)}, u32[]{:S(2)}) collective-permute-start(bf16[16,32,512]{2,1,0:T(8,128)(2,1)S(1)} %shard_map.57.d0), channel_id=1, source_target_pairs={{960,0},{65,1},{0,64},{129,65},{64,128},{193,129},{128,192},{257,1... | collective-permute-start | bytes 1572872 | tf_op jit(solution)/shard_map/ppermute | solution.py:25
  89.0 11.7 %collective-permute-start.13 = (bf16[16,32,512]{2,1,0:T(8,128)(2,1)S(1)}, bf16[16,32,512]{2,1,0:T(8,128)(2,1)S(1)}, u32[]{:S(2)}, u32[]{:S(2)}) collective-permute-start(bf16[16,32,512]{2,1,0:T(8,128)(2,1)S(1)} %collective-permute-done.11.dy), channel_id=1, source_target_pairs={{960,0},{65,1},{0,64},{129,65},{64,128},{193,129},{128,192},{257,1... | collective-permute-start | bytes 1572872 | tf_op jit(solution)/shard_map/ppermute | solution.py:25
  101.9 14.1 %collective-permute-start.14 = (bf16[2,256,1024]{2,1,0:T(8,128)(2,1)S(1)}, bf16[2,256,1024]{2,1,0:T(8,128)(2,1)S(1)}, u32[]{:S(2)}, u32[]{:S(2)}) collective-permute-start(bf16[2,256,1024]{2,1,0:T(8,128)(2,1)S(1)} %get-tuple-element.20), channel_id=1, source_target_pairs={{0,1},{1,0},{2,3},{3,2},{4,5},{5,4},{6,7},{7,6},{8,9},{9,8},{10,11... | collective-permute-start | bytes 3145736 | tf_op jit(solution)/shard_map/ppermute | solution.py:240
  116.2 8.3 %collective-permute-start.16 = (bf16[2,64,1024]{2,1,0:T(8,128)(2,1)S(1)}, bf16[2,64,1024]{2,1,0:T(8,128)(2,1)S(1)}, u32[]{:S(2)}, u32[]{:S(2)}) collective-permute-start(bf16[2,64,1024]{2,1,0:T(8,128)(2,1)S(1)} %get-tuple-element.24), channel_id=1, source_target_pairs={{0,2},{1,7},{2,0},{3,5},{4,6},{5,3},{6,4},{7,1},{8,10},{9,15},{10,... | collective-permute-start | bytes 786440 | tf_op jit(solution)/shard_map/ppermute | solution.py:33
  120.6 8.3 %collective-permute-start.15 = (bf16[2,64,1024]{2,1,0:T(8,128)(2,1)S(1)}, bf16[2,64,1024]{2,1,0:T(8,128)(2,1)S(1)}, u32[]{:S(2)}, u32[]{:S(2)}) collective-permute-start(bf16[2,64,1024]{2,1,0:T(8,128)(2,1)S(1)} %get-tuple-element.22), channel_id=1, source_target_pairs={{0,2},{1,7},{2,0},{3,5},{4,6},{5,3},{6,4},{7,1},{8,10},{9,15},{10,... | collective-permute-start | bytes 786440 | tf_op jit(solution)/shard_map/ppermute | solution.py:33
  124.6 7.4 %collective-permute-start.17 = (bf16[2,64,1024]{2,1,0:T(8,128)(2,1)S(1)}, bf16[2,64,1024]{2,1,0:T(8,128)(2,1)S(1)}, u32[]{:S(2)}, u32[]{:S(2)}) collective-permute-start(bf16[2,64,1024]{2,1,0:T(8,128)(2,1)S(1)} %shard_map.62), channel_id=1, source_target_pairs={{0,6},{1,3},{2,4},{3,1},{4,2},{5,7},{6,0},{7,5},{8,14},{9,11},{10,... | collective-permute-start | bytes 786440 | tf_op jit(solution)/shard_map/ppermute | solution.py:33

commit v9 on v8

--- a/solution.py
+++ b/solution.py
@@ -12,16 +12,16 @@
 VMEM = pl.BlockSpec(memory_space=pltpu.VMEM)
 
 
-UP_STEPS = (("y", 4), ("z", 4), ("y", 2), ("z", 2))
-DOWN_STEPS = (("z", 4), ("y", 4), ("z", 2), ("y", 2))
+UP_STEPS = (("z", 4), ("y", 4), ("y", 2), ("z", 2))
+DOWN_STEPS = (("y", 4), ("z", 4), ("z", 2), ("y", 2))
 
 
 def from_side(array, axis, shift):
     names, size = (("y", "core"), Y) if axis == "y" else (("rep", "z", "core"), REP * Z)
     pairs = []
     for i in range(size):
-        pairs.append(((i - shift) % size * 2, i * 2))
-        pairs.append(((i + shift) % size * 2 + 1, i * 2 + 1))
+        pairs.append(((i + shift) % size * 2, i * 2))
+        pairs.append(((i - shift) % size * 2 + 1, i * 2 + 1))
     return lax.ppermute(array, names, pairs)
 
 
@@ -96,7 +96,7 @@
 
 def place(piece, laid, whole, halved):
     z, y = lax.axis_index("z"), lax.axis_index("y")
-    sign = 2 * lax.axis_index("core") - 1
+    sign = 1 - 2 * lax.axis_index("core")
     for j, (dz, dy) in enumerate(laid):
         at_z = (z + sign * dz) & (Z - 1)
         at_y = (y + sign * dy) & (Y - 1)

time: 135 us -> 135 us (level)
  starting transfers between devices: 99.5 us -> 87 us
  waiting for transfers between devices: 22.2 us -> 34.5 us
    ppermute x14, waiting for transfers between devices: 15 us -> 27.4 us  [from_side(): return lax.ppermute(array, names, pairs)]
    ppermute x14, starting transfers between devices: 78.9 us -> 68.5 us  [from_side(): return lax.ppermute(array, names, pairs)]
    ppermute x1, starting transfers between devices: 11.9 us -> 9.85 us  [shards(): beside = lax.ppermute(theirs, 'core', [(0, 1), (1, 0)])]
  transfers between devices with their start and end apart: 18 -> 18, of which waited for: 13 -> 12; matrix products, arithmetic and copies ran while one was open for 0% -> 0% of each run, Pallas kernels for 5% -> 5%
where the time goes in v9:
time: 135 us; the launch traced here: 133 us
  starting transfers between devices  87 us (64%)
  waiting for transfers between devices  34.5 us (26%)
  Pallas kernels  9.5 us (7%)
  local copies, waits for them, and re-layouts  1.53 us (1%)
    ppermute x14, starting transfers between devices, from_side(): return lax.ppermute(array, names, pairs)  68.5 us
    ppermute x14, waiting for transfers between devices, from_side(): return lax.ppermute(array, names, pairs)  27.4 us
    ppermute x1, starting transfers between devices, shards(): beside = lax.ppermute(theirs, 'core', [(0, 1), (1, 0)])  9.85 us
    ppermute x3, starting transfers between devices, between_x(): return lax.ppermute(array, ('x', 'core'), pairs)  8.69 us
    ppermute x3, waiting for transfers between devices, between_x(): return lax.ppermute(array, ('x', 'core'), pairs)  7.03 us
  transfers between devices with their start and end apart: 18, of which 12 were waited for; matrix products, arithmetic and copies ran while one was open for 0% of the time, Pallas kernels for 5%

profile of v9, /device:TPU:1, one launch (start us, length us, event | category | flops | bytes accessed | tf_op | source)
XLA Modules:
  0.0 132.9 jit_solution(10964697806056414214)
XLA Ops:
  0.0 11.6 %collective-permute-start = (bf16[1,32,512]{2,1,0:T(8,128)(2,1)}, bf16[1,32,512]{2,1,0:T(8,128)(2,1)S(1)}, u32[]{:S(2)}, u32[]{:S(2)}) collective-permute-start(bf16[1,32,512]{2,1,0:T(8,128)(2,1)} %bitcast.5), channel_id=1, source_target_pairs={{256,0},{769,1},{320,64},{833,65},{384,128},{897,129},{448,192},{9... | collective-permute-start | bytes 98312 | tf_op jit(solution)/shard_map/ppermute | solution.py:25
  12.4 8.1 %collective-permute-done.b = bf16[1,32,512]{2,1,0:T(8,128)(2,1)S(1)} collective-permute-done((bf16[1,32,512]{2,1,0:T(8,128)(2,1)}, bf16[1,32,512]{2,1,0:T(8,128)(2,1)S(1)}, u32[]{:S(2)}, u32[]{:S(2)}) %collective-permute-start) | collective-permute-done | bytes 32800 | tf_op jit(solution)/shard_map/ppermute | solution.py:25
  20.5 7.4 %collective-permute-start.1 = (bf16[2,32,512]{2,1,0:T(8,128)(2,1)S(1)}, bf16[2,32,512]{2,1,0:T(8,128)(2,1)S(1)}, u32[]{:S(2)}, u32[]{:S(2)}) collective-permute-start(bf16[2,32,512]{2,1,0:T(8,128)(2,1)S(1)} %shard_map.48.a), channel_id=1, source_target_pairs={{32,0},{33,1},{40,8},{41,9},{48,16},{49,17},{56,24},{57,25},{0,32}... | collective-permute-start | bytes 196616 | tf_op jit(solution)/shard_map/ppermute | solution.py:25
  27.9 1.7 %collective-permute-done.1.b = bf16[2,32,512]{2,1,0:T(8,128)(2,1)S(1)} collective-permute-done((bf16[2,32,512]{2,1,0:T(8,128)(2,1)S(1)}, bf16[2,32,512]{2,1,0:T(8,128)(2,1)S(1)}, u32[]{:S(2)}, u32[]{:S(2)}) %collective-permute-start.1) | collective-permute-done | bytes 65568 | tf_op jit(solution)/shard_map/ppermute | solution.py:25
  29.6 4.7 %collective-permute-start.2 = (bf16[4,32,512]{2,1,0:T(8,128)(2,1)S(1)}, bf16[4,32,512]{2,1,0:T(8,128)(2,1)S(1)}, u32[]{:S(2)}, u32[]{:S(2)}) collective-permute-start(bf16[4,32,512]{2,1,0:T(8,128)(2,1)S(1)} %shard_map.49.a), channel_id=1, source_target_pairs={{16,0},{49,1},{24,8},{57,9},{32,16},{1,17},{40,24},{9,25},{48,32},... | collective-permute-start | bytes 393224 | tf_op jit(solution)/shard_map/ppermute | solution.py:25
  34.4 5.1 %collective-permute-start.7 = (bf16[1,32,512]{2,1,0:T(8,128)(2,1)}, bf16[1,32,512]{2,1,0:T(8,128)(2,1)S(1)}, u32[]{:S(2)}, u32[]{:S(2)}) collective-permute-start(bf16[1,32,512]{2,1,0:T(8,128)(2,1)} %bitcast.7), channel_id=1, source_target_pairs={{32,0},{33,1},{40,8},{41,9},{48,16},{49,17},{56,24},{57,25},{0,32}... | collective-permute-start | bytes 98312 | tf_op jit(solution)/shard_map/ppermute | solution.py:25
  40.3 2.9 %collective-permute-done.7.b = bf16[1,32,512]{2,1,0:T(8,128)(2,1)S(1)} collective-permute-done((bf16[1,32,512]{2,1,0:T(8,128)(2,1)}, bf16[1,32,512]{2,1,0:T(8,128)(2,1)S(1)}, u32[]{:S(2)}, u32[]{:S(2)}) %collective-permute-start.7) | collective-permute-done | bytes 32800 | tf_op jit(solution)/shard_map/ppermute | solution.py:25
  43.2 3.1 %collective-permute-start.8 = (bf16[2,32,512]{2,1,0:T(8,128)(2,1)S(1)}, bf16[2,32,512]{2,1,0:T(8,128)(2,1)S(1)}, u32[]{:S(2)}, u32[]{:S(2)}) collective-permute-start(bf16[2,32,512]{2,1,0:T(8,128)(2,1)S(1)} %shard_map.54.a), channel_id=1, source_target_pairs={{256,0},{769,1},{320,64},{833,65},{384,128},{897,129},{448,192},{9... | collective-permute-start | bytes 196616 | tf_op jit(solution)/shard_map/ppermute | solution.py:25
  46.2 5.8 %collective-permute-done.8.b = bf16[2,32,512]{2,1,0:T(8,128)(2,1)S(1)} collective-permute-done((bf16[2,32,512]{2,1,0:T(8,128)(2,1)S(1)}, bf16[2,32,512]{2,1,0:T(8,128)(2,1)S(1)}, u32[]{:S(2)}, u32[]{:S(2)}) %collective-permute-start.8) | collective-permute-done | bytes 65568 | tf_op jit(solution)/shard_map/ppermute | solution.py:25
  52.1 6.4 %collective-permute-start.9 = (bf16[4,32,512]{2,1,0:T(8,128)(2,1)S(1)}, bf16[4,32,512]{2,1,0:T(8,128)(2,1)S(1)}, u32[]{:S(2)}, u32[]{:S(2)}) collective-permute-start(bf16[4,32,512]{2,1,0:T(8,128)(2,1)S(1)} %shard_map.55.a), channel_id=1, source_target_pairs={{128,0},{897,1},{192,64},{961,65},{256,128},{1,129},{320,192},{65,... | collective-permute-start | bytes 393224 | tf_op jit(solution)/shard_map/ppermute | solution.py:25
  58.5 1.9 %collective-permute-start.3 = (bf16[8,32,512]{2,1,0:T(8,128)(2,1)S(1)}, bf16[8,32,512]{2,1,0:T(8,128)(2,1)S(1)}, u32[]{:S(2)}, u32[]{:S(2)}) collective-permute-start(bf16[8,32,512]{2,1,0:T(8,128)(2,1)S(1)} %shard_map.50.a), channel_id=1, source_target_pairs={{128,0},{897,1},{192,64},{961,65},{256,128},{1,129},{320,192},{65,... | collective-permute-start | bytes 786440 | tf_op jit(solution)/shard_map/ppermute | solution.py:25
  60.4 2.7 %collective-permute-done.9.b = bf16[4,32,512]{2,1,0:T(8,128)(2,1)S(1)} collective-permute-done((bf16[4,32,512]{2,1,0:T(8,128)(2,1)S(1)}, bf16[4,32,512]{2,1,0:T(8,128)(2,1)S(1)}, u32[]{:S(2)}, u32[]{:S(2)}) %collective-permute-start.9) | collective-permute-done | bytes 131104 | tf_op jit(solution)/shard_map/ppermute | solution.py:25
  63.1 6.1 %collective-permute-start.10 = (bf16[8,32,512]{2,1,0:T(8,128)(2,1)S(1)}, bf16[8,32,512]{2,1,0:T(8,128)(2,1)S(1)}, u32[]{:S(2)}, u32[]{:S(2)}) collective-permute-start(bf16[8,32,512]{2,1,0:T(8,128)(2,1)S(1)} %shard_map.56.a), channel_id=1, source_target_pairs={{16,0},{49,1},{24,8},{57,9},{32,16},{1,17},{40,24},{9,25},{48,32},... | collective-permute-start | bytes 786440 | tf_op jit(solution)/shard_map/ppermute | solution.py:25
  69.3 5.5 %collective-permute-start.4 = (bf16[16,32,512]{2,1,0:T(8,128)(2,1)S(1)}, bf16[16,32,512]{2,1,0:T(8,128)(2,1)S(1)}, u32[]{:S(2)}, u32[]{:S(2)}) collective-permute-start(bf16[16,32,512]{2,1,0:T(8,128)(2,1)S(1)} %shard_map.51.u0), channel_id=1, source_target_pairs={{64,0},{961,1},{128,64},{1,65},{192,128},{65,129},{256,192},{129,1... | collective-permute-start | bytes 1572872 | tf_op jit(solution)/shard_map/ppermute | solution.py:25
  75.1 3.3 %collective-permute-start.11 = (bf16[16,32,512]{2,1,0:T(8,128)(2,1)S(1)}, bf16[16,32,512]{2,1,0:T(8,128)(2,1)S(1)}, u32[]{:S(2)}, u32[]{:S(2)}) collective-permute-start(bf16[16,32,512]{2,1,0:T(8,128)(2,1)S(1)} %shard_map.57.d0), channel_id=1, source_target_pairs={{8,0},{57,1},{16,8},{1,9},{24,16},{9,17},{32,24},{17,25},{40,32},{... | collective-permute-start | bytes 1572872 | tf_op jit(solution)/shard_map/ppermute | solution.py:25
  78.4 3.9 %collective-permute-start.5 = (bf16[16,32,512]{2,1,0:T(8,128)(2,1)S(1)}, bf16[16,32,512]{2,1,0:T(8,128)(2,1)S(1)}, u32[]{:S(2)}, u32[]{:S(2)}) collective-permute-start(bf16[16,32,512]{2,1,0:T(8,128)(2,1)S(1)} %shard_map.51.u0), channel_id=1, source_target_pairs={{8,0},{57,1},{16,8},{1,9},{24,16},{9,17},{32,24},{17,25},{40,32},{... | collective-permute-start | bytes 1572872 | tf_op jit(solution)/shard_map/ppermute | solution.py:25
  82.4 1.9 %collective-permute-start.6 = (bf16[16,32,512]{2,1,0:T(8,128)(2,1)S(1)}, bf16[16,32,512]{2,1,0:T(8,128)(2,1)S(1)}, u32[]{:S(2)}, u32[]{:S(2)}) collective-permute-start(bf16[16,32,512]{2,1,0:T(8,128)(2,1)S(1)} %collective-permute-done.4.uz), channel_id=1, source_target_pairs={{8,0},{57,1},{16,8},{1,9},{24,16},{9,17},{32,24},{17,25},{40,32},{... | collective-permute-start | bytes 1572872 | tf_op jit(solution)/shard_map/ppermute | solution.py:25
  84.3 5.2 %collective-permute-start.12 = (bf16[16,32,512]{2,1,0:T(8,128)(2,1)S(1)}, bf16[16,32,512]{2,1,0:T(8,128)(2,1)S(1)}, u32[]{:S(2)}, u32[]{:S(2)}) collective-permute-start(bf16[16,32,512]{2,1,0:T(8,128)(2,1)S(1)} %shard_map.57.d0), channel_id=1, source_target_pairs={{64,0},{961,1},{128,64},{1,65},{192,128},{65,129},{256,192},{129,1... | collective-permute-start | bytes 1572872 | tf_op jit(solution)/shard_map/ppermute | solution.py:25
  89.6 2.2 %collective-permute-start.13 = (bf16[16,32,512]{2,1,0:T(8,128)(2,1)S(1)}, bf16[16,32,512]{2,1,0:T(8,128)(2,1)S(1)}, u32[]{:S(2)}, u32[]{:S(2)}) collective-permute-start(bf16[16,32,512]{2,1,0:T(8,128)(2,1)S(1)} %collective-permute-done.11.dy), channel_id=1, source_target_pairs={{64,0},{961,1},{128,64},{1,65},{192,128},{65,129},{256,192},{129,1... | collective-permute-start | bytes 1572872 | tf_op jit(solution)/shard_map/ppermute | solution.py:25
  91.9 2.1 %shard_map.46 = (bf16[512,2048]{1,0:T(8,128)(2,1)S(1)}, bf16[64,2048]{1,0:T(8,128)(2,1)S(1)}) custom-call(bf16[512,2048]{1,0:T(8,128)(2,1)S(1)} %copy-done, f32[1,2048]{1,0:T(1,128)S(1)} %bitcast.9), custom_call_target="tpu_custom_call" | custom-call | flops 16777216 | bytes 1048576 | tf_op jit(solution)/shard_map/pallas_call | solution.py:223
  94.0 3.5 %collective-permute-done.6.uzy = bf16[16,32,512]{2,1,0:T(8,128)(2,1)S(1)} collective-permute-done((bf16[16,32,512]{2,1,0:T(8,128)(2,1)S(1)}, bf16[16,32,512]{2,1,0:T(8,128)(2,1)S(1)}, u32[]{:S(2)}, u32[]{:S(2)}) %collective-permute-start.6) | collective-permute-done | bytes 524320 | tf_op jit(solution)/shard_map/ppermute | solution.py:25
  97.5 1.6 %shard_map.52.hidden = bf16[512,512]{1,0:T(8,128)(2,1)S(1)} custom-call(bf16[512,2048]{1,0:T(8,128)(2,1)S(1)} %get-tuple-element.16.normed, bf16[16,32,512]{2,1,0:T(8,128)(2,1)S(1)} %shard_map.51.u0, bf16[16,32,512]{2,1,0:T(8,128)(2,1)S(1)} %collective-permute-done.4.uz, bf16[16,32,512]{2,1,0:T(8,128)(2,1)S(1)} %collective-permute-done.5.uy, ...), custom_call_target="tpu_custom_call" | custom-call | flops 1073741824 | bytes 1048576 | tf_op jit(solution)/shard_map/pallas_call | solution.py:226
  99.1 1.2 shard_map.58
  100.3 2.3 %collective-permute-done.13.dyz = bf16[16,32,512]{2,1,0:T(8,128)(2,1)S(1)} collective-permute-done((bf16[16,32,512]{2,1,0:T(8,128)(2,1)S(1)}, bf16[16,32,512]{2,1,0:T(8,128)(2,1)S(1)}, u32[]{:S(2)}, u32[]{:S(2)}) %collective-permute-start.13) | collective-permute-done | bytes 524320 | tf_op jit(solution)/shard_map/ppermute | solution.py:25
  103.8 9.8 %collective-permute-start.14 = (bf16[2,256,1024]{2,1,0:T(8,128)(2,1)S(1)}, bf16[2,256,1024]{2,1,0:T(8,128)(2,1)S(1)}, u32[]{:S(2)}, u32[]{:S(2)}) collective-permute-start(bf16[2,256,1024]{2,1,0:T(8,128)(2,1)S(1)} %get-tuple-element.20), channel_id=1, source_target_pairs={{0,1},{1,0},{2,3},{3,2},{4,5},{5,4},{6,7},{7,6},{8,9},{9,8},{10,11... | collective-permute-start | bytes 3145736 | tf_op jit(solution)/shard_map/ppermute | solution.py:240
  113.7 2.1 %shard_map.60.own = bf16[2,256,1024]{2,1,0:T(8,128)(2,1)S(1)} custom-call(bf16[512,512]{1,0:T(8,128)(2,1)S(1)} %shard_map.52.hidden, bf16[1024,512]{1,0:T(8,128)(2,1)S(1)} %get-tuple-element.17.first, bf16[1024,512]{1,0:T(8,128)(2,1)S(1)} %get-tuple-element.19.second), custom_call_target="tpu_custom_call" | custom-call | flops 536870912 | bytes 1048576 | tf_op jit(solution)/shard_map/pallas_call | solution.py:241
  116.2 4.4 %collective-permute-start.16 = (bf16[2,64,1024]{2,1,0:T(8,128)(2,1)S(1)}, bf16[2,64,1024]{2,1,0:T(8,128)(2,1)S(1)}, u32[]{:S(2)}, u32[]{:S(2)}) collective-permute-start(bf16[2,64,1024]{2,1,0:T(8,128)(2,1)S(1)} %get-tuple-element.24), channel_id=1, source_target_pairs={{0,2},{1,7},{2,0},{3,5},{4,6},{5,3},{6,4},{7,1},{8,10},{9,15},{10,... | collective-permute-start | bytes 786440 | tf_op jit(solution)/shard_map/ppermute | solution.py:33
  120.6 2.1 %collective-permute-start.15 = (bf16[2,64,1024]{2,1,0:T(8,128)(2,1)S(1)}, bf16[2,64,1024]{2,1,0:T(8,128)(2,1)S(1)}, u32[]{:S(2)}, u32[]{:S(2)}) collective-permute-start(bf16[2,64,1024]{2,1,0:T(8,128)(2,1)S(1)} %get-tuple-element.22), channel_id=1, source_target_pairs={{0,2},{1,7},{2,0},{3,5},{4,6},{5,3},{6,4},{7,1},{8,10},{9,15},{10,... | collective-permute-start | bytes 786440 | tf_op jit(solution)/shard_map/ppermute | solution.py:33
  122.7 1.8 %collective-permute-done.16.came = bf16[2,64,1024]{2,1,0:T(8,128)(2,1)S(1)} collective-permute-done((bf16[2,64,1024]{2,1,0:T(8,128)(2,1)S(1)}, bf16[2,64,1024]{2,1,0:T(8,128)(2,1)S(1)}, u32[]{:S(2)}, u32[]{:S(2)}) %collective-permute-start.16) | collective-permute-done | bytes 262176 | tf_op jit(solution)/shard_map/ppermute | solution.py:33
  124.6 2.2 %collective-permute-start.17 = (bf16[2,64,1024]{2,1,0:T(8,128)(2,1)S(1)}, bf16[2,64,1024]{2,1,0:T(8,128)(2,1)S(1)}, u32[]{:S(2)}, u32[]{:S(2)}) collective-permute-start(bf16[2,64,1024]{2,1,0:T(8,128)(2,1)S(1)} %shard_map.62), channel_id=1, source_target_pairs={{0,6},{1,3},{2,4},{3,1},{4,2},{5,7},{6,0},{7,5},{8,14},{9,11},{10,... | collective-permute-start | bytes 786440 | tf_op jit(solution)/shard_map/ppermute | solution.py:33
  126.8 2.1 %collective-permute-done.15.came = bf16[2,64,1024]{2,1,0:T(8,128)(2,1)S(1)} collective-permute-done((bf16[2,64,1024]{2,1,0:T(8,128)(2,1)S(1)}, bf16[2,64,1024]{2,1,0:T(8,128)(2,1)S(1)}, u32[]{:S(2)}, u32[]{:S(2)}) %collective-permute-start.15) | collective-permute-done | bytes 262176 | tf_op jit(solution)/shard_map/ppermute | solution.py:33
  128.9 3.1 %collective-permute-done.17.late = bf16[2,64,1024]{2,1,0:T(8,128)(2,1)S(1)} collective-permute-done((bf16[2,64,1024]{2,1,0:T(8,128)(2,1)S(1)}, bf16[2,64,1024]{2,1,0:T(8,128)(2,1)S(1)}, u32[]{:S(2)}, u32[]{:S(2)}) %collective-permute-start.17) | collective-permute-done | bytes 262176 | tf_op jit(solution)/shard_map/ppermute | solution.py:33
  (30 shorter events, 4.4 us)
Async XLA Ops:
  0.0 91.8 %copy-start = (bf16[512,2048]{1,0:T(8,128)(2,1)S(1)}, bf16[512,2048]{1,0:T(8,128)(2,1)}, u32[]{:S(2)}) copy-start(bf16[512,2048]{1,0:T(8,128)(2,1)} %tokens.1) | copy-start | bytes 6291460
  0.0 20.5 %collective-permute-start = (bf16[1,32,512]{2,1,0:T(8,128)(2,1)}, bf16[1,32,512]{2,1,0:T(8,128)(2,1)S(1)}, u32[]{:S(2)}, u32[]{:S(2)}) collective-permute-start(bf16[1,32,512]{2,1,0:T(8,128)(2,1)} %bitcast.5), channel_id=1, source_target_pairs={{256,0},{769,1},{320,64},{833,65},{384,128},{897,129},{448,192},{9... | collective-permute-start | bytes 98312 | tf_op jit(solution)/shard_map/ppermute | solution.py:25
  11.6 0.8 copy-start.1
  20.5 9.2 %collective-permute-start.1 = (bf16[2,32,512]{2,1,0:T(8,128)(2,1)S(1)}, bf16[2,32,512]{2,1,0:T(8,128)(2,1)S(1)}, u32[]{:S(2)}, u32[]{:S(2)}) collective-permute-start(bf16[2,32,512]{2,1,0:T(8,128)(2,1)S(1)} %shard_map.48.a), channel_id=1, source_target_pairs={{32,0},{33,1},{40,8},{41,9},{48,16},{49,17},{56,24},{57,25},{0,32}... | collective-permute-start | bytes 196616 | tf_op jit(solution)/shard_map/ppermute | solution.py:25
  29.6 28.8 %collective-permute-start.2 = (bf16[4,32,512]{2,1,0:T(8,128)(2,1)S(1)}, bf16[4,32,512]{2,1,0:T(8,128)(2,1)S(1)}, u32[]{:S(2)}, u32[]{:S(2)}) collective-permute-start(bf16[4,32,512]{2,1,0:T(8,128)(2,1)S(1)} %shard_map.49.a), channel_id=1, source_target_pairs={{16,0},{49,1},{24,8},{57,9},{32,16},{1,17},{40,24},{9,25},{48,32},... | collective-permute-start | bytes 393224 | tf_op jit(solution)/shard_map/ppermute | solution.py:25
  34.4 8.8 %collective-permute-start.7 = (bf16[1,32,512]{2,1,0:T(8,128)(2,1)}, bf16[1,32,512]{2,1,0:T(8,128)(2,1)S(1)}, u32[]{:S(2)}, u32[]{:S(2)}) collective-permute-start(bf16[1,32,512]{2,1,0:T(8,128)(2,1)} %bitcast.7), channel_id=1, source_target_pairs={{32,0},{33,1},{40,8},{41,9},{48,16},{49,17},{56,24},{57,25},{0,32}... | collective-permute-start | bytes 98312 | tf_op jit(solution)/shard_map/ppermute | solution.py:25
  39.5 0.8 copy-start.2
  40.3 51.6 %copy-start.3 = (f32[2048]{0:T(1024)S(1)}, f32[2048]{0:T(1024)}, u32[]{:S(2)}) copy-start(f32[2048]{0:T(1024)} %param.5) | copy-start | bytes 24580
  43.2 8.9 %collective-permute-start.8 = (bf16[2,32,512]{2,1,0:T(8,128)(2,1)S(1)}, bf16[2,32,512]{2,1,0:T(8,128)(2,1)S(1)}, u32[]{:S(2)}, u32[]{:S(2)}) collective-permute-start(bf16[2,32,512]{2,1,0:T(8,128)(2,1)S(1)} %shard_map.54.a), channel_id=1, source_target_pairs={{256,0},{769,1},{320,64},{833,65},{384,128},{897,129},{448,192},{9... | collective-permute-start | bytes 196616 | tf_op jit(solution)/shard_map/ppermute | solution.py:25
  52.1 11.0 %collective-permute-start.9 = (bf16[4,32,512]{2,1,0:T(8,128)(2,1)S(1)}, bf16[4,32,512]{2,1,0:T(8,128)(2,1)S(1)}, u32[]{:S(2)}, u32[]{:S(2)}) collective-permute-start(bf16[4,32,512]{2,1,0:T(8,128)(2,1)S(1)} %shard_map.55.a), channel_id=1, source_target_pairs={{128,0},{897,1},{192,64},{961,65},{256,128},{1,129},{320,192},{65,... | collective-permute-start | bytes 393224 | tf_op jit(solution)/shard_map/ppermute | solution.py:25
  58.5 10.8 %collective-permute-start.3 = (bf16[8,32,512]{2,1,0:T(8,128)(2,1)S(1)}, bf16[8,32,512]{2,1,0:T(8,128)(2,1)S(1)}, u32[]{:S(2)}, u32[]{:S(2)}) collective-permute-start(bf16[8,32,512]{2,1,0:T(8,128)(2,1)S(1)} %shard_map.50.a), channel_id=1, source_target_pairs={{128,0},{897,1},{192,64},{961,65},{256,128},{1,129},{320,192},{65,... | collective-permute-start | bytes 786440 | tf_op jit(solution)/shard_map/ppermute | solution.py:25
  63.1 12.0 %collective-permute-start.10 = (bf16[8,32,512]{2,1,0:T(8,128)(2,1)S(1)}, bf16[8,32,512]{2,1,0:T(8,128)(2,1)S(1)}, u32[]{:S(2)}, u32[]{:S(2)}) collective-permute-start(bf16[8,32,512]{2,1,0:T(8,128)(2,1)S(1)} %shard_map.56.a), channel_id=1, source_target_pairs={{16,0},{49,1},{24,8},{57,9},{32,16},{1,17},{40,24},{9,25},{48,32},... | collective-permute-start | bytes 786440 | tf_op jit(solution)/shard_map/ppermute | solution.py:25
  69.3 13.0 %collective-permute-start.4 = (bf16[16,32,512]{2,1,0:T(8,128)(2,1)S(1)}, bf16[16,32,512]{2,1,0:T(8,128)(2,1)S(1)}, u32[]{:S(2)}, u32[]{:S(2)}) collective-permute-start(bf16[16,32,512]{2,1,0:T(8,128)(2,1)S(1)} %shard_map.51.u0), channel_id=1, source_target_pairs={{64,0},{961,1},{128,64},{1,65},{192,128},{65,129},{256,192},{129,1... | collective-permute-start | bytes 1572872 | tf_op jit(solution)/shard_map/ppermute | solution.py:25
  75.1 14.4 %collective-permute-start.11 = (bf16[16,32,512]{2,1,0:T(8,128)(2,1)S(1)}, bf16[16,32,512]{2,1,0:T(8,128)(2,1)S(1)}, u32[]{:S(2)}, u32[]{:S(2)}) collective-permute-start(bf16[16,32,512]{2,1,0:T(8,128)(2,1)S(1)} %shard_map.57.d0), channel_id=1, source_target_pairs={{8,0},{57,1},{16,8},{1,9},{24,16},{9,17},{32,24},{17,25},{40,32},{... | collective-permute-start | bytes 1572872 | tf_op jit(solution)/shard_map/ppermute | solution.py:25
  78.4 15.5 %collective-permute-start.5 = (bf16[16,32,512]{2,1,0:T(8,128)(2,1)S(1)}, bf16[16,32,512]{2,1,0:T(8,128)(2,1)S(1)}, u32[]{:S(2)}, u32[]{:S(2)}) collective-permute-start(bf16[16,32,512]{2,1,0:T(8,128)(2,1)S(1)} %shard_map.51.u0), channel_id=1, source_target_pairs={{8,0},{57,1},{16,8},{1,9},{24,16},{9,17},{32,24},{17,25},{40,32},{... | collective-permute-start | bytes 1572872 | tf_op jit(solution)/shard_map/ppermute | solution.py:25
  82.4 15.1 %collective-permute-start.6 = (bf16[16,32,512]{2,1,0:T(8,128)(2,1)S(1)}, bf16[16,32,512]{2,1,0:T(8,128)(2,1)S(1)}, u32[]{:S(2)}, u32[]{:S(2)}) collective-permute-start(bf16[16,32,512]{2,1,0:T(8,128)(2,1)S(1)} %collective-permute-done.4.uz), channel_id=1, source_target_pairs={{8,0},{57,1},{16,8},{1,9},{24,16},{9,17},{32,24},{17,25},{40,32},{... | collective-permute-start | bytes 1572872 | tf_op jit(solution)/shard_map/ppermute | solution.py:25
  84.3 16.0 %collective-permute-start.12 = (bf16[16,32,512]{2,1,0:T(8,128)(2,1)S(1)}, bf16[16,32,512]{2,1,0:T(8,128)(2,1)S(1)}, u32[]{:S(2)}, u32[]{:S(2)}) collective-permute-start(bf16[16,32,512]{2,1,0:T(8,128)(2,1)S(1)} %shard_map.57.d0), channel_id=1, source_target_pairs={{64,0},{961,1},{128,64},{1,65},{192,128},{65,129},{256,192},{129,1... | collective-permute-start | bytes 1572872 | tf_op jit(solution)/shard_map/ppermute | solution.py:25
  89.6 13.1 %collective-permute-start.13 = (bf16[16,32,512]{2,1,0:T(8,128)(2,1)S(1)}, bf16[16,32,512]{2,1,0:T(8,128)(2,1)S(1)}, u32[]{:S(2)}, u32[]{:S(2)}) collective-permute-start(bf16[16,32,512]{2,1,0:T(8,128)(2,1)S(1)} %collective-permute-done.11.dy), channel_id=1, source_target_pairs={{64,0},{961,1},{128,64},{1,65},{192,128},{65,129},{256,192},{129,1... | collective-permute-start | bytes 1572872 | tf_op jit(solution)/shard_map/ppermute | solution.py:25
  103.8 12.1 %collective-permute-start.14 = (bf16[2,256,1024]{2,1,0:T(8,128)(2,1)S(1)}, bf16[2,256,1024]{2,1,0:T(8,128)(2,1)S(1)}, u32[]{:S(2)}, u32[]{:S(2)}) collective-permute-start(bf16[2,256,1024]{2,1,0:T(8,128)(2,1)S(1)} %get-tuple-element.20), channel_id=1, source_target_pairs={{0,1},{1,0},{2,3},{3,2},{4,5},{5,4},{6,7},{7,6},{8,9},{9,8},{10,11... | collective-permute-start | bytes 3145736 | tf_op jit(solution)/shard_map/ppermute | solution.py:240
  116.2 8.3 %collective-permute-start.16 = (bf16[2,64,1024]{2,1,0:T(8,128)(2,1)S(1)}, bf16[2,64,1024]{2,1,0:T(8,128)(2,1)S(1)}, u32[]{:S(2)}, u32[]{:S(2)}) collective-permute-start(bf16[2,64,1024]{2,1,0:T(8,128)(2,1)S(1)} %get-tuple-element.24), channel_id=1, source_target_pairs={{0,2},{1,7},{2,0},{3,5},{4,6},{5,3},{6,4},{7,1},{8,10},{9,15},{10,... | collective-permute-start | bytes 786440 | tf_op jit(solution)/shard_map/ppermute | solution.py:33
  120.6 8.3 %collective-permute-start.15 = (bf16[2,64,1024]{2,1,0:T(8,128)(2,1)S(1)}, bf16[2,64,1024]{2,1,0:T(8,128)(2,1)S(1)}, u32[]{:S(2)}, u32[]{:S(2)}) collective-permute-start(bf16[2,64,1024]{2,1,0:T(8,128)(2,1)S(1)} %get-tuple-element.22), channel_id=1, source_target_pairs={{0,2},{1,7},{2,0},{3,5},{4,6},{5,3},{6,4},{7,1},{8,10},{9,15},{10,... | collective-permute-start | bytes 786440 | tf_op jit(solution)/shard_map/ppermute | solution.py:33
  124.6 7.4 %collective-permute-start.17 = (bf16[2,64,1024]{2,1,0:T(8,128)(2,1)S(1)}, bf16[2,64,1024]{2,1,0:T(8,128)(2,1)S(1)}, u32[]{:S(2)}, u32[]{:S(2)}) collective-permute-start(bf16[2,64,1024]{2,1,0:T(8,128)(2,1)S(1)} %shard_map.62), channel_id=1, source_target_pairs={{0,6},{1,3},{2,4},{3,1},{4,2},{5,7},{6,0},{7,5},{8,14},{9,11},{10,... | collective-permute-start | bytes 786440 | tf_op jit(solution)/shard_map/ppermute | solution.py:33
